TPU v7x, 256 devices: a 4x2x16 block of a 4x16x16 slice. The times are simulated.
256 devices in a mesh: grp: 2 (over y), sp: 32 (over z, core), tp: 4 (over x).
Axes of the slice: x: 4, y: 2, z: 16, core: 2. Of those that a mesh axis runs over, the one named last changes fastest.
The devices are a block of a 4x16x16 slice.
Arguments:
- residual: bfloat16 [45056, 2048], P(('grp', 'sp')), parts along dimension 0, may hold values from -6 to 6
- mix_input: bfloat16 [45056, 2048], P(('grp', 'sp'), 'tp'), parts along dimension 0, may hold values from -6 to 6
- gate_input: bfloat16 [45056, 2048], P(('grp', 'sp'), 'tp'), parts along dimension 0, may hold values from -6 to 6
- mix_kernel: bfloat16 [4, 2048], P(None, 'tp'), may hold values from -3 to 3
- recur_gate_map: bfloat16 [16, 128, 128], P('tp'), may hold values from -0.5 to 0.5
- input_gate_map: bfloat16 [16, 128, 128], P('tp'), may hold values from -0.5 to 0.5
- decay_param: float32 [2048], P('tp')
- jump_log: float32 [45056, 2048], P(('grp', 'sp'), 'tp'), parts along dimension 0, may hold values from -2.1 to 0
- out_weight: bfloat16 [2048, 2048], P('tp'), may hold values from -0.125 to 0.125
- mix_gain: float32 [2048], replicated, may hold values from 0.1 to 1.9
- inner_gain: float32 [2048], replicated, may hold values from 0.1 to 1.9
- final_gain: float32 [2048], replicated, may hold values from 0.1 to 1.9
- gate_weight: bfloat16 [2048, 5632], P('sp', 'tp'), may hold values from -0.125 to 0.125
- value_weight: bfloat16 [2048, 5632], P('sp', 'tp'), may hold values from -0.125 to 0.125
- gate_kernel: bfloat16 [3, 5632], P(None, 'tp'), may hold values from -3.5 to 3.5
- value_kernel: bfloat16 [3, 5632], P(None, 'tp'), may hold values from -3.5 to 3.5
- down_weight: bfloat16 [5632, 2048], P('tp', 'sp'), may hold values from -0.078125 to 0.078125
Outputs:
- layer_output: bfloat16 [45056, 2048], P(('grp', 'sp', 'tp')), parts along dimension 0
There are 2 independent parts, one for each index of `grp`. A program takes and returns all parts, laid end to end along the dimension named above; an argument that names none is the same for every part. Nothing has to cross between parts.
All inputs are finite; a program needn't handle non-finite values.
Results may differ from a plain program's by a relative error of at most 0.02.
Values may be sent and summed in bfloat16 or wider, within the bound.
No kernel may reach another device: no remote copies, remote signals or barrier semaphores. Data moves between devices by JAX's collectives and lax.ppermute only.
A program may use at most 128 MiB of HBM per device.

v0:
```python
import jax
import jax.numpy as jnp
from jax import lax
from jax.sharding import PartitionSpec as P

EPS = 1e-06
GATE_SCALE = 8.0


def turned_gather(arrays, axis, dims):
    turned = [jnp.moveaxis(a, dim, 0) for a, dim in zip(arrays, dims)]
    widths = [t[0].size for t in turned]
    both = jnp.concatenate([t.reshape(-1, w) for t, w in zip(turned, widths)], axis=1)
    filled = lax.all_gather(both, axis, axis=0, tiled=True)
    tiles = jnp.split(filled, [sum(widths[:k]) for k in range(1, len(widths))], axis=1)
    return tuple(
        (
            jnp.moveaxis(b.reshape(-1, *t.shape[1:]), 0, dim)
            for b, t, dim in zip(tiles, turned, dims)
        )
    )


def from_behind(value, axis, steps):
    count = lax.axis_size(axis)
    initial, last = (max(0, -steps), min(count, count - steps))
    return lax.ppermute(value, axis, [(source, source + steps) for source in range(initial, last)])


def copy_for_each(shard, axis):
    copies = jnp.broadcast_to(shard, (lax.axis_size(axis), *shard.shape))
    return lax.all_to_all(copies, axis, split_axis=0, concat_axis=0, tiled=True)


def collected_together(shard, axis):
    leaves = jax.tree.leaves(shard)
    order = sorted(range(len(leaves)), key=lambda k: -leaves[k].size)
    width = (1, *leaves[order[0]].shape)[-1]
    lines = [
        jnp.pad(leaves[k].reshape(-1), (0, -leaves[k].size % width)).reshape(-1, width)
        for k in order
    ]
    both, at, found = (copy_for_each(jnp.concatenate(lines), axis), 0, {})
    for k, line in zip(order, lines):
        share = both[:, at : at + len(line)].reshape(len(both), -1)
        found[k] = share[:, : leaves[k].size].reshape(-1, *leaves[k].shape)
        at += len(line)
    numbers = iter(range(len(leaves)))
    return jax.tree.map(lambda _: found[next(numbers)], shard)


def joined_by_halves(pieces, combine):
    while len(jax.tree.leaves(pieces)[0]) > 1:
        pieces = jax.vmap(combine)(
            *(jax.tree.map(lambda part: part[side::2], pieces) for side in (0, 1))
        )
    return jax.tree.map(lambda part: part[0], pieces)


def prefix(shard, axis, combine, identity):
    size, index = (lax.axis_size(axis), lax.axis_index(axis))
    passed = jnp.arange(size) < index

    def kept(part, zero, own):
        part = jnp.where(
            passed.reshape(-1, *(1 for _ in own.shape)), part, jnp.asarray(zero, own.dtype)
        )
        return part

    pieces = collected_together(shard, axis)
    return joined_by_halves(jax.tree.map(kept, pieces, identity, shard), combine)


def in_blocks(shard, dim, size):
    before, after = (shard.shape[:dim], shard.shape[dim + 1 :])
    return jnp.moveaxis(shard.reshape(*before, size, -1, *after), dim, 0)


def summed_on_arrival(shard, axis, dim):
    tiles = in_blocks(shard, dim, lax.axis_size(axis))
    arrived = lax.all_to_all(tiles, axis, split_axis=0, concat_axis=0, tiled=True)
    return arrived.astype(jnp.float32).sum(axis=0)


def laid_out(tiles, dim):
    lengths = list(tiles.shape[1:])
    lengths[dim] *= tiles.shape[0]
    return jnp.moveaxis(tiles, 0, dim).reshape(lengths)


def gather_directly(shard, axis, dim):
    return laid_out(copy_for_each(shard, axis), dim)


def norm_scale(values, gain_vec):
    values = values.astype(jnp.float32)
    return values * lax.rsqrt(jnp.mean(values * values, axis=-1, keepdims=True) + EPS) * gain_vec


def causal_taps(padded, kernel, length):
    kernel = kernel.astype(jnp.float32)
    result = jnp.zeros((length, padded.shape[1]), jnp.float32)
    for offset in range(kernel.shape[0]):
        result = result + padded[offset : offset + length] * kernel[offset]
    return result


def linear_pair(before_pair, after_pair):
    return (before_pair[0] * after_pair[0], after_pair[0] * before_pair[1] + after_pair[1])


def rounded(values):
    return lax.optimization_barrier(values.astype(jnp.bfloat16)).astype(jnp.float32)


def local(
    residual,
    mix_input,
    gate_input,
    mix_kernel,
    recur_gate_map,
    input_gate_map,
    decay_param,
    jump_log,
    out_weight,
    mix_gain,
    inner_gain,
    final_gain,
    gate_weight,
    value_weight,
    gate_kernel,
    value_kernel,
    down_weight,
):
    length = mix_input.shape[0]
    row_share = length // lax.axis_size("tp")
    column_index = lax.axis_index("tp")
    gate_whole, value_whole, down_whole = turned_gather(
        (gate_weight, value_weight, down_weight), "sp", (0, 0, 1)
    )
    mix_taps = mix_kernel.shape[0]
    mix_edge = from_behind(mix_input[length - mix_taps + 1 :], "sp", 1)
    padded = jnp.concatenate([mix_edge, mix_input], axis=0).astype(jnp.float32)
    conv_rows = causal_taps(padded, mix_kernel, length).astype(jnp.bfloat16)
    groups = recur_gate_map.shape[0]
    block_width = recur_gate_map.shape[1]
    grouped = conv_rows.reshape(length, groups, block_width)
    recur_gate = jax.nn.sigmoid(
        jnp.einsum("tnd,nde->tne", grouped, recur_gate_map, preferred_element_type=jnp.float32)
    ).reshape(length, groups * block_width)
    input_gate = jax.nn.sigmoid(
        jnp.einsum("tnd,nde->tne", grouped, input_gate_map, preferred_element_type=jnp.float32)
    ).reshape(length, groups * block_width)
    log_decay = -GATE_SCALE * recur_gate * jax.nn.softplus(-decay_param) + jump_log
    drive = jnp.sqrt(-jnp.expm1(2.0 * log_decay)) * input_gate * conv_rows.astype(jnp.float32)
    cumulative, local_state = lax.associative_scan(linear_pair, (jnp.exp(log_decay), drive), axis=0)
    block_end = (cumulative[length - 1], local_state[length - 1])
    carried = prefix(
        block_end, "sp", linear_pair, (jnp.ones_like(block_end[0]), jnp.zeros_like(block_end[1]))
    )
    state = local_state + cumulative * carried[1]
    branch = (state * jax.nn.gelu(gate_input.astype(jnp.float32), approximate=True)).astype(
        jnp.bfloat16
    )
    chosen = branch
    mixed = summed_on_arrival(
        rounded(jnp.dot(chosen, out_weight, preferred_element_type=jnp.float32)).astype(
            jnp.bfloat16
        ),
        "tp",
        0,
    ).astype(jnp.bfloat16)
    own_rows = lax.dynamic_slice_in_dim(residual, column_index * row_share, row_share, 0)
    hidden_state = (own_rows.astype(jnp.float32) + norm_scale(mixed, mix_gain)).astype(jnp.bfloat16)
    normed = gather_directly(norm_scale(hidden_state, inner_gain).astype(jnp.bfloat16), "tp", 0)
    up_gate = jnp.dot(normed, gate_whole, preferred_element_type=jnp.float32).astype(jnp.bfloat16)
    up_value = jnp.dot(normed, value_whole, preferred_element_type=jnp.float32).astype(jnp.bfloat16)
    hidden_taps = gate_kernel.shape[0]
    tails = jnp.stack([up_gate[length - hidden_taps + 1 :], up_value[length - hidden_taps + 1 :]])
    hidden_edge = from_behind(tails, "sp", 1)
    gate_conv = causal_taps(
        jnp.concatenate([hidden_edge[0], up_gate], axis=0).astype(jnp.float32), gate_kernel, length
    )
    value_conv = causal_taps(
        jnp.concatenate([hidden_edge[1], up_value], axis=0).astype(jnp.float32),
        value_kernel,
        length,
    )
    activation = (jax.nn.gelu(gate_conv, approximate=True) * value_conv).astype(jnp.bfloat16)
    chosen = activation
    down_sum = summed_on_arrival(
        rounded(jnp.dot(chosen, down_whole, preferred_element_type=jnp.float32)).astype(
            jnp.bfloat16
        ),
        "tp",
        0,
    )
    down = down_sum.astype(jnp.bfloat16)
    return (hidden_state.astype(jnp.float32) + norm_scale(down, final_gain)).astype(jnp.bfloat16)


def solution(mesh):
    return jax.shard_map(
        local,
        mesh=mesh,
        in_specs=(
            P(("grp", "sp"), None),
            P(("grp", "sp"), "tp"),
            P(("grp", "sp"), "tp"),
            P(None, "tp"),
            P("tp", None, None),
            P("tp", None, None),
            P("tp"),
            P(("grp", "sp"), "tp"),
            P("tp", None),
            P(),
            P(),
            P(),
            P("sp", "tp"),
            P("sp", "tp"),
            P(None, "tp"),
            P(None, "tp"),
            P("tp", "sp"),
        ),
        out_specs=P(("grp", "sp", "tp"), None),
        check_vma=False,
    )
```

profile of v0, /device:TPU:33, one launch (start us, length us, event | category | flops | bytes accessed | tf_op | source)
XLA Modules:
  0.0 335.7 jit_solution(13415458491723378446)
XLA Ops:
  6.6 2.2 pad_maximum_fusion.2
  8.9 5.7 %collective-permute-start = (bf16[3,512]{1,0:T(4,128)(2,1)S(1)}, bf16[3,512]{1,0:T(4,128)(2,1)S(1)}, u32[]{:S(2)}, u32[]{:S(2)}) collective-permute-start(bf16[3,512]{1,0:T(4,128)(2,1)S(1)} %slice.393), channel_id=1, source_target_pairs={{0,4},{4,8},{8,12},{12,16},{16,20},{20,24},{24,28},{28,32},{32,36}... | collective-permute-start | bytes 9224 | tf_op jit(solution)/shard_map/ppermute | solution.py:27
  14.7 16.6 %collective-permute-done = bf16[3,512]{1,0:T(4,128)(2,1)S(1)} collective-permute-done((bf16[3,512]{1,0:T(4,128)(2,1)S(1)}, bf16[3,512]{1,0:T(4,128)(2,1)S(1)}, u32[]{:S(2)}, u32[]{:S(2)}) %collective-permute-start) | collective-permute-done | bytes 3104 | tf_op jit(solution)/shard_map/ppermute | solution.py:27
  34.6 2.8 fusion.64
  38.2 4.9 %slice.466 = f32[351,512]{1,0:T(8,128)} slice(f32[704,512]{1,0:T(8,128)} %get-tuple-element.17), slice={[2:704:2], [0:512:1]} | slice | bytes 1437696 | tf_op jit(solution)/shard_map/slice | solution.py:156
  43.0 4.7 %slice.406 = f32[352,512]{1,0:T(8,128)} slice(f32[704,512]{1,0:T(8,128)} %get-tuple-element.17), slice={[1:704:2], [0:512:1]} | slice | bytes 1441792 | tf_op jit(solution)/shard_map/slice | solution.py:156
  47.8 4.7 %slice.405 = f32[352,512]{1,0:T(8,128)} slice(f32[704,512]{1,0:T(8,128)} %get-tuple-element.17), slice={[0:703:2], [0:512:1]} | slice | bytes 1441792 | tf_op jit(solution)/shard_map/slice | solution.py:156
  52.5 2.7 slice.408
  55.2 2.7 slice.404
  58.0 2.8 slice.403
  60.7 2.1 multiply_add_fusion
  62.8 1.5 slice.464
  64.3 1.4 slice.412
  65.7 1.4 slice.411
  67.2 1.4 slice.414
  68.6 1.4 slice.410
  70.0 1.5 slice.409
  71.5 1.2 multiply_add_fusion.1
  79.2 1.0 pad.141
  81.8 1.0 fusion.82
  82.9 0.8 copy-done.13
  84.5 1.1 pad.124
  85.7 2.8 pad.125
  88.5 2.8 pad.143
  91.3 2.2 add.323
  93.5 1.0 add.313
  95.3 1.4 fusion.73
  96.8 3.1 pad.144
  100.0 3.0 pad.126
  103.0 3.1 pad.127
  106.1 3.0 pad.145
  109.1 0.9 slice_add_fusion.1
  111.4 8.1 %all-to-all-start = ((f32[32,2,512]{2,1,0:T(2,128)}), f32[32,2,512]{2,1,0:T(2,128)}, u32[]{:S(2)}, u32[]{:S(2)}) async-start(f32[32,2,512]{2,1,0:T(2,128)} %broadcast_in_dim.34), calls=%async_computation | async-start | bytes 262144 | tf_op jit(solution)/shard_map/all_to_all | solution.py:32
  119.5 18.0 %all-to-all-done = f32[32,2,512]{2,1,0:T(2,128)} async-done(((f32[32,2,512]{2,1,0:T(2,128)}), f32[32,2,512]{2,1,0:T(2,128)}, u32[]{:S(2)}, u32[]{:S(2)}) %all-to-all-start) | async-done | bytes 131104 | tf_op jit(solution)/shard_map/all_to_all | solution.py:32
  137.5 1.1 fusion.100
  139.3 1.5 slice.486
  140.8 1.4 slice.485
  142.2 1.5 slice.496
  143.7 1.5 slice.495
  145.1 1.4 fusion.101
  146.6 1.4 slice.488
  147.9 1.4 slice.487
  149.3 1.4 slice.498
  150.7 1.4 slice.497
  152.0 1.4 fusion.102
  153.4 1.3 slice.490
  154.7 1.3 slice.489
  160.7 6.1 %convolution_convert_fusion = bf16[704,2048]{1,0:T(8,128)(2,1)} fusion(bf16[512,2048]{1,0:T(8,128)(2,1)S(1)} %copy-done, bf16[704,512]{1,0:T(8,128)(2,1)} %param.19, f32[704,512]{1,0:T(8,128)S(1)} %copy-done.9, f32[704,512]{1,0:T(8,128)} %pad.145, f32[704,512]{1,0:T(8,128)} %pad.126, f32[704,512]{1,0:T(8,128)} %pad.127, f32[512]{0:T(512)S(1)} %bitcast.64), kind=kOutput, calls=%fused_computation.26 | convolution fusion | flops 1483243520 | bytes 11470848 | tf_op jit(solution)/shard_map/dot_general | solution.py:167
  166.7 4.3 %all-to-all-start.1 = ((bf16[4,176,2048]{2,1,0:T(8,128)(2,1)}), bf16[4,176,2048]{2,1,0:T(8,128)(2,1)S(1)}, u32[]{:S(2)}, u32[]{:S(2)}) async-start(bf16[4,176,2048]{2,1,0:T(8,128)(2,1)} %bitcast.53), calls=%async_computation.1 | async-start | bytes 5767168 | tf_op jit(solution)/shard_map/all_to_all | solution.py:81
  171.0 33.6 %all-to-all-done.1 = bf16[4,176,2048]{2,1,0:T(8,128)(2,1)S(1)} async-done(((bf16[4,176,2048]{2,1,0:T(8,128)(2,1)}), bf16[4,176,2048]{2,1,0:T(8,128)(2,1)S(1)}, u32[]{:S(2)}, u32[]{:S(2)}) %all-to-all-start.1) | async-done | bytes 2883616 | tf_op jit(solution)/shard_map/all_to_all | solution.py:81
  204.6 1.6 reduce_sum.51
  206.2 1.3 fusion.47
  207.5 1.8 fusion.53
  209.6 2.0 broadcast_in_dim.37
  211.6 4.9 %all-to-all-start.2 = ((bf16[4,176,2048]{2,1,0:T(8,128)(2,1)}), bf16[4,176,2048]{2,1,0:T(8,128)(2,1)}, u32[]{:S(2)}, u32[]{:S(2)}) async-start(bf16[4,176,2048]{2,1,0:T(8,128)(2,1)} %broadcast_in_dim.37), calls=%async_computation.2 | async-start | bytes 5767168 | tf_op jit(solution)/shard_map/all_to_all | solution.py:32
  216.5 32.7 %all-to-all-done.2 = bf16[4,176,2048]{2,1,0:T(8,128)(2,1)} async-done(((bf16[4,176,2048]{2,1,0:T(8,128)(2,1)}), bf16[4,176,2048]{2,1,0:T(8,128)(2,1)}, u32[]{:S(2)}, u32[]{:S(2)}) %all-to-all-start.2) | async-done | bytes 2883616 | tf_op jit(solution)/shard_map/all_to_all | solution.py:32
  249.2 8.3 %fusion.19 = bf16[704,1408]{1,0:T(8,128)(2,1)S(1)} fusion(bf16[704,2048]{1,0:T(8,128)(2,1)} %bitcast.9, bf16[2048,4224]{1,0:T(8,128)(2,1)} %all-gather.2.cloned.1.call-done), kind=kOutput, calls=%fused_computation.27 | convolution fusion | flops 4061077504 | bytes 10633216 | tf_op jit(solution)/shard_map/dot_general | solution.py:176
  257.6 6.5 %fusion.22 = bf16[704,1408]{1,0:T(8,128)(2,1)S(1)} fusion(bf16[704,2048]{1,0:T(8,128)(2,1)} %bitcast.9, bf16[2048,4224]{1,0:T(8,128)(2,1)S(1)} %copy-done.25), kind=kOutput, calls=%fused_computation.28 | convolution fusion | flops 4061077504 | bytes 10633216 | tf_op jit(solution)/shard_map/dot_general | solution.py:177
  264.1 4.4 %collective-permute-start.1 = (bf16[2,2,1408]{2,1,0:T(2,128)(2,1)S(1)}, bf16[2,2,1408]{2,1,0:T(2,128)(2,1)S(1)}, u32[]{:S(2)}, u32[]{:S(2)}) collective-permute-start(bf16[2,2,1408]{2,1,0:T(2,128)(2,1)S(1)} %pad_maximum_fusion.15), channel_id=1, source_target_pairs={{0,4},{4,8},{8,12},{12,16},{16,20},{20,24},{24,28},{28,32},{32,36}... | collective-permute-start | bytes 33800 | tf_op jit(solution)/shard_map/ppermute | solution.py:27
  269.5 2.3 maximum_convert_fusion.1
  271.8 13.3 %fusion.25 = bf16[704,2048]{1,0:T(8,128)(2,1)} fusion(bf16[2048,4224]{1,0:T(8,128)(2,1)} %all-gather.2.cloned.1.call-done, f32[706,1408]{1,0:T(8,128)} %maximum_convert_fusion.1, f32[706,1408]{1,0:T(8,128)S(1)} %maximum_convert_fusion, f32[1408]{0:T(1024)S(1)} %get-tuple-element.9, f32[1408]{0:T(1024)S(1)} %get-tuple-element.10, ...), kind=kOutput, calls=%fused_computation.29 | convolution fusion | flops 4081352704 | bytes 32489472 | tf_op jit(solution)/shard_map/dot_general | solution.py:192
  285.2 39.6 %all_to_all.20 = bf16[4,176,2048]{2,1,0:T(8,128)(2,1)} all-to-all(bf16[4,176,2048]{2,1,0:T(8,128)(2,1)} %bitcast.54), channel_id=1, replica_groups=mesh['grp'=2,'sp'=32,'tp'=4] {'tp'}, dimensions={0} | all-to-all | bytes 5767168 | tf_op jit(solution)/shard_map/all_to_all | solution.py:81
  324.8 2.6 reduce_sum.54
  327.6 1.3 fusion.56
  (207 shorter events, 22.0 us)
Async XLA Ops:
  6.5 154.1 %copy-start = (bf16[512,2048]{1,0:T(8,128)(2,1)S(1)}, bf16[512,2048]{1,0:T(8,128)(2,1)}, u32[]{:S(2)}) copy-start(bf16[512,2048]{1,0:T(8,128)(2,1)} %param.25) | copy-start | bytes 6291460
  6.6 2.3 copy-start.16
  6.6 8.1 %copy-start.17 = (bf16[4,512]{1,0:T(4,128)(2,1)S(1)}, bf16[4,512]{1,0:T(4,128)(2,1)}, u32[]{:S(2)}) copy-start(bf16[4,512]{1,0:T(4,128)(2,1)} %param.20) | copy-start | bytes 12292
  6.6 8.1 %copy-start.24 = (f32[512]{0:T(512)S(1)}, f32[512]{0:T(512)}, u32[]{:S(2)}) copy-start(f32[512]{0:T(512)} %param.23) | copy-start | bytes 6148
  6.6 242.6 %all-gather.2.cloned.1.call-start = ((), (), s32[]{:S(2)}) async-start(), calls=%async_computation.4 | async-start | bytes 17842176 | tf_op jit(solution)/shard_map/all_gather | solution.py:14
  8.9 22.4 %collective-permute-start = (bf16[3,512]{1,0:T(4,128)(2,1)S(1)}, bf16[3,512]{1,0:T(4,128)(2,1)S(1)}, u32[]{:S(2)}, u32[]{:S(2)}) collective-permute-start(bf16[3,512]{1,0:T(4,128)(2,1)S(1)} %slice.393), channel_id=1, source_target_pairs={{0,4},{4,8},{8,12},{12,16},{16,20},{20,24},{24,28},{28,32},{32,36}... | collective-permute-start | bytes 9224 | tf_op jit(solution)/shard_map/ppermute | solution.py:27
  31.4 0.9 copy-start.26
  32.4 0.9 copy-start.27
  33.3 1.4 copy-start.10
  67.2 4.3 %copy-start.14 = (f32[176,512]{1,0:T(8,128)S(1)}, f32[176,512]{1,0:T(8,128)}, u32[]{:S(2)}) copy-start(f32[176,512]{1,0:T(8,128)} %slice.412) | copy-start | bytes 1081348
  67.2 4.3 %copy-start.15 = (f32[176,512]{1,0:T(8,128)S(1)}, f32[176,512]{1,0:T(8,128)}, u32[]{:S(2)}) copy-start(f32[176,512]{1,0:T(8,128)} %slice.411) | copy-start | bytes 1081348
  77.4 0.8 copy-start.23
  80.2 1.6 copy-start.11
  80.2 1.6 copy-start.12
  82.8 1.0 copy-start.13
  91.3 2.2 copy-start.2
  93.5 1.3 copy-start.3
  93.5 1.6 copy-start.6
  93.5 1.8 copy-start.7
  96.8 3.1 copy-start.8
  99.9 3.0 copy-start.5
  103.0 3.1 copy-start.4
  109.1 51.5 %copy-start.9 = (f32[704,512]{1,0:T(8,128)S(1)}, f32[704,512]{1,0:T(8,128)}, u32[]{:S(2)}) copy-start(f32[704,512]{1,0:T(8,128)} %pad.144) | copy-start | bytes 4325380
  111.4 26.0 %all-to-all-start = ((f32[32,2,512]{2,1,0:T(2,128)}), f32[32,2,512]{2,1,0:T(2,128)}, u32[]{:S(2)}, u32[]{:S(2)}) async-start(f32[32,2,512]{2,1,0:T(2,128)} %broadcast_in_dim.34), calls=%async_computation | async-start | bytes 262144 | tf_op jit(solution)/shard_map/all_to_all | solution.py:32
  166.7 37.8 %all-to-all-start.1 = ((bf16[4,176,2048]{2,1,0:T(8,128)(2,1)}), bf16[4,176,2048]{2,1,0:T(8,128)(2,1)S(1)}, u32[]{:S(2)}, u32[]{:S(2)}) async-start(bf16[4,176,2048]{2,1,0:T(8,128)(2,1)} %bitcast.53), calls=%async_computation.1 | async-start | bytes 5767168 | tf_op jit(solution)/shard_map/all_to_all | solution.py:81
  171.0 36.5 %copy-start.20 = (f32[2048]{0:T(1024)S(1)}, f32[2048]{0:T(1024)}, u32[]{:S(2)}) copy-start(f32[2048]{0:T(1024)} %param.26) | copy-start | bytes 24580
  206.1 3.2 copy-start.21
  211.6 4.9 %copy-start.18 = (bf16[3,1408]{1,0:T(4,128)(2,1)S(1)}, bf16[3,1408]{1,0:T(4,128)(2,1)}, u32[]{:S(2)}) copy-start(bf16[3,1408]{1,0:T(4,128)(2,1)} %param.31) | copy-start | bytes 25348
  211.6 4.9 %copy-start.19 = (bf16[3,1408]{1,0:T(4,128)(2,1)S(1)}, bf16[3,1408]{1,0:T(4,128)(2,1)}, u32[]{:S(2)}) copy-start(bf16[3,1408]{1,0:T(4,128)(2,1)} %param.32) | copy-start | bytes 25348
  211.6 37.6 %all-to-all-start.2 = ((bf16[4,176,2048]{2,1,0:T(8,128)(2,1)}), bf16[4,176,2048]{2,1,0:T(8,128)(2,1)}, u32[]{:S(2)}, u32[]{:S(2)}) async-start(bf16[4,176,2048]{2,1,0:T(8,128)(2,1)} %broadcast_in_dim.37), calls=%async_computation.2 | async-start | bytes 5767168 | tf_op jit(solution)/shard_map/all_to_all | solution.py:32
  249.2 8.4 %copy-start.25 = (bf16[2048,4224]{1,0:T(8,128)(2,1)S(1)}, bf16[2048,4224]{1,0:T(8,128)(2,1)}, u32[]{:S(2)}) copy-start(bf16[2048,4224]{1,0:T(8,128)(2,1)} %all-gather.2.cloned.1.call-done) | copy-start | bytes 51904516
  264.1 5.0 %collective-permute-start.1 = (bf16[2,2,1408]{2,1,0:T(2,128)(2,1)S(1)}, bf16[2,2,1408]{2,1,0:T(2,128)(2,1)S(1)}, u32[]{:S(2)}, u32[]{:S(2)}) collective-permute-start(bf16[2,2,1408]{2,1,0:T(2,128)(2,1)S(1)} %pad_maximum_fusion.15), channel_id=1, source_target_pairs={{0,4},{4,8},{8,12},{12,16},{16,20},{20,24},{24,28},{28,32},{32,36}... | collective-permute-start | bytes 33800 | tf_op jit(solution)/shard_map/ppermute | solution.py:27
  324.8 2.8 copy-start.22
  324.8 4.1 %copy-start.1 = (bf16[512,2048]{1,0:T(8,128)(2,1)S(1)}, bf16[512,2048]{1,0:T(8,128)(2,1)}, u32[]{:S(2)}) copy-start(bf16[512,2048]{1,0:T(8,128)(2,1)} %param.25) | copy-start | bytes 6291460
Sparse Core Ops, SparseCore 0:
  9.2 128.0 all-gather.1
where the time goes:
time: 338 us; the launch traced here: 336 us
  waiting for transfers between devices  101 us (30%)
  local copies, waits for them, and re-layouts  79.5 us (24%)
  blocking collectives  39.6 us (12%)
  other arithmetic  38.3 us (11%)
  matrix products  35.2 us (10%)
  starting transfers between devices  27.3 us (8%)
  between operations  14.4 us (4%)
    all_to_all x2, waiting for transfers between devices, copy_for_each(): return lax.all_to_all(copies, axis, split_axis=0, concat_axis=0, tiled=True)  50.6 us
    all_to_all x1, blocking collectives, summed_on_arrival(): lax.all_to_all(tiles, axis, split_axis=0, concat_axis=0, tiled=True)  39.6 us
    slice x64, local copies, waits for them, and re-layouts, local(): lax.associative_scan(linear_pair, (jnp.exp(log_decay), drive), axis=0)  35.4 us
    all_to_all x1, waiting for transfers between devices, summed_on_arrival(): lax.all_to_all(tiles, axis, split_axis=0, concat_axis=0, tiled=True)  33.6 us
    pad x32, local copies, waits for them, and re-layouts, local(): lax.associative_scan(linear_pair, (jnp.exp(log_decay), drive), axis=0)  20.6 us
    ppermute x2, waiting for transfers between devices, from_behind(): lax.ppermute(value, axis, [(source, source + steps) for source in range(i...  17 us
    slice x16, local copies, waits for them, and re-layouts, joined_by_halves(): part[side::2]  16.4 us
    dot_general x1, matrix products, local(): jnp.dot(chosen, down_whole, preferred_element_type=jnp.float32)  13.3 us
  transfers between devices with their start and end apart: 6, of which 5 were waited for; matrix products, arithmetic and copies ran while one was open for 34% of the time, Pallas kernels for 0%

commit v1 on v0

v1 whole, which is shorter than its diff:
```python
import functools

import jax
import jax.numpy as jnp
from jax import lax
from jax.experimental import pallas as pl
from jax.experimental.pallas import tpu as pltpu
from jax.sharding import PartitionSpec as P

EPS = 1e-06
GATE_SCALE = 8.0
SEGMENTS = 8
LANES = 128
GELU_A = 0.7978845608028654
GELU_B = 0.044715


def gelu(v):
    return 0.5 * v * (1.0 + jnp.tanh(GELU_A * (v + GELU_B * (v * v * v))))


def minus_expm1(y):
    series = 1.0 + y * (1.0 / 7.0)
    for n in (6.0, 5.0, 4.0, 3.0, 2.0):
        series = 1.0 + y * (1.0 / n) * series
    return jnp.where(y > -0.3, -y * series, 1.0 - jnp.exp(y))


def sigmoid(v):
    return 0.5 * jnp.tanh(0.5 * v) + 0.5


def scan_kernel(
    x_ref, edge_ref, taps_ref, rmap_ref, imap_ref, soft_ref, jump_ref,
    cum_ref, loc_ref, seg_ref, ends_ref,
    xs, decay, drive,
):
    group = pl.program_id(0)
    groups = pl.num_programs(0)
    length = x_ref.shape[0]
    taps = taps_ref.shape[0]
    xs[0:8, :] = edge_ref[...].astype(jnp.float32)
    xs[8 : 8 + length, :] = x_ref[...].astype(jnp.float32)
    rows = length // 4
    kernel = taps_ref[...].astype(jnp.float32)
    soft = soft_ref[...]
    for at in range(0, length, rows):
        conv = jnp.zeros((rows, LANES), jnp.float32)
        for k in range(taps):
            first = 8 + at - (taps - 1) + k
            conv = conv + xs[first : first + rows, :] * kernel[k : k + 1, :]
        conv = conv.astype(jnp.bfloat16)
        rgate = sigmoid(jnp.dot(conv, rmap_ref[0], preferred_element_type=jnp.float32))
        igate = sigmoid(jnp.dot(conv, imap_ref[0], preferred_element_type=jnp.float32))
        log_decay = -GATE_SCALE * rgate * soft + jump_ref[at : at + rows, :]
        decay[at : at + rows, :] = jnp.exp(log_decay)
        drive[at : at + rows, :] = (
            jnp.sqrt(minus_expm1(2.0 * log_decay)) * igate * conv.astype(jnp.float32)
        )
    steps = length // SEGMENTS

    def step(i, carry):
        state, product = carry
        where = pl.ds(i, SEGMENTS, steps)
        a = decay[where, :]
        state = a * state + drive[where, :]
        product = a * product
        loc_ref[where, :] = state
        cum_ref[where, :] = product
        return state, product

    zero = jnp.zeros((SEGMENTS, LANES), jnp.float32)
    state, product = lax.fori_loop(0, steps, step, (zero, zero + 1.0), unroll=8)
    seg_ref[0, :, :] = product
    seg_ref[1, :, :] = state
    all_state = state[0:1]
    all_product = product[0:1]
    for s in range(1, SEGMENTS):
        all_state = product[s : s + 1] * all_state + state[s : s + 1]
        all_product = product[s : s + 1] * all_product
    count = ends_ref.shape[0]
    ends_ref[:, pl.ds(group, 1), :] = jnp.broadcast_to(all_product[None], (count, 1, LANES))
    ends_ref[:, pl.ds(groups + group, 1), :] = jnp.broadcast_to(all_state[None], (count, 1, LANES))


def local_scan(x, edge, taps, rmap, imap, soft, jump, copies):
    length, channels = x.shape
    groups = channels // LANES
    column = lambda rows: pl.BlockSpec((rows, LANES), lambda g: (0, g))
    square = pl.BlockSpec((1, LANES, LANES), lambda g: (g, 0, 0))
    return pl.pallas_call(
        scan_kernel,
        grid=(groups,),
        in_specs=[column(length), column(8), column(taps.shape[0]), square, square, column(1), column(length)],
        out_specs=[
            column(length),
            column(length),
            pl.BlockSpec((2, SEGMENTS, LANES), lambda g: (0, 0, g)),
            pl.BlockSpec((copies, 2 * groups, LANES), lambda g: (0, 0, 0)),
        ],
        out_shape=[
            jax.ShapeDtypeStruct((length, channels), jnp.float32),
            jax.ShapeDtypeStruct((length, channels), jnp.float32),
            jax.ShapeDtypeStruct((2, SEGMENTS, channels), jnp.float32),
            jax.ShapeDtypeStruct((copies, 2 * groups, LANES), jnp.float32),
        ],
        scratch_shapes=[
            pltpu.VMEM((length + 8, LANES), jnp.float32),
            pltpu.VMEM((length, LANES), jnp.float32),
            pltpu.VMEM((length, LANES), jnp.float32),
        ],
        name="local_scan",
    )(x, edge, taps, rmap, imap, soft, jump)


def branch_kernel(me_ref, arrived_ref, seg_ref, cum_ref, loc_ref, gate_ref, w_ref, out_ref, carry, branch):
    block = pl.program_id(0)
    groups = cum_ref.shape[1] // LANES
    count = arrived_ref.shape[0]
    rows = cum_ref.shape[0]
    seg_rows = rows * pl.num_programs(0) // SEGMENTS
    per_block = rows // seg_rows

    @pl.when(block == 0)
    def _():
        def join(j, state):
            return arrived_ref[j, 0:groups, :] * state + arrived_ref[j, groups : 2 * groups, :]

        state = lax.fori_loop(0, me_ref[0], join, jnp.zeros((groups, LANES), jnp.float32))
        for g in range(groups):
            lanes = slice(g * LANES, (g + 1) * LANES)
            now = state[g : g + 1, :]
            for s in range(SEGMENTS):
                carry[s, 0:1, lanes] = now
                now = seg_ref[0, s : s + 1, lanes] * now + seg_ref[1, s : s + 1, lanes]

    for part in range(per_block):
        at = slice(part * seg_rows, (part + 1) * seg_rows)
        state = loc_ref[at, :] + cum_ref[at, :] * carry[block * per_block + part, 0:1, :]
        branch[at, :] = state
    gate = gate_ref[...].astype(jnp.float32)
    out = (branch[...] * gelu(gate)).astype(jnp.bfloat16)
    out_ref[0] = jnp.dot(out, w_ref[...], preferred_element_type=jnp.float32).astype(jnp.bfloat16)


def branch_shares(me, arrived, seg, cum, loc, gate, weight, blocks):
    length, channels = cum.shape
    width = weight.shape[1]
    rows = length // blocks
    row_block = pl.BlockSpec((rows, channels), lambda b: (b, 0))
    whole = lambda a: pl.BlockSpec(a.shape, lambda b: (0,) * a.ndim)
    return pl.pallas_call(
        branch_kernel,
        grid=(blocks,),
        in_specs=[
            pl.BlockSpec(memory_space=pltpu.SMEM),
            whole(arrived), whole(seg), row_block, row_block, row_block, whole(weight),
        ],
        out_specs=pl.BlockSpec((1, rows, width), lambda b: (b, 0, 0)),
        out_shape=jax.ShapeDtypeStruct((blocks, rows, width), jnp.bfloat16),
        scratch_shapes=[
            pltpu.VMEM((SEGMENTS, 1, channels), jnp.float32),
            pltpu.VMEM((rows, channels), jnp.float32),
        ],
        name="branch_shares",
    )(me, arrived, seg, cum, loc, gate, weight)


def scaled(v, gain):
    return v * lax.rsqrt(jnp.mean(v * v, axis=-1, keepdims=True) + EPS) * gain


def arrived_sum(ref):
    total = ref[0].astype(jnp.float32)
    for k in range(1, ref.shape[0]):
        total = total + ref[k].astype(jnp.float32)
    return total.astype(jnp.bfloat16).astype(jnp.float32)


def mid_kernel(me_ref, shares_ref, res_ref, mix_ref, inner_ref, hidden_ref, normed_ref):
    hidden = (
        res_ref[...].astype(jnp.float32) + scaled(arrived_sum(shares_ref), mix_ref[...])
    ).astype(jnp.bfloat16)
    hidden_ref[...] = hidden
    normed_ref[...] = scaled(hidden.astype(jnp.float32), inner_ref[...]).astype(jnp.bfloat16)


def mid(me, shares, residual, mix_gain, inner_gain):
    count, rows, width = shares.shape
    gain = pl.BlockSpec((1, width), lambda i, me: (0, 0))
    steps = 1
    some = pl.BlockSpec((rows // steps, width), lambda i, me: (i, 0))
    return pl.pallas_call(
        mid_kernel,
        grid_spec=pltpu.PrefetchScalarGridSpec(
            num_scalar_prefetch=1,
            grid=(steps,),
            in_specs=[
                pl.BlockSpec((count, rows // steps, width), lambda i, me: (0, i, 0)),
                pl.BlockSpec((rows // steps, width), lambda i, me: (me[0] * steps + i, 0)),
                gain,
                gain,
            ],
            out_specs=[some, some],
        ),
        out_shape=[jax.ShapeDtypeStruct((rows, width), jnp.bfloat16)] * 2,
        name="mid",
    )(me, shares, residual, mix_gain, inner_gain)


def last_kernel(shares_ref, hidden_ref, gain_ref, out_ref):
    out_ref[...] = (
        hidden_ref[...].astype(jnp.float32) + scaled(arrived_sum(shares_ref), gain_ref[...])
    ).astype(jnp.bfloat16)


def last(shares, hidden, gain):
    return pl.pallas_call(
        last_kernel,
        out_shape=jax.ShapeDtypeStruct(hidden.shape, jnp.bfloat16),
        name="last",
    )(shares, hidden, gain)


def from_behind(value, axis):
    count = lax.axis_size(axis)
    return lax.ppermute(value, axis, [(i, i + 1) for i in range(count - 1)])


def exchanged(tiles, axis):
    return lax.all_to_all(tiles, axis, split_axis=0, concat_axis=0, tiled=True)


def causal_taps(padded, kernel, length):
    kernel = kernel.astype(jnp.float32)
    result = jnp.zeros((length, padded.shape[1]), jnp.float32)
    for offset in range(kernel.shape[0]):
        result = result + padded[offset : offset + length] * kernel[offset]
    return result


def local(
    residual,
    mix_input,
    gate_input,
    mix_kernel,
    recur_gate_map,
    input_gate_map,
    decay_param,
    jump_log,
    out_weight,
    mix_gain,
    inner_gain,
    final_gain,
    gate_weight,
    value_weight,
    gate_kernel,
    value_kernel,
    down_weight,
):
    length = mix_input.shape[0]
    n_tp, n_sp = lax.axis_size("tp"), lax.axis_size("sp")
    tp_me = lax.axis_index("tp").astype(jnp.int32).reshape(1)
    sp_me = lax.axis_index("sp").astype(jnp.int32).reshape(1)
    hidden_units = gate_weight.shape[1]

    edge = from_behind(mix_input[length - 8 :], "sp")
    up_whole = lax.all_gather(
        jnp.concatenate([gate_weight, value_weight], axis=1), "sp", axis=0, tiled=True
    )
    turned = lax.optimization_barrier((down_weight.T, edge))[0]
    down_whole = lax.all_gather(turned, "sp", axis=0, tiled=True)

    soft = jax.nn.softplus(-decay_param)[None]
    cum, loc, seg, ends = local_scan(
        mix_input, edge, mix_kernel, recur_gate_map, input_gate_map, soft, jump_log, n_sp
    )
    arrived = exchanged(ends, "sp")
    shares = branch_shares(sp_me, arrived, seg, cum, loc, gate_input, out_weight, n_tp)
    hidden_state, normed = mid(
        tp_me, exchanged(shares, "tp"), residual, mix_gain[None], inner_gain[None]
    )
    everyone = exchanged(jnp.broadcast_to(normed, (n_tp, *normed.shape)), "tp").reshape(length, -1)

    up_gate = jnp.dot(
        everyone, up_whole[:, :hidden_units], preferred_element_type=jnp.float32
    ).astype(jnp.bfloat16)
    up_value = jnp.dot(
        everyone, up_whole[:, hidden_units:], preferred_element_type=jnp.float32
    ).astype(jnp.bfloat16)
    behind = gate_kernel.shape[0] - 1
    tails = jnp.stack([up_gate[length - behind :], up_value[length - behind :]])
    hidden_edge = from_behind(tails, "sp")
    gate_conv = causal_taps(
        jnp.concatenate([hidden_edge[0], up_gate], axis=0).astype(jnp.float32), gate_kernel, length
    )
    value_conv = causal_taps(
        jnp.concatenate([hidden_edge[1], up_value], axis=0).astype(jnp.float32), value_kernel, length
    )
    activation = (jax.nn.gelu(gate_conv, approximate=True) * value_conv).astype(jnp.bfloat16)
    down = lax.dot_general(
        activation, down_whole, (((1,), (1,)), ((), ())), preferred_element_type=jnp.float32
    ).astype(jnp.bfloat16)
    down_shares = exchanged(down.reshape(n_tp, length // n_tp, -1), "tp")
    return last(down_shares, hidden_state, final_gain[None])


def solution(mesh):
    return jax.shard_map(
        local,
        mesh=mesh,
        in_specs=(
            P(("grp", "sp"), None),
            P(("grp", "sp"), "tp"),
            P(("grp", "sp"), "tp"),
            P(None, "tp"),
            P("tp", None, None),
            P("tp", None, None),
            P("tp"),
            P(("grp", "sp"), "tp"),
            P("tp", None),
            P(),
            P(),
            P(),
            P("sp", "tp"),
            P("sp", "tp"),
            P(None, "tp"),
            P(None, "tp"),
            P("tp", "sp"),
        ),
        out_specs=P(("grp", "sp", "tp"), None),
        check_vma=False,
    )
```

time: 338 us -> 249 us (0.74)
  local copies, waits for them, and re-layouts: 79.5 us -> 6.11 us
  other arithmetic: 38.3 us -> 7.59 us
  Pallas kernels: 0 us -> 20.6 us
  waiting for transfers between devices: 101 us -> 109 us
  matrix products: 35.2 us -> 27.8 us
    slice x82 -> x1, local copies, waits for them, and re-layouts: 52.8 us -> 0.7 us  [local(): edge = from_behind(mix_input[length - 8:], 'sp')]
    pad x32 -> x0, local copies, waits for them, and re-layouts: 20.6 us -> none  [local(): lax.associative_scan(linear_pair, (jnp.exp(log_decay), drive), axis=0)]
    pallas_call x0 -> x4, Pallas kernels: none -> 20.6 us  [the longest x1 6.74 us: local_scan(): pl.pallas_call(scan_kernel, grid=(groups,), in_specs=[column(length), col...]
    add x32 -> x0, other arithmetic: 14.5 us -> none  [the longest x17 7.35 us: linear_pair(): after_pair[0] * before_pair[1] + after_pair[1]]
    reduce_sum x5 -> x0, other arithmetic: 7.56 us -> none  [the longest x2 4.16 us: summed_on_arrival(): return arrived.astype(jnp.float32).sum(axis=0)]
    dot_general x6 -> x3, matrix products: 35.2 us -> 27.8 us  [the longest x1 15.7 us: local(): lax.dot_general(activation, down_whole, (((1,), (1,)), ((), ())), preferr...]
    mul x5 -> x0, other arithmetic: 6.39 us -> none  [the longest x3 3.56 us: linear_pair(): before_pair[0] * after_pair[0]]
    all_gather x1 -> x2, waiting for transfers between devices: 0.01 us -> 5.64 us  [the longest x1 5.64 us: local(): down_whole = lax.all_gather(turned, 'sp', axis=0, tiled=True)]
  transfers between devices with their start and end apart: 6 -> 7, of which waited for: 5 -> 6; matrix products, arithmetic and copies ran while one was open for 34% -> 9% of each run, Pallas kernels for 0% -> 7%
where the time goes in v1:
time: 249 us; the launch traced here: 248 us
  waiting for transfers between devices  109 us (44%)
  blocking collectives  38.2 us (15%)
  matrix products  27.8 us (11%)
  starting transfers between devices  25.1 us (10%)
  Pallas kernels  20.6 us (8%)
  between operations  13.6 us (5%)
  other arithmetic  7.59 us (3%)
  local copies, waits for them, and re-layouts  6.11 us (2%)
    all_to_all x3, waiting for transfers between devices, exchanged(): return lax.all_to_all(tiles, axis, split_axis=0, concat_axis=0, tiled=True)  85.4 us
    all_to_all x1, blocking collectives, exchanged(): return lax.all_to_all(tiles, axis, split_axis=0, concat_axis=0, tiled=True)  38.2 us
    ppermute x2, waiting for transfers between devices, from_behind(): return lax.ppermute(value, axis, [(i, i + 1) for i in range(count - 1)])  17.9 us
    all_to_all x3, starting transfers between devices, exchanged(): return lax.all_to_all(tiles, axis, split_axis=0, concat_axis=0, tiled=True)  16.2 us
    dot_general x1, matrix products, local(): lax.dot_general(activation, down_whole, (((1,), (1,)), ((), ())), preferr...  15.7 us
    ppermute x2, starting transfers between devices, from_behind(): return lax.ppermute(value, axis, [(i, i + 1) for i in range(count - 1)])  8.77 us
    dot_general x1, matrix products, local(): jnp.dot(everyone, up_whole[:, :hidden_units], preferred_element_type=jnp....  7.49 us
    pallas_call x1, Pallas kernels, local_scan(): pl.pallas_call(scan_kernel, grid=(groups,), in_specs=[column(length), col...  6.74 us
  transfers between devices with their start and end apart: 7, of which 6 were waited for; matrix products, arithmetic and copies ran while one was open for 9% of the time, Pallas kernels for 7%

profile of v1, /device:TPU:33, one launch (start us, length us, event | category | flops | bytes accessed | tf_op | source)
XLA Modules:
  0.0 248.0 jit_solution(12371950291843272271)
XLA Ops:
  6.5 0.0 all-gather.3.cloned.1.call-start
  6.6 1.8 pad_maximum_fusion
  8.3 0.1 all-gather.3.cloned.1.call-update
  8.4 0.1 all-gather.5.cloned.1.call-start
  8.4 0.7 slice.57
  9.1 5.7 %collective-permute-start = (bf16[8,512]{1,0:T(8,128)(2,1)S(1)}, bf16[8,512]{1,0:T(8,128)(2,1)S(1)}, u32[]{:S(2)}, u32[]{:S(2)}) collective-permute-start(bf16[8,512]{1,0:T(8,128)(2,1)S(1)} %slice.57), channel_id=1, source_target_pairs={{0,4},{4,8},{8,12},{12,16},{16,20},{20,24},{24,28},{28,32},{32,36}... | collective-permute-start | bytes 24584 | tf_op jit(solution)/shard_map/ppermute | solution.py:227
  14.9 16.6 %collective-permute-done.edge_ref = bf16[8,512]{1,0:T(8,128)(2,1)S(1)} collective-permute-done((bf16[8,512]{1,0:T(8,128)(2,1)S(1)}, bf16[8,512]{1,0:T(8,128)(2,1)S(1)}, u32[]{:S(2)}, u32[]{:S(2)}) %collective-permute-start) | collective-permute-done | bytes 8224 | tf_op jit(solution)/shard_map/ppermute | solution.py:227
  31.5 0.0 copy-start.4
  31.5 0.1 all-gather.5.cloned.1.call-update
  31.6 1.2 compare_select_fusion
  32.8 0.0 copy-done.4
  32.8 6.7 %local_scan.1 = (f32[704,512]{1,0:T(8,128)}, f32[704,512]{1,0:T(8,128)}, f32[2,8,512]{2,1,0:T(8,128)}, f32[32,8,128]{2,1,0:T(8,128)}) custom-call(bf16[704,512]{1,0:T(8,128)(2,1)} %x_ref.1, bf16[8,512]{1,0:T(8,128)(2,1)} %copy-done.4, bf16[4,512]{1,0:T(4,128)(2,1)} %taps_ref.1, bf16[4,128,128]{2,1,0:T(8,128)(2,1)} %rmap_ref.1, ...), custom_call_target="tpu_custom_call" | custom-call | tf_op jit(solution)/shard_map/local_scan/pallas_call | solution.py:91
  39.6 8.1 %all-to-all-start = ((f32[32,8,128]{2,1,0:T(8,128)}), f32[32,8,128]{2,1,0:T(8,128)S(1)}, u32[]{:S(2)}, u32[]{:S(2)}) async-start(f32[32,8,128]{2,1,0:T(8,128)} %get-tuple-element.12), calls=%async_computation | async-start | bytes 262144 | tf_op jit(solution)/shard_map/all_to_all | solution.py:231
  47.7 18.3 %all-to-all-done.arrived_ref = f32[32,8,128]{2,1,0:T(8,128)S(1)} async-done(((f32[32,8,128]{2,1,0:T(8,128)}), f32[32,8,128]{2,1,0:T(8,128)S(1)}, u32[]{:S(2)}, u32[]{:S(2)}) %all-to-all-start) | async-done | bytes 131104 | tf_op jit(solution)/shard_map/all_to_all | solution.py:231
  66.0 0.0 copy-start.1
  66.0 0.7 copy-done.1
  66.6 6.4 %branch_shares.1 = bf16[4,176,2048]{2,1,0:T(8,128)(2,1)} custom-call(s32[1]{0:T(128)} %bitcast.1.me_ref, f32[32,8,128]{2,1,0:T(8,128)} %copy-done.1, f32[2,8,512]{2,1,0:T(8,128)} %get-tuple-element.13.seg_ref, f32[704,512]{1,0:T(8,128)} %get-tuple-element.14.cum_ref, f32[704,512]{1,0:T(8,128)} %get-tuple-element.15.loc_ref, bf16[704,512]{1,0:T(8,128)(2,1)} %gate_ref.1, ...), custom_call_target="tpu_custom_call" | custom-call | tf_op jit(solution)/shard_map/branch_shares/pallas_call | solution.py:152
  73.0 4.3 %all-to-all-start.1 = ((bf16[4,176,2048]{2,1,0:T(8,128)(2,1)}), bf16[4,176,2048]{2,1,0:T(8,128)(2,1)S(1)}, u32[]{:S(2)}, u32[]{:S(2)}) async-start(bf16[4,176,2048]{2,1,0:T(8,128)(2,1)} %branch_shares.1), calls=%async_computation.1 | async-start | bytes 5767168 | tf_op jit(solution)/shard_map/all_to_all | solution.py:231
  77.4 34.1 %all-to-all-done.1.shares_ref = bf16[4,176,2048]{2,1,0:T(8,128)(2,1)S(1)} async-done(((bf16[4,176,2048]{2,1,0:T(8,128)(2,1)}), bf16[4,176,2048]{2,1,0:T(8,128)(2,1)S(1)}, u32[]{:S(2)}, u32[]{:S(2)}) %all-to-all-start.1) | async-done | bytes 2883616 | tf_op jit(solution)/shard_map/all_to_all | solution.py:231
  111.4 0.0 copy-start
  111.4 1.6 copy-done
  113.0 3.8 %mid.1 = (bf16[176,2048]{1,0:T(8,128)(2,1)}, bf16[176,2048]{1,0:T(8,128)(2,1)}) custom-call(s32[1]{0:T(128)} %bitcast.me_ref, bf16[4,176,2048]{2,1,0:T(8,128)(2,1)} %copy-done, bf16[704,2048]{1,0:T(8,128)(2,1)} %res_ref.1, f32[1,2048]{1,0:T(1,128)} %bitcast.24, f32[1,2048]{1,0:T(1,128)} %bitcast.25), custom_call_target="tpu_custom_call" | custom-call | tf_op jit(solution)/shard_map/mid/pallas_call | solution.py:193
  116.9 0.0 copy-start.2
  116.9 0.0 copy-start.3
  116.9 3.1 %broadcast_in_dim.18 = bf16[4,176,2048]{2,1,0:T(8,128)(2,1)} broadcast(bf16[176,2048]{1,0:T(8,128)(2,1)} %get-tuple-element.16), dimensions={1,2} | broadcast | bytes 3604480 | tf_op jit(solution)/shard_map/broadcast_in_dim | solution.py:283
  119.9 3.8 %all-to-all-start.2 = ((bf16[4,176,2048]{2,1,0:T(8,128)(2,1)}), bf16[4,176,2048]{2,1,0:T(8,128)(2,1)S(1)}, u32[]{:S(2)}, u32[]{:S(2)}) async-start(bf16[4,176,2048]{2,1,0:T(8,128)(2,1)} %broadcast_in_dim.18), calls=%async_computation.2 | async-start | bytes 5767168 | tf_op jit(solution)/shard_map/all_to_all | solution.py:231
  123.7 0.0 copy-done.2
  123.7 0.0 copy-done.3
  123.7 33.1 %all-to-all-done.2 = bf16[4,176,2048]{2,1,0:T(8,128)(2,1)S(1)} async-done(((bf16[4,176,2048]{2,1,0:T(8,128)(2,1)}), bf16[4,176,2048]{2,1,0:T(8,128)(2,1)S(1)}, u32[]{:S(2)}, u32[]{:S(2)}) %all-to-all-start.2) | async-done | bytes 2883616 | tf_op jit(solution)/shard_map/all_to_all | solution.py:231
  156.8 0.0 all-gather.3.cloned.1.call-done
  156.8 0.0 copy-start.5
  156.8 7.5 %fusion.17 = bf16[704,1408]{1,0:T(8,128)(2,1)S(1)} fusion(bf16[704,2048]{1,0:T(8,128)(2,1)S(1)} %bitcast.20, bf16[2048,2816]{1,0:T(8,128)(2,1)} %all-gather.3.cloned.1.call-done), kind=kOutput, calls=%fused_computation.24 | convolution fusion | flops 4061077504 | bytes 10633216 | tf_op jit(solution)/shard_map/dot_general | solution.py:285
  164.3 0.0 copy-done.5
  164.3 4.6 %fusion.20 = bf16[704,1408]{1,0:T(8,128)(2,1)S(1)} fusion(bf16[704,2048]{1,0:T(8,128)(2,1)S(1)} %bitcast.21, bf16[2048,2816]{1,0:T(8,128)(2,1)S(1)} %copy-done.5), kind=kOutput, calls=%fused_computation.25 | convolution fusion | flops 4061077504 | bytes 10633216 | tf_op jit(solution)/shard_map/dot_general | solution.py:288
  169.0 3.0 %collective-permute-start.1 = (bf16[2,2,1408]{2,1,0:T(2,128)(2,1)S(1)}, bf16[2,2,1408]{2,1,0:T(2,128)(2,1)S(1)}, u32[]{:S(2)}, u32[]{:S(2)}) collective-permute-start(bf16[2,2,1408]{2,1,0:T(2,128)(2,1)S(1)} %pad_maximum_fusion.1), channel_id=1, source_target_pairs={{0,4},{4,8},{8,12},{12,16},{16,20},{20,24},{24,28},{28,32},{32,36}... | collective-permute-start | bytes 33800 | tf_op jit(solution)/shard_map/ppermute | solution.py:227
  172.1 0.1 slice_reduce_fusion.2
  172.2 1.3 collective-permute-done.1
  173.5 2.3 maximum_convert_fusion
  175.7 2.3 maximum_convert_fusion.1
  178.0 5.6 %all-gather.5.cloned.1.call-done = bf16[2048,1408]{1,0:T(8,128)(2,1)} async-done(((bf16[64,1408]{1,0:T(8,128)(2,1)}), bf16[2048,1408]{1,0:T(8,128)(2,1)}) %all-gather.5.cloned.1.call-update) | async-done | bytes 5767184 | tf_op jit(solution)/shard_map/all_gather | solution.py:272
  183.7 15.7 %convolution_convert_fusion = bf16[704,2048]{1,0:T(8,128)(2,1)S(1)} fusion(bf16[2048,1408]{1,0:T(8,128)(2,1)} %all-gather.5.cloned.1.call-done, f32[706,1408]{1,0:T(8,128)} %maximum_convert_fusion.1, f32[706,1408]{1,0:T(8,128)} %maximum_convert_fusion, f32[1408]{0:T(1024)S(1)} %get-tuple-element.23, f32[1408]{0:T(1024)S(1)} %get-tuple-element.24, ...), kind=kOutput, calls=%fused_computation.26 | convolution fusion | flops 4081352704 | bytes 32474112 | tf_op jit(solution)/shard_map/dot_general | solution.py:301
  199.4 38.2 %all_to_all.20.shares_ref = bf16[4,176,2048]{2,1,0:T(8,128)(2,1)} all-to-all(bf16[4,176,2048]{2,1,0:T(8,128)(2,1)S(1)} %bitcast.22), channel_id=1, replica_groups=mesh['grp'=2,'sp'=32,'tp'=4] {'tp'}, dimensions={0} | all-to-all | bytes 5767168 | tf_op jit(solution)/shard_map/all_to_all | solution.py:231
  237.6 3.6 %last.1 = bf16[176,2048]{1,0:T(8,128)(2,1)} custom-call(bf16[4,176,2048]{2,1,0:T(8,128)(2,1)} %all_to_all.20.shares_ref, bf16[176,2048]{1,0:T(8,128)(2,1)} %get-tuple-element.18.hidden_ref, f32[1,2048]{1,0:T(1,128)} %bitcast.26), custom_call_target="tpu_custom_call" | custom-call | tf_op jit(solution)/shard_map/last/pallas_call | solution.py:218
  (5 shorter events, 0.1 us)
Async XLA Ops:
  6.5 150.3 %all-gather.3.cloned.1.call-start = ((), (), s32[]{:S(2)}) async-start(), calls=%async_computation.4 | async-start | bytes 11894784 | tf_op jit(solution)/shard_map/all_gather | solution.py:268
  8.4 175.3 %all-gather.5.cloned.1.call-start = ((), (), s32[]{:S(2)}) async-start(), calls=%async_computation.5 | async-start | bytes 5947392 | tf_op jit(solution)/shard_map/all_gather | solution.py:272
  9.1 22.4 %collective-permute-start = (bf16[8,512]{1,0:T(8,128)(2,1)S(1)}, bf16[8,512]{1,0:T(8,128)(2,1)S(1)}, u32[]{:S(2)}, u32[]{:S(2)}) collective-permute-start(bf16[8,512]{1,0:T(8,128)(2,1)S(1)} %slice.57), channel_id=1, source_target_pairs={{0,4},{4,8},{8,12},{12,16},{16,20},{20,24},{24,28},{28,32},{32,36}... | collective-permute-start | bytes 24584 | tf_op jit(solution)/shard_map/ppermute | solution.py:227
  31.5 1.3 copy-start.4
  39.6 26.4 %all-to-all-start = ((f32[32,8,128]{2,1,0:T(8,128)}), f32[32,8,128]{2,1,0:T(8,128)S(1)}, u32[]{:S(2)}, u32[]{:S(2)}) async-start(f32[32,8,128]{2,1,0:T(8,128)} %get-tuple-element.12), calls=%async_computation | async-start | bytes 262144 | tf_op jit(solution)/shard_map/all_to_all | solution.py:231
  66.0 0.7 copy-start.1
  73.0 38.4 %all-to-all-start.1 = ((bf16[4,176,2048]{2,1,0:T(8,128)(2,1)}), bf16[4,176,2048]{2,1,0:T(8,128)(2,1)S(1)}, u32[]{:S(2)}, u32[]{:S(2)}) async-start(bf16[4,176,2048]{2,1,0:T(8,128)(2,1)} %branch_shares.1), calls=%async_computation.1 | async-start | bytes 5767168 | tf_op jit(solution)/shard_map/all_to_all | solution.py:231
  111.4 1.6 copy-start
  116.9 6.8 %copy-start.2 = (bf16[3,1408]{1,0:T(4,128)(2,1)S(1)}, bf16[3,1408]{1,0:T(4,128)(2,1)}, u32[]{:S(2)}) copy-start(bf16[3,1408]{1,0:T(4,128)(2,1)} %param.31) | copy-start | bytes 25348
  116.9 6.9 %copy-start.3 = (bf16[3,1408]{1,0:T(4,128)(2,1)S(1)}, bf16[3,1408]{1,0:T(4,128)(2,1)}, u32[]{:S(2)}) copy-start(bf16[3,1408]{1,0:T(4,128)(2,1)} %param.32) | copy-start | bytes 25348
  119.9 36.9 %all-to-all-start.2 = ((bf16[4,176,2048]{2,1,0:T(8,128)(2,1)}), bf16[4,176,2048]{2,1,0:T(8,128)(2,1)S(1)}, u32[]{:S(2)}, u32[]{:S(2)}) async-start(bf16[4,176,2048]{2,1,0:T(8,128)(2,1)} %broadcast_in_dim.18), calls=%async_computation.2 | async-start | bytes 5767168 | tf_op jit(solution)/shard_map/all_to_all | solution.py:231
  156.8 7.5 %copy-start.5 = (bf16[2048,2816]{1,0:T(8,128)(2,1)S(1)}, bf16[2048,2816]{1,0:T(8,128)(2,1)}, u32[]{:S(2)}) copy-start(bf16[2048,2816]{1,0:T(8,128)(2,1)} %all-gather.3.cloned.1.call-done) | copy-start | bytes 34603012
  169.0 4.4 %collective-permute-start.1 = (bf16[2,2,1408]{2,1,0:T(2,128)(2,1)S(1)}, bf16[2,2,1408]{2,1,0:T(2,128)(2,1)S(1)}, u32[]{:S(2)}, u32[]{:S(2)}) collective-permute-start(bf16[2,2,1408]{2,1,0:T(2,128)(2,1)S(1)} %pad_maximum_fusion.1), channel_id=1, source_target_pairs={{0,4},{4,8},{8,12},{12,16},{16,20},{20,24},{24,28},{28,32},{32,36}... | collective-permute-start | bytes 33800 | tf_op jit(solution)/shard_map/ppermute | solution.py:227
Sparse Core Ops, SparseCore 0:
  9.2 102.5 all-gather.2
  113.6 69.9 all-gather.4

commit v2 on v1

v2 whole, which is shorter than its diff:
```python
import functools

import jax
import jax.numpy as jnp
from jax import lax
from jax.experimental import pallas as pl
from jax.experimental.pallas import tpu as pltpu
from jax.sharding import PartitionSpec as P

EPS = 1e-06
GATE_SCALE = 8.0
SEGMENTS = 8
LANES = 128
BLOCKS = 4
HALO = 16
GELU_A = 0.7978845608028654
GELU_B = 0.044715


def gelu(v):
    return 0.5 * v * (1.0 + jnp.tanh(GELU_A * (v + GELU_B * (v * v * v))))


def minus_expm1(y):
    series = 1.0 + y * (1.0 / 7.0)
    for n in (6.0, 5.0, 4.0, 3.0, 2.0):
        series = 1.0 + y * (1.0 / n) * series
    return jnp.where(y > -0.3, -y * series, 1.0 - jnp.exp(y))


def sigmoid(v):
    return 0.5 * jnp.tanh(0.5 * v) + 0.5


def scan_kernel(
    x_ref, edge_ref, taps_ref, rmap_ref, imap_ref, soft_ref, jump_ref,
    cum_ref, loc_ref, seg_ref, ends_ref,
    xs, decay, drive,
):
    group = pl.program_id(0)
    groups = pl.num_programs(0)
    length = x_ref.shape[0]
    taps = taps_ref.shape[0]
    xs[0:8, :] = edge_ref[...].astype(jnp.float32)
    xs[8 : 8 + length, :] = x_ref[...].astype(jnp.float32)
    rows = length // 4
    kernel = taps_ref[...].astype(jnp.float32)
    v = -soft_ref[...]
    soft = jnp.maximum(v, 0.0) + jnp.log1p(jnp.exp(-jnp.abs(v)))
    for at in range(0, length, rows):
        conv = jnp.zeros((rows, LANES), jnp.float32)
        for k in range(taps):
            first = 8 + at - (taps - 1) + k
            conv = conv + xs[first : first + rows, :] * kernel[k : k + 1, :]
        conv = conv.astype(jnp.bfloat16)
        rgate = sigmoid(jnp.dot(conv, rmap_ref[0], preferred_element_type=jnp.float32))
        igate = sigmoid(jnp.dot(conv, imap_ref[0], preferred_element_type=jnp.float32))
        log_decay = -GATE_SCALE * rgate * soft + jump_ref[at : at + rows, :]
        decay[at : at + rows, :] = jnp.exp(log_decay)
        drive[at : at + rows, :] = (
            jnp.sqrt(minus_expm1(2.0 * log_decay)) * igate * conv.astype(jnp.float32)
        )
    steps = length // SEGMENTS

    def step(i, carry):
        state, product = carry
        where = pl.ds(i, SEGMENTS, steps)
        a = decay[where, :]
        state = a * state + drive[where, :]
        product = a * product
        loc_ref[where, :] = state
        cum_ref[where, :] = product
        return state, product

    zero = jnp.zeros((SEGMENTS, LANES), jnp.float32)
    state, product = lax.fori_loop(0, steps, step, (zero, zero + 1.0), unroll=8)
    seg_ref[0, :, :] = product
    seg_ref[1, :, :] = state
    all_state = state[0:1]
    all_product = product[0:1]
    for s in range(1, SEGMENTS):
        all_state = product[s : s + 1] * all_state + state[s : s + 1]
        all_product = product[s : s + 1] * all_product
    count = ends_ref.shape[0]
    ends_ref[:, pl.ds(group, 1), :] = jnp.broadcast_to(all_product[None], (count, 1, LANES))
    ends_ref[:, pl.ds(groups + group, 1), :] = jnp.broadcast_to(all_state[None], (count, 1, LANES))


def local_scan(x, edge, taps, rmap, imap, soft, jump, copies):
    length, channels = x.shape
    groups = channels // LANES
    column = lambda rows: pl.BlockSpec((rows, LANES), lambda g: (0, g))
    square = pl.BlockSpec((1, LANES, LANES), lambda g: (g, 0, 0))
    return pl.pallas_call(
        scan_kernel,
        grid=(groups,),
        in_specs=[column(length), column(8), column(taps.shape[0]), square, square, column(1), column(length)],
        out_specs=[
            column(length),
            column(length),
            pl.BlockSpec((2, SEGMENTS, LANES), lambda g: (0, 0, g)),
            pl.BlockSpec((copies, 2 * groups, LANES), lambda g: (0, 0, 0)),
        ],
        out_shape=[
            jax.ShapeDtypeStruct((length, channels), jnp.float32),
            jax.ShapeDtypeStruct((length, channels), jnp.float32),
            jax.ShapeDtypeStruct((2, SEGMENTS, channels), jnp.float32),
            jax.ShapeDtypeStruct((copies, 2 * groups, LANES), jnp.float32),
        ],
        scratch_shapes=[
            pltpu.VMEM((length + 8, LANES), jnp.float32),
            pltpu.VMEM((length, LANES), jnp.float32),
            pltpu.VMEM((length, LANES), jnp.float32),
        ],
        name="local_scan",
    )(x, edge, taps, rmap, imap, soft, jump)


def branch_kernel(me_ref, arrived_ref, seg_ref, cum_ref, loc_ref, gate_ref, w_ref, *rest):
    outs, carry, branch = rest[:-2], rest[-2], rest[-1]
    block = row_block_at(pl.program_id(0), me_ref, len(outs) == 2)
    groups = cum_ref.shape[1] // LANES
    rows = cum_ref.shape[0]
    per_block = SEGMENTS // BLOCKS
    seg_rows = rows // per_block

    @pl.when(pl.program_id(0) == 0)
    def _():
        def join(j, state):
            return arrived_ref[j, 0:groups, :] * state + arrived_ref[j, groups : 2 * groups, :]

        state = lax.fori_loop(0, me_ref[1], join, jnp.zeros((groups, LANES), jnp.float32))
        for g in range(groups):
            lanes = slice(g * LANES, (g + 1) * LANES)
            now = state[g : g + 1, :]
            for s in range(SEGMENTS):
                carry[s, 0:1, lanes] = now
                now = seg_ref[0, s : s + 1, lanes] * now + seg_ref[1, s : s + 1, lanes]

    for part in range(per_block):
        at = slice(part * seg_rows, (part + 1) * seg_rows)
        state = loc_ref[at, :] + cum_ref[at, :] * carry[block * per_block + part, 0:1, :]
        branch[at, :] = state
    gate = gate_ref[...].astype(jnp.float32)
    out = (branch[...] * gelu(gate)).astype(jnp.bfloat16)
    share = jnp.dot(out, w_ref[...], preferred_element_type=jnp.float32).astype(jnp.bfloat16)
    put(outs, share)


def row_block_at(step, me_ref, opposite):
    turned = 2 if opposite else 1 + (step * (5 - step) >> 1)
    return lax.rem(me_ref[0] + turned, BLOCKS)


def put(outs, share):
    if len(outs) == 1:
        outs[0][0] = share
    else:
        half = share.shape[1] // 2
        outs[0][...] = share[:, :half]
        outs[1][...] = share[:, half:]


def share_outputs(count, rows, width, halves):
    if halves:
        return (
            [pl.BlockSpec((rows, width // 2), lambda b, *_: (0, 0))] * 2,
            [jax.ShapeDtypeStruct((rows, width // 2), jnp.bfloat16)] * 2,
        )
    return (
        [pl.BlockSpec((1, rows, width), lambda b, *_: (b, 0, 0))],
        [jax.ShapeDtypeStruct((count, rows, width), jnp.bfloat16)],
    )


def branch_shares(me, arrived, seg, cum, loc, gate, weight, halves):
    length, channels = cum.shape
    width = weight.shape[1]
    rows = length // BLOCKS
    count = 1 if halves else BLOCKS - 1
    row_block = pl.BlockSpec((rows, channels), lambda b, me: (row_block_at(b, me, halves), 0))
    whole = lambda a: pl.BlockSpec(a.shape, lambda b, me: (0,) * a.ndim)
    out_specs, out_shape = share_outputs(count, rows, width, halves)
    return pl.pallas_call(
        branch_kernel,
        grid_spec=pltpu.PrefetchScalarGridSpec(
            num_scalar_prefetch=1,
            grid=(count,),
            in_specs=[whole(arrived), whole(seg), row_block, row_block, row_block, whole(weight)],
            out_specs=out_specs,
            scratch_shapes=[
                pltpu.VMEM((SEGMENTS, 1, channels), jnp.float32),
                pltpu.VMEM((rows, channels), jnp.float32),
            ],
        ),
        out_shape=out_shape,
        cost_estimate=pl.CostEstimate(
            flops=2 * count * rows * channels * width,
            bytes_accessed=count * rows * (10 * channels + 2 * width) + 2 * channels * width,
            transcendentals=count * rows * channels,
        ),
        name="branch_first" if halves else "branch_rest",
    )(me, arrived, seg, cum, loc, gate, weight)


def feed_kernel(*refs, names, first):
    me_ref, outside, own, right, left, low, high, w_ref, w_all, gk_ref, vk_ref = refs[:11]
    outs = refs[11:-5]
    lhs, up, act, down, sem = refs[-5:]
    chunk = pl.program_id(0)
    rows = own.shape[0]
    tall = rows + HALO
    taps = gk_ref.shape[0]
    width, units = down.shape
    half = width // 2
    fetch = pltpu.make_async_copy(w_all.at[:, pl.ds(2 * units, units)], down, sem)

    def fill(b, name):
        at = b * tall
        tail = slice(rows - HALO, rows)
        steps = {"own": 0, "right": 1, "opposite": 2, "left": 3}[name]
        if name == "left":
            lhs[at : at + HALO, :half] = low[tail, :]
            lhs[at : at + HALO, half:] = high[tail, :]
        else:
            behind = {"own": left, "right": own, "opposite": right}[name]
            lhs[at : at + HALO, :] = behind[tail, :]

        @pl.when(lax.rem(me_ref[0] + steps, BLOCKS) == 0)
        def _():
            lhs[at : at + HALO, :] = outside[...]

        at = at + HALO
        if name == "opposite":
            lhs[at : at + rows, :half] = low[...]
            lhs[at : at + rows, half:] = high[...]
        else:
            lhs[at : at + rows, :] = {"own": own, "right": right, "left": left}[name][...]

    @pl.when(chunk == 0)
    def _():
        fetch.start()
        for b, name in enumerate(names):
            fill(b, name)

    up[...] = (
        jnp.dot(lhs[...], w_ref[...], preferred_element_type=jnp.float32)
        .astype(jnp.bfloat16)
        .astype(jnp.float32)
    )
    gate_taps = gk_ref[...].astype(jnp.float32)
    value_taps = vk_ref[...].astype(jnp.float32)
    lanes = pl.ds(pl.multiple_of(chunk * LANES, LANES), LANES)
    for b in range(len(names)):
        gate = jnp.zeros((rows, LANES), jnp.float32)
        value = jnp.zeros((rows, LANES), jnp.float32)
        for k in range(taps):
            at = b * tall + HALO - (taps - 1) + k
            gate = gate + up[at : at + rows, 0:LANES] * gate_taps[k : k + 1, :]
            value = value + up[at : at + rows, LANES : 2 * LANES] * value_taps[k : k + 1, :]
        act[b * rows : (b + 1) * rows, lanes] = (gelu(gate) * value).astype(jnp.bfloat16)

    @pl.when(chunk == pl.num_programs(0) - 1)
    def _():
        fetch.wait()
        for b in range(len(names)):
            share = lax.dot_general(
                act[b * rows : (b + 1) * rows, :],
                down[...],
                (((1,), (1,)), ((), ())),
                preferred_element_type=jnp.float32,
            ).astype(jnp.bfloat16)
            if first:
                put(outs, share)
            else:
                outs[0][b] = share


def feed(me, outside, blocks, weights, gate_kernel, value_kernel, names, first):
    count = len(names)
    rows, width = blocks[0].shape
    units = gate_kernel.shape[1]
    chunks = units // LANES
    taps = gate_kernel.shape[0]
    out_specs, out_shape = share_outputs(count, rows, width, first)
    if not first:
        out_specs = [pl.BlockSpec((count, rows, width), lambda c: (0, 0, 0))]
    return pl.pallas_call(
        functools.partial(feed_kernel, names=names, first=first),
        grid=(chunks,),
        in_specs=[
            pl.BlockSpec(memory_space=pltpu.SMEM),
            *[pl.BlockSpec(memory_space=pltpu.VMEM)] * (1 + len(blocks)),
            pl.BlockSpec((width, 2 * LANES), lambda c: (0, c)),
            pl.BlockSpec(memory_space=pl.ANY),
            pl.BlockSpec((taps, LANES), lambda c: (0, c)),
            pl.BlockSpec((taps, LANES), lambda c: (0, c)),
        ],
        out_specs=out_specs,
        out_shape=out_shape,
        scratch_shapes=[
            pltpu.VMEM((count * (rows + HALO), width), jnp.bfloat16),
            pltpu.VMEM((count * (rows + HALO), 2 * LANES), jnp.float32),
            pltpu.VMEM((count * rows, units), jnp.bfloat16),
            pltpu.VMEM((width, units), jnp.bfloat16),
            pltpu.SemaphoreType.DMA,
        ],
        cost_estimate=pl.CostEstimate(
            flops=6 * count * rows * width * units,
            bytes_accessed=6 * width * units + 4 * count * rows * width,
            transcendentals=count * rows * units,
        ),
        name="feed_first" if first else "feed_rest",
    )(me, outside, *blocks, weights, weights, gate_kernel, value_kernel)


def pack_kernel(gate_ref, value_ref, turned_ref, out_ref):
    units = gate_ref.shape[1]
    for at in range(0, units, LANES):
        out_ref[:, 2 * at : 2 * at + LANES] = gate_ref[:, at : at + LANES]
        out_ref[:, 2 * at + LANES : 2 * at + 2 * LANES] = value_ref[:, at : at + LANES]
    out_ref[:, 2 * units :] = turned_ref[...]


def packed(gate, value, turned):
    rows, units = gate.shape
    return pl.pallas_call(
        pack_kernel,
        out_shape=jax.ShapeDtypeStruct((rows, 3 * units), jnp.bfloat16),
        name="pack",
    )(gate, value, turned)


def scaled(v, gain):
    return v * lax.rsqrt(jnp.mean(v * v, axis=-1, keepdims=True) + EPS) * gain


def three_sum(rest_ref, left_ref, right_ref, at):
    total = rest_ref[2, at, :].astype(jnp.float32) + left_ref[at, :].astype(jnp.float32)
    total = total + right_ref[at, :].astype(jnp.float32)
    return total.astype(jnp.bfloat16).astype(jnp.float32)


def by_rows(rows, body):
    def step(i, carry):
        body(pl.ds(pl.multiple_of(i * HALO, HALO), HALO))
        return carry

    lax.fori_loop(0, rows // HALO, step, 0)


def mid_kernel(
    me_ref, rest_ref, left_ref, right_ref, res_ref, mix_ref, inner_ref,
    hidden_ref, normed_ref, res, sem,
):
    rows = left_ref.shape[0]
    first = pl.multiple_of(me_ref[0] * rows, rows)
    fetch = pltpu.make_async_copy(res_ref.at[pl.ds(first, rows), :], res, sem)
    fetch.start()
    mix, inner = mix_ref[...], inner_ref[...]
    fetch.wait()

    def body(at):
        hidden = (
            res[at, :].astype(jnp.float32)
            + scaled(three_sum(rest_ref, left_ref, right_ref, at), mix)
        ).astype(jnp.bfloat16)
        hidden_ref[at, :] = hidden
        normed_ref[at, :] = scaled(hidden.astype(jnp.float32), inner).astype(jnp.bfloat16)

    by_rows(rows, body)


VMEM = pl.BlockSpec(memory_space=pltpu.VMEM)


def mid(me, rest, left, right, residual, mix_gain, inner_gain):
    rows, width = left.shape
    return pl.pallas_call(
        mid_kernel,
        in_specs=[
            pl.BlockSpec(memory_space=pltpu.SMEM),
            VMEM, VMEM, VMEM,
            pl.BlockSpec(memory_space=pl.ANY),
            VMEM, VMEM,
        ],
        out_specs=[VMEM, VMEM],
        out_shape=[jax.ShapeDtypeStruct((rows, width), jnp.bfloat16)] * 2,
        scratch_shapes=[pltpu.VMEM((rows, width), jnp.bfloat16), pltpu.SemaphoreType.DMA],
        name="mid",
    )(me, rest, left, right, residual, mix_gain, inner_gain)


def last_kernel(rest_ref, left_ref, right_ref, hidden_ref, gain_ref, out_ref):
    gain = gain_ref[...]

    def body(at):
        out_ref[at, :] = (
            hidden_ref[at, :].astype(jnp.float32)
            + scaled(three_sum(rest_ref, left_ref, right_ref, at), gain)
        ).astype(jnp.bfloat16)

    by_rows(hidden_ref.shape[0], body)


def last(rest, left, right, hidden, gain):
    return pl.pallas_call(
        last_kernel,
        in_specs=[VMEM] * 5,
        out_specs=VMEM,
        out_shape=jax.ShapeDtypeStruct(hidden.shape, jnp.bfloat16),
        name="last",
    )(rest, left, right, hidden, gain)


def join_kernel(rest_ref, low_ref, high_ref, right_ref, left_ref):
    half = low_ref.shape[1]
    add = lambda a, b: (a.astype(jnp.float32) + b.astype(jnp.float32)).astype(jnp.bfloat16)

    def body(at):
        right_ref[at, :half] = add(rest_ref[0, at, :half], low_ref[at, :])
        right_ref[at, half:] = rest_ref[0, at, half:]
        left_ref[at, :half] = rest_ref[1, at, :half]
        left_ref[at, half:] = add(rest_ref[1, at, half:], high_ref[at, :])

    by_rows(low_ref.shape[0], body)


def join(rest, low, high):
    _, rows, width = rest.shape
    return pl.pallas_call(
        join_kernel,
        in_specs=[VMEM] * 3,
        out_specs=[VMEM] * 2,
        out_shape=[jax.ShapeDtypeStruct((rows, width), jnp.bfloat16)] * 2,
        name="join",
    )(rest, low, high)


def turn(value, axis, steps):
    count = lax.axis_size(axis)
    return lax.ppermute(value, axis, [(i, (i + steps) % count) for i in range(count)])


def ring_sum(first, rest):
    low, high = turn(first[0], "tp", 1), turn(first[1], "tp", -1)
    to_right, to_left = join(rest, low, high)
    return rest, turn(to_right, "tp", 1), turn(to_left, "tp", -1)


def from_behind(value, axis):
    count = lax.axis_size(axis)
    return lax.ppermute(value, axis, [(i, i + 1) for i in range(count - 1)])


def exchanged(tiles, axis):
    return lax.all_to_all(tiles, axis, split_axis=0, concat_axis=0, tiled=True)


def local(
    residual,
    mix_input,
    gate_input,
    mix_kernel,
    recur_gate_map,
    input_gate_map,
    decay_param,
    jump_log,
    out_weight,
    mix_gain,
    inner_gain,
    final_gain,
    gate_weight,
    value_weight,
    gate_kernel,
    value_kernel,
    down_weight,
):
    n_tp, n_sp = lax.axis_size("tp"), lax.axis_size("sp")
    assert n_tp == BLOCKS
    tp_me = lax.axis_index("tp").astype(jnp.int32)
    me = jnp.stack([tp_me, lax.axis_index("sp").astype(jnp.int32)])

    edge = from_behind(mix_input[mix_input.shape[0] - 8 :], "sp")
    weights = lax.all_gather(packed(gate_weight, value_weight, down_weight.T), "sp", axis=0, tiled=True)

    cum, loc, seg, ends = local_scan(
        mix_input, edge, mix_kernel, recur_gate_map, input_gate_map, decay_param[None], jump_log, n_sp
    )
    arrived = exchanged(ends, "sp")
    shares = functools.partial(
        branch_shares, arrived=arrived, seg=seg, cum=cum, loc=loc, gate=gate_input, weight=out_weight
    )
    first = shares(me, halves=True)
    rest = shares(me, halves=False)[0]
    hidden_state, own = mid(
        me, *ring_sum(first, rest), residual, mix_gain[None], inner_gain[None]
    )
    left, right = turn(own, "tp", 1), turn(own, "tp", -1)
    half = own.shape[1] // 2
    low, high = turn(left[:, :half], "tp", 1), turn(right[:, half:], "tp", -1)
    tails = [own[-HALO:], right[-HALO:], jnp.concatenate([low[-HALO:], high[-HALO:]], axis=1), left[-HALO:]]
    outside = from_behind(lax.select_n(n_tp - 1 - tp_me, *tails), "sp")
    blocks = (own, right, left, low, high)
    given = (me, outside, blocks, weights, gate_kernel, value_kernel)
    first = feed(*given, names=("opposite",), first=True)
    rest = feed(*given, names=("right", "left", "own"), first=False)[0]
    return last(*ring_sum(first, rest), hidden_state, final_gain[None])


def solution(mesh):
    return jax.shard_map(
        local,
        mesh=mesh,
        in_specs=(
            P(("grp", "sp"), None),
            P(("grp", "sp"), "tp"),
            P(("grp", "sp"), "tp"),
            P(None, "tp"),
            P("tp", None, None),
            P("tp", None, None),
            P("tp"),
            P(("grp", "sp"), "tp"),
            P("tp", None),
            P(),
            P(),
            P(),
            P("sp", "tp"),
            P("sp", "tp"),
            P(None, "tp"),
            P(None, "tp"),
            P("tp", "sp"),
        ),
        out_specs=P(("grp", "sp", "tp"), None),
        check_vma=False,
    )
```

time: 249 us -> 222 us (0.89)
  Pallas kernels: 20.6 us -> 75 us
  blocking collectives: 38.2 us -> 0 us
  matrix products: 27.8 us -> 0 us
  waiting for transfers between devices: 109 us -> 88.1 us
  starting transfers between devices: 25.1 us -> 34.8 us
  other arithmetic: 7.59 us -> 1.59 us
    all_to_all x3 -> x1, waiting for transfers between devices: 85.4 us -> 17.3 us  [exchanged(): return lax.all_to_all(tiles, axis, split_axis=0, concat_axis=0, tiled=True)]
    pallas_call x3 -> x9, Pallas kernels: 13.8 us -> 68.2 us  [the longest x2 38.1 us: feed(): pl.pallas_call(functools.partial(feed_kernel, names=names, first=first),...]
    ppermute x0 -> x12, waiting for transfers between devices: none -> 52.2 us  [turn(): lax.ppermute(value, axis, [(i, (i + steps) % count) for i in range(count)])]
    all_to_all x1 -> x0, blocking collectives: 38.2 us -> none  [exchanged(): return lax.all_to_all(tiles, axis, split_axis=0, concat_axis=0, tiled=True)]
    dot_general x3 -> x0, matrix products: 27.8 us -> none  [the longest x1 15.7 us: local(): lax.dot_general(activation, down_whole, (((1,), (1,)), ((), ())), preferr...]
    ppermute x0 -> x12, starting transfers between devices: none -> 16.8 us  [turn(): lax.ppermute(value, axis, [(i, (i + steps) % count) for i in range(count)])]
    all_to_all x3 -> x1, starting transfers between devices: 16.2 us -> 8.26 us  [exchanged(): return lax.all_to_all(tiles, axis, split_axis=0, concat_axis=0, tiled=True)]
    all_gather x2 -> x1, waiting for transfers between devices: 5.64 us -> 0.01 us  [local(): lax.all_gather(packed(gate_weight, value_weight, down_weight.T), 'sp', ax...]
  transfers between devices with their start and end apart: 7 -> 16, of which waited for: 6 -> 8; matrix products, arithmetic and copies ran while one was open for 9% -> 1% of each run, Pallas kernels for 7% -> 22%
where the time goes in v2:
time: 222 us; the launch traced here: 221 us
  waiting for transfers between devices  88.1 us (40%)
  Pallas kernels  75 us (34%)
  starting transfers between devices  34.8 us (16%)
  between operations  13.6 us (6%)
  local copies, waits for them, and re-layouts  7.79 us (4%)
    ppermute x12, waiting for transfers between devices, turn(): lax.ppermute(value, axis, [(i, (i + steps) % count) for i in range(count)])  52.2 us
    pallas_call x2, Pallas kernels, feed(): pl.pallas_call(functools.partial(feed_kernel, names=names, first=first),...  38.1 us
    ppermute x2, waiting for transfers between devices, from_behind(): return lax.ppermute(value, axis, [(i, i + 1) for i in range(count - 1)])  18.6 us
    all_to_all x1, waiting for transfers between devices, exchanged(): return lax.all_to_all(tiles, axis, split_axis=0, concat_axis=0, tiled=True)  17.3 us
    ppermute x12, starting transfers between devices, turn(): lax.ppermute(value, axis, [(i, (i + steps) % count) for i in range(count)])  16.8 us
    pallas_call x2, Pallas kernels, branch_shares(): pl.pallas_call(branch_kernel, grid_spec=pltpu.PrefetchScalarGridSpec(num_...  10.4 us
    ppermute x2, starting transfers between devices, from_behind(): return lax.ppermute(value, axis, [(i, i + 1) for i in range(count - 1)])  9.67 us
    all_to_all x1, starting transfers between devices, exchanged(): return lax.all_to_all(tiles, axis, split_axis=0, concat_axis=0, tiled=True)  8.26 us
  transfers between devices with their start and end apart: 16, of which 8 were waited for; matrix products, arithmetic and copies ran while one was open for 1% of the time, Pallas kernels for 22%

profile of v2, /device:TPU:33, one launch (start us, length us, event | category | flops | bytes accessed | tf_op | source)
XLA Modules:
  0.0 220.9 jit_solution(12858306141151872414)
XLA Ops:
  6.5 0.0 all-gather.2.cloned.1.call-start
  6.6 2.0 pack.1
  8.5 0.1 all-gather.2.cloned.1.call-update
  8.6 0.7 slice.24
  9.3 5.7 %collective-permute-start = (bf16[8,512]{1,0:T(8,128)(2,1)S(1)}, bf16[8,512]{1,0:T(8,128)(2,1)S(1)}, u32[]{:S(2)}, u32[]{:S(2)}) collective-permute-start(bf16[8,512]{1,0:T(8,128)(2,1)S(1)} %slice.24), channel_id=1, source_target_pairs={{0,4},{4,8},{8,12},{12,16},{16,20},{20,24},{24,28},{28,32},{32,36}... | collective-permute-start | bytes 24584 | tf_op jit(solution)/shard_map/ppermute | solution.py:453
  15.0 16.6 %collective-permute-done.edge_ref = bf16[8,512]{1,0:T(8,128)(2,1)S(1)} collective-permute-done((bf16[8,512]{1,0:T(8,128)(2,1)S(1)}, bf16[8,512]{1,0:T(8,128)(2,1)S(1)}, u32[]{:S(2)}, u32[]{:S(2)}) %collective-permute-start) | collective-permute-done | bytes 8224 | tf_op jit(solution)/shard_map/ppermute | solution.py:453
  31.7 0.0 copy-start.14
  31.7 0.6 copy-done.14
  32.3 6.7 %local_scan.1 = (f32[704,512]{1,0:T(8,128)}, f32[704,512]{1,0:T(8,128)}, f32[2,8,512]{2,1,0:T(8,128)}, f32[32,8,128]{2,1,0:T(8,128)}) custom-call(bf16[704,512]{1,0:T(8,128)(2,1)} %x_ref.1, bf16[8,512]{1,0:T(8,128)(2,1)} %copy-done.14, bf16[4,512]{1,0:T(4,128)(2,1)} %taps_ref.1, bf16[4,128,128]{2,1,0:T(8,128)(2,1)} %rmap_ref.1, ...), custom_call_target="tpu_custom_call" | custom-call | tf_op jit(solution)/shard_map/local_scan/pallas_call | solution.py:94
  39.0 8.3 %all-to-all-start = ((f32[32,8,128]{2,1,0:T(8,128)}), f32[32,8,128]{2,1,0:T(8,128)S(1)}, u32[]{:S(2)}, u32[]{:S(2)}) async-start(f32[32,8,128]{2,1,0:T(8,128)} %get-tuple-element.19), calls=%async_computation | async-start | bytes 262144 | tf_op jit(solution)/shard_map/all_to_all | solution.py:457
  47.3 0.6 pad_add_fusion.me_ref.refs_0_
  47.9 17.3 %all-to-all-done.arrived_ref = f32[32,8,128]{2,1,0:T(8,128)S(1)} async-done(((f32[32,8,128]{2,1,0:T(8,128)}), f32[32,8,128]{2,1,0:T(8,128)S(1)}, u32[]{:S(2)}, u32[]{:S(2)}) %all-to-all-start) | async-done | bytes 131104 | tf_op jit(solution)/shard_map/all_to_all | solution.py:457
  65.2 0.7 copy-done.4
  65.8 4.1 %branch_first.1 = (bf16[176,1024]{1,0:T(8,128)(2,1)}, bf16[176,1024]{1,0:T(8,128)(2,1)}) custom-call(s32[2]{0:T(128)} %pad_add_fusion.me_ref.refs_0_, f32[32,8,128]{2,1,0:T(8,128)} %copy-done.4, f32[2,8,512]{2,1,0:T(8,128)} %get-tuple-element.20.seg_ref, f32[704,512]{1,0:T(8,128)} %get-tuple-element.21.cum_ref, f32[704,512]{1,0:T(8,128)} %get-tuple-element.22.loc_ref, ...), custom_call_target="tpu_custom_call" | custom-call | flops 369098752 | bytes 3719168 | tf_op jit(solution)/shard_map/branch_first/pallas_call | solution.py:184
  69.9 1.4 collective-permute-start.1
  71.3 1.5 collective-permute-start.2
  72.7 6.3 %branch_rest.1.rest_ref = bf16[3,176,2048]{2,1,0:T(8,128)(2,1)} custom-call(s32[2]{0:T(128)} %pad_add_fusion.me_ref.refs_0_, f32[32,8,128]{2,1,0:T(8,128)} %copy-done.4, f32[2,8,512]{2,1,0:T(8,128)} %get-tuple-element.20.seg_ref, f32[704,512]{1,0:T(8,128)} %get-tuple-element.21.cum_ref, f32[704,512]{1,0:T(8,128)} %get-tuple-element.22.loc_ref, ...), custom_call_target="tpu_custom_call" | custom-call | flops 1107296256 | bytes 6963200 | tf_op jit(solution)/shard_map/branch_rest/pallas_call | solution.py:184
  79.1 1.7 collective-permute-done.1.low_ref
  80.8 0.0 collective-permute-done.2.high_ref
  80.8 0.7 copy-done.10
  81.5 0.7 copy-done.12
  82.2 3.1 %join.2 = (bf16[176,2048]{1,0:T(8,128)(2,1)}, bf16[176,2048]{1,0:T(8,128)(2,1)}) custom-call(bf16[3,176,2048]{2,1,0:T(8,128)(2,1)} %branch_rest.1.rest_ref, bf16[176,1024]{1,0:T(8,128)(2,1)} %copy-done.10, bf16[176,1024]{1,0:T(8,128)(2,1)} %copy-done.12), custom_call_target="tpu_custom_call" | custom-call | tf_op jit(solution)/shard_map/join/pallas_call | solution.py:431
  85.3 0.2 collective-permute-start.3
  85.5 2.5 %collective-permute-start.4 = (bf16[176,2048]{1,0:T(8,128)(2,1)}, bf16[176,2048]{1,0:T(8,128)(2,1)S(1)}, u32[]{:S(2)}, u32[]{:S(2)}) collective-permute-start(bf16[176,2048]{1,0:T(8,128)(2,1)} %get-tuple-element.26), channel_id=1, source_target_pairs={{0,3},{1,0},{2,1},{3,2},{4,7},{5,4},{6,5},{7,6},{8,11},{9,8},{10,9... | collective-permute-start | bytes 2162696 | tf_op jit(solution)/shard_map/ppermute | solution.py:442
  88.0 15.0 %collective-permute-done.3.left_ref = bf16[176,2048]{1,0:T(8,128)(2,1)S(1)} collective-permute-done((bf16[176,2048]{1,0:T(8,128)(2,1)}, bf16[176,2048]{1,0:T(8,128)(2,1)S(1)}, u32[]{:S(2)}, u32[]{:S(2)}) %collective-permute-start.3) | collective-permute-done | bytes 720928 | tf_op jit(solution)/shard_map/ppermute | solution.py:442
  103.0 0.0 collective-permute-done.4.right_ref
  103.0 0.9 copy-done.5
  103.8 0.3 copy-done.7
  104.1 6.9 %mid.1 = (bf16[176,2048]{1,0:T(8,128)(2,1)}, bf16[176,2048]{1,0:T(8,128)(2,1)}) custom-call(s32[2]{0:T(128)} %pad_add_fusion.me_ref.refs_0_, bf16[3,176,2048]{2,1,0:T(8,128)(2,1)} %branch_rest.1.rest_ref, bf16[176,2048]{1,0:T(8,128)(2,1)} %copy-done.5, bf16[176,2048]{1,0:T(8,128)(2,1)} %copy-done.7, bf16[704,2048]{1,0:T(8,128)(2,1)} %res_ref.1, ...), custom_call_target="tpu_custom_call" | custom-call | tf_op jit(solution)/shard_map/mid/pallas_call | solution.py:379
  111.0 0.1 collective-permute-start.6
  111.1 2.7 %collective-permute-start.5 = (bf16[176,2048]{1,0:T(8,128)(2,1)}, bf16[176,2048]{1,0:T(8,128)(2,1)S(1)}, u32[]{:S(2)}, u32[]{:S(2)}) collective-permute-start(bf16[176,2048]{1,0:T(8,128)(2,1)} %get-tuple-element.27.refs_2_), channel_id=1, source_target_pairs={{0,3},{1,0},{2,1},{3,2},{4,7},{5,4},{6,5},{7,6},{8,11},{9,8},{10,9... | collective-permute-start | bytes 2162696 | tf_op jit(solution)/shard_map/ppermute | solution.py:442
  113.8 14.3 %collective-permute-done.6.refs_4_ = bf16[176,2048]{1,0:T(8,128)(2,1)S(1)} collective-permute-done((bf16[176,2048]{1,0:T(8,128)(2,1)}, bf16[176,2048]{1,0:T(8,128)(2,1)S(1)}, u32[]{:S(2)}, u32[]{:S(2)}) %collective-permute-start.6) | collective-permute-done | bytes 720928 | tf_op jit(solution)/shard_map/ppermute | solution.py:442
  128.1 0.1 collective-permute-start.7
  128.2 0.0 collective-permute-done.5.refs_3_
  128.2 0.0 copy-start.1
  128.3 2.7 %collective-permute-start.8 = (bf16[176,1024]{1,0:T(8,128)(2,1)S(1)}, bf16[176,1024]{1,0:T(8,128)(2,1)S(1)}, u32[]{:S(2)}, u32[]{:S(2)}) collective-permute-start(bf16[176,1024]{1,0:T(8,128)(2,1)S(1)} %slice.35), channel_id=1, source_target_pairs={{0,3},{1,0},{2,1},{3,2},{4,7},{5,4},{6,5},{7,6},{8,11},{9,8},{10,9... | collective-permute-start | bytes 1081352 | tf_op jit(solution)/shard_map/ppermute | solution.py:442
  131.0 5.3 %collective-permute-done.7.refs_5_ = bf16[176,1024]{1,0:T(8,128)(2,1)S(1)} collective-permute-done((bf16[176,1024]{1,0:T(8,128)(2,1)S(1)}, bf16[176,1024]{1,0:T(8,128)(2,1)S(1)}, u32[]{:S(2)}, u32[]{:S(2)}) %collective-permute-start.7) | collective-permute-done | bytes 360480 | tf_op jit(solution)/shard_map/ppermute | solution.py:442
  136.3 0.0 collective-permute-done.8.refs_6_
  136.3 0.0 copy-start.3
  136.3 1.0 fusion
  137.3 3.9 %collective-permute-start.9 = (bf16[16,2048]{1,0:T(8,128)(2,1)S(1)}, bf16[16,2048]{1,0:T(8,128)(2,1)S(1)}, u32[]{:S(2)}, u32[]{:S(2)}) collective-permute-start(bf16[16,2048]{1,0:T(8,128)(2,1)S(1)} %fusion), channel_id=1, source_target_pairs={{0,4},{4,8},{8,12},{12,16},{16,20},{20,24},{24,28},{28,32},{32,36}... | collective-permute-start | bytes 196616 | tf_op jit(solution)/shard_map/ppermute | solution.py:453
  141.3 2.0 collective-permute-done.9.refs_1_
  143.2 0.0 copy-done
  143.3 0.0 copy-done.1
  143.3 0.0 copy-done.2
  143.3 0.0 copy-done.3
  143.3 0.6 copy-done.13
  143.9 15.6 %feed_first.1 = (bf16[176,1024]{1,0:T(8,128)(2,1)}, bf16[176,1024]{1,0:T(8,128)(2,1)}) custom-call(s32[2]{0:T(128)} %pad_add_fusion.me_ref.refs_0_, bf16[16,2048]{1,0:T(8,128)(2,1)} %copy-done.13, bf16[176,2048]{1,0:T(8,128)(2,1)} %get-tuple-element.27.refs_2_, bf16[176,2048]{1,0:T(8,128)(2,1)} %copy-done.1, bf16[176,2048]{1,0:T(8,128)(2,1)} %copy-done, ...), custom_call_target="tpu_custom_call" | custom-call | flops 3045064704 | bytes 18743296 | tf_op jit(solution)/shard_map/feed_first/pallas_call | solution.py:288
  159.4 0.1 collective-permute-start.10
  159.6 2.9 %collective-permute-start.11 = (bf16[176,1024]{1,0:T(8,128)(2,1)}, bf16[176,1024]{1,0:T(8,128)(2,1)S(1)}, u32[]{:S(2)}, u32[]{:S(2)}) collective-permute-start(bf16[176,1024]{1,0:T(8,128)(2,1)} %get-tuple-element.29), channel_id=1, source_target_pairs={{0,3},{1,0},{2,1},{3,2},{4,7},{5,4},{6,5},{7,6},{8,11},{9,8},{10,9... | collective-permute-start | bytes 1081352 | tf_op jit(solution)/shard_map/ppermute | solution.py:442
  162.4 22.6 %feed_rest.1.rest_ref = bf16[3,176,2048]{2,1,0:T(8,128)(2,1)} custom-call(s32[2]{0:T(128)} %pad_add_fusion.me_ref.refs_0_, bf16[16,2048]{1,0:T(8,128)(2,1)} %copy-done.13, bf16[176,2048]{1,0:T(8,128)(2,1)} %get-tuple-element.27.refs_2_, bf16[176,2048]{1,0:T(8,128)(2,1)} %copy-done.1, bf16[176,2048]{1,0:T(8,128)(2,1)} %copy-done, ...), custom_call_target="tpu_custom_call" | custom-call | flops 9135194112 | bytes 21626880 | tf_op jit(solution)/shard_map/feed_rest/pallas_call | solution.py:288
  185.0 0.0 collective-permute-done.10.low_ref
  185.0 0.0 copy-start.9
  185.0 0.0 collective-permute-done.11.high_ref
  185.0 0.7 copy-done.9
  185.8 0.7 copy-done.11
  186.5 3.1 %join.3 = (bf16[176,2048]{1,0:T(8,128)(2,1)}, bf16[176,2048]{1,0:T(8,128)(2,1)}) custom-call(bf16[3,176,2048]{2,1,0:T(8,128)(2,1)} %feed_rest.1.rest_ref, bf16[176,1024]{1,0:T(8,128)(2,1)} %copy-done.9, bf16[176,1024]{1,0:T(8,128)(2,1)} %copy-done.11), custom_call_target="tpu_custom_call" | custom-call | tf_op jit(solution)/shard_map/join/pallas_call | solution.py:431
  189.6 0.0 collective-permute-start.12
  189.6 2.7 %collective-permute-start.13 = (bf16[176,2048]{1,0:T(8,128)(2,1)}, bf16[176,2048]{1,0:T(8,128)(2,1)S(1)}, u32[]{:S(2)}, u32[]{:S(2)}) collective-permute-start(bf16[176,2048]{1,0:T(8,128)(2,1)} %get-tuple-element.31), channel_id=1, source_target_pairs={{0,3},{1,0},{2,1},{3,2},{4,7},{5,4},{6,5},{7,6},{8,11},{9,8},{10,9... | collective-permute-start | bytes 2162696 | tf_op jit(solution)/shard_map/ppermute | solution.py:442
  192.3 15.9 %collective-permute-done.12.left_ref = bf16[176,2048]{1,0:T(8,128)(2,1)S(1)} collective-permute-done((bf16[176,2048]{1,0:T(8,128)(2,1)}, bf16[176,2048]{1,0:T(8,128)(2,1)S(1)}, u32[]{:S(2)}, u32[]{:S(2)}) %collective-permute-start.12) | collective-permute-done | bytes 720928 | tf_op jit(solution)/shard_map/ppermute | solution.py:442
  208.2 0.0 collective-permute-done.13.right_ref
  208.2 0.9 copy-done.6
  209.1 0.3 copy-done.8
  209.4 4.6 %last.1 = bf16[176,2048]{1,0:T(8,128)(2,1)} custom-call(bf16[3,176,2048]{2,1,0:T(8,128)(2,1)} %feed_rest.1.rest_ref, bf16[176,2048]{1,0:T(8,128)(2,1)} %copy-done.6, bf16[176,2048]{1,0:T(8,128)(2,1)} %copy-done.8, bf16[176,2048]{1,0:T(8,128)(2,1)} %get-tuple-element.32.hidden_ref, f32[1,2048]{1,0:T(1,128)} %bitcast.10), custom_call_target="tpu_custom_call" | custom-call | tf_op jit(solution)/shard_map/last/pallas_call | solution.py:407
  (16 shorter events, 0.1 us)
Async XLA Ops:
  6.5 136.7 %all-gather.2.cloned.1.call-start = ((), (), s32[]{:S(2)}) async-start(), calls=%async_computation.1 | async-start | bytes 17842176 | tf_op jit(solution)/shard_map/all_gather | solution.py:485
  9.3 22.4 %collective-permute-start = (bf16[8,512]{1,0:T(8,128)(2,1)S(1)}, bf16[8,512]{1,0:T(8,128)(2,1)S(1)}, u32[]{:S(2)}, u32[]{:S(2)}) collective-permute-start(bf16[8,512]{1,0:T(8,128)(2,1)S(1)} %slice.24), channel_id=1, source_target_pairs={{0,4},{4,8},{8,12},{12,16},{16,20},{20,24},{24,28},{28,32},{32,36}... | collective-permute-start | bytes 24584 | tf_op jit(solution)/shard_map/ppermute | solution.py:453
  31.7 0.6 copy-start.14
  39.0 26.2 %all-to-all-start = ((f32[32,8,128]{2,1,0:T(8,128)}), f32[32,8,128]{2,1,0:T(8,128)S(1)}, u32[]{:S(2)}, u32[]{:S(2)}) async-start(f32[32,8,128]{2,1,0:T(8,128)} %get-tuple-element.19), calls=%async_computation | async-start | bytes 262144 | tf_op jit(solution)/shard_map/all_to_all | solution.py:457
  65.2 0.7 copy-start.4
  69.9 10.9 %collective-permute-start.1 = (bf16[176,1024]{1,0:T(8,128)(2,1)}, bf16[176,1024]{1,0:T(8,128)(2,1)S(1)}, u32[]{:S(2)}, u32[]{:S(2)}) collective-permute-start(bf16[176,1024]{1,0:T(8,128)(2,1)} %get-tuple-element.23), channel_id=1, source_target_pairs={{0,1},{1,2},{2,3},{3,0},{4,5},{5,6},{6,7},{7,4},{8,9},{9,10},{10,1... | collective-permute-start | bytes 1081352 | tf_op jit(solution)/shard_map/ppermute | solution.py:442
  71.3 9.5 %collective-permute-start.2 = (bf16[176,1024]{1,0:T(8,128)(2,1)}, bf16[176,1024]{1,0:T(8,128)(2,1)S(1)}, u32[]{:S(2)}, u32[]{:S(2)}) collective-permute-start(bf16[176,1024]{1,0:T(8,128)(2,1)} %get-tuple-element.24), channel_id=1, source_target_pairs={{0,3},{1,0},{2,1},{3,2},{4,7},{5,4},{6,5},{7,6},{8,11},{9,8},{10,9... | collective-permute-start | bytes 1081352 | tf_op jit(solution)/shard_map/ppermute | solution.py:442
  80.8 0.7 copy-start.10
  81.5 0.7 copy-start.12
  85.3 17.6 %collective-permute-start.3 = (bf16[176,2048]{1,0:T(8,128)(2,1)}, bf16[176,2048]{1,0:T(8,128)(2,1)S(1)}, u32[]{:S(2)}, u32[]{:S(2)}) collective-permute-start(bf16[176,2048]{1,0:T(8,128)(2,1)} %get-tuple-element.25), channel_id=1, source_target_pairs={{0,1},{1,2},{2,3},{3,0},{4,5},{5,6},{6,7},{7,4},{8,9},{9,10},{10,1... | collective-permute-start | bytes 2162696 | tf_op jit(solution)/shard_map/ppermute | solution.py:442
  85.5 17.4 %collective-permute-start.4 = (bf16[176,2048]{1,0:T(8,128)(2,1)}, bf16[176,2048]{1,0:T(8,128)(2,1)S(1)}, u32[]{:S(2)}, u32[]{:S(2)}) collective-permute-start(bf16[176,2048]{1,0:T(8,128)(2,1)} %get-tuple-element.26), channel_id=1, source_target_pairs={{0,3},{1,0},{2,1},{3,2},{4,7},{5,4},{6,5},{7,6},{8,11},{9,8},{10,9... | collective-permute-start | bytes 2162696 | tf_op jit(solution)/shard_map/ppermute | solution.py:442
  102.9 0.9 copy-start.5
  103.0 1.1 copy-start.7
  111.0 17.0 %collective-permute-start.6 = (bf16[176,2048]{1,0:T(8,128)(2,1)}, bf16[176,2048]{1,0:T(8,128)(2,1)S(1)}, u32[]{:S(2)}, u32[]{:S(2)}) collective-permute-start(bf16[176,2048]{1,0:T(8,128)(2,1)} %get-tuple-element.27.refs_2_), channel_id=1, source_target_pairs={{0,1},{1,2},{2,3},{3,0},{4,5},{5,6},{6,7},{7,4},{8,9},{9,10},{10,1... | collective-permute-start | bytes 2162696 | tf_op jit(solution)/shard_map/ppermute | solution.py:442
  111.1 17.1 %collective-permute-start.5 = (bf16[176,2048]{1,0:T(8,128)(2,1)}, bf16[176,2048]{1,0:T(8,128)(2,1)S(1)}, u32[]{:S(2)}, u32[]{:S(2)}) collective-permute-start(bf16[176,2048]{1,0:T(8,128)(2,1)} %get-tuple-element.27.refs_2_), channel_id=1, source_target_pairs={{0,3},{1,0},{2,1},{3,2},{4,7},{5,4},{6,5},{7,6},{8,11},{9,8},{10,9... | collective-permute-start | bytes 2162696 | tf_op jit(solution)/shard_map/ppermute | solution.py:442
  128.0 15.2 %copy-start = (bf16[176,2048]{1,0:T(8,128)(2,1)}, bf16[176,2048]{1,0:T(8,128)(2,1)S(1)}, u32[]{:S(2)}) copy-start(bf16[176,2048]{1,0:T(8,128)(2,1)S(1)} %collective-permute-done.6.refs_4_) | copy-start | bytes 2162692
  128.1 8.3 %collective-permute-start.7 = (bf16[176,1024]{1,0:T(8,128)(2,1)S(1)}, bf16[176,1024]{1,0:T(8,128)(2,1)S(1)}, u32[]{:S(2)}, u32[]{:S(2)}) collective-permute-start(bf16[176,1024]{1,0:T(8,128)(2,1)S(1)} %slice.33), channel_id=1, source_target_pairs={{0,1},{1,2},{2,3},{3,0},{4,5},{5,6},{6,7},{7,4},{8,9},{9,10},{10,1... | collective-permute-start | bytes 1081352 | tf_op jit(solution)/shard_map/ppermute | solution.py:442
  128.2 15.0 %copy-start.1 = (bf16[176,2048]{1,0:T(8,128)(2,1)}, bf16[176,2048]{1,0:T(8,128)(2,1)S(1)}, u32[]{:S(2)}) copy-start(bf16[176,2048]{1,0:T(8,128)(2,1)S(1)} %collective-permute-done.5.refs_3_) | copy-start | bytes 2162692
  128.3 8.1 %collective-permute-start.8 = (bf16[176,1024]{1,0:T(8,128)(2,1)S(1)}, bf16[176,1024]{1,0:T(8,128)(2,1)S(1)}, u32[]{:S(2)}, u32[]{:S(2)}) collective-permute-start(bf16[176,1024]{1,0:T(8,128)(2,1)S(1)} %slice.35), channel_id=1, source_target_pairs={{0,3},{1,0},{2,1},{3,2},{4,7},{5,4},{6,5},{7,6},{8,11},{9,8},{10,9... | collective-permute-start | bytes 1081352 | tf_op jit(solution)/shard_map/ppermute | solution.py:442
  136.3 6.9 %copy-start.2 = (bf16[176,1024]{1,0:T(8,128)(2,1)}, bf16[176,1024]{1,0:T(8,128)(2,1)S(1)}, u32[]{:S(2)}) copy-start(bf16[176,1024]{1,0:T(8,128)(2,1)S(1)} %collective-permute-done.7.refs_5_) | copy-start | bytes 1081348
  136.3 6.9 %copy-start.3 = (bf16[176,1024]{1,0:T(8,128)(2,1)}, bf16[176,1024]{1,0:T(8,128)(2,1)S(1)}, u32[]{:S(2)}) copy-start(bf16[176,1024]{1,0:T(8,128)(2,1)S(1)} %collective-permute-done.8.refs_6_) | copy-start | bytes 1081348
  137.3 5.9 %collective-permute-start.9 = (bf16[16,2048]{1,0:T(8,128)(2,1)S(1)}, bf16[16,2048]{1,0:T(8,128)(2,1)S(1)}, u32[]{:S(2)}, u32[]{:S(2)}) collective-permute-start(bf16[16,2048]{1,0:T(8,128)(2,1)S(1)} %fusion), channel_id=1, source_target_pairs={{0,4},{4,8},{8,12},{12,16},{16,20},{20,24},{24,28},{28,32},{32,36}... | collective-permute-start | bytes 196616 | tf_op jit(solution)/shard_map/ppermute | solution.py:453
  143.2 0.6 copy-start.13
  159.4 25.6 %collective-permute-start.10 = (bf16[176,1024]{1,0:T(8,128)(2,1)}, bf16[176,1024]{1,0:T(8,128)(2,1)S(1)}, u32[]{:S(2)}, u32[]{:S(2)}) collective-permute-start(bf16[176,1024]{1,0:T(8,128)(2,1)} %get-tuple-element.28), channel_id=1, source_target_pairs={{0,1},{1,2},{2,3},{3,0},{4,5},{5,6},{6,7},{7,4},{8,9},{9,10},{10,1... | collective-permute-start | bytes 1081352 | tf_op jit(solution)/shard_map/ppermute | solution.py:442
  159.6 25.5 %collective-permute-start.11 = (bf16[176,1024]{1,0:T(8,128)(2,1)}, bf16[176,1024]{1,0:T(8,128)(2,1)S(1)}, u32[]{:S(2)}, u32[]{:S(2)}) collective-permute-start(bf16[176,1024]{1,0:T(8,128)(2,1)} %get-tuple-element.29), channel_id=1, source_target_pairs={{0,3},{1,0},{2,1},{3,2},{4,7},{5,4},{6,5},{7,6},{8,11},{9,8},{10,9... | collective-permute-start | bytes 1081352 | tf_op jit(solution)/shard_map/ppermute | solution.py:442
  185.0 0.7 copy-start.9
  185.8 0.7 copy-start.11
  189.6 18.6 %collective-permute-start.12 = (bf16[176,2048]{1,0:T(8,128)(2,1)}, bf16[176,2048]{1,0:T(8,128)(2,1)S(1)}, u32[]{:S(2)}, u32[]{:S(2)}) collective-permute-start(bf16[176,2048]{1,0:T(8,128)(2,1)} %get-tuple-element.30), channel_id=1, source_target_pairs={{0,1},{1,2},{2,3},{3,0},{4,5},{5,6},{6,7},{7,4},{8,9},{9,10},{10,1... | collective-permute-start | bytes 2162696 | tf_op jit(solution)/shard_map/ppermute | solution.py:442
  189.6 18.6 %collective-permute-start.13 = (bf16[176,2048]{1,0:T(8,128)(2,1)}, bf16[176,2048]{1,0:T(8,128)(2,1)S(1)}, u32[]{:S(2)}, u32[]{:S(2)}) collective-permute-start(bf16[176,2048]{1,0:T(8,128)(2,1)} %get-tuple-element.31), channel_id=1, source_target_pairs={{0,3},{1,0},{2,1},{3,2},{4,7},{5,4},{6,5},{7,6},{8,11},{9,8},{10,9... | collective-permute-start | bytes 2162696 | tf_op jit(solution)/shard_map/ppermute | solution.py:442
  208.2 0.9 copy-start.6
  208.2 1.2 copy-start.8
Sparse Core Ops, SparseCore 0:
  9.2 128.1 all-gather.1

commit v3 on v2

--- a/solution.py
+++ b/solution.py
@@ -13,6 +13,7 @@
 LANES = 128
 BLOCKS = 4
 HALO = 16
+MIB = 1 << 20
 GELU_A = 0.7978845608028654
 GELU_B = 0.044715
 
@@ -112,65 +113,65 @@
             pltpu.VMEM((length, LANES), jnp.float32),
             pltpu.VMEM((length, LANES), jnp.float32),
         ],
+        compiler_params=pltpu.CompilerParams(vmem_limit_bytes=12 * MIB),
         name="local_scan",
     )(x, edge, taps, rmap, imap, soft, jump)
 
 
 def branch_kernel(me_ref, arrived_ref, seg_ref, cum_ref, loc_ref, gate_ref, w_ref, *rest):
     outs, carry, branch = rest[:-2], rest[-2], rest[-1]
-    block = row_block_at(pl.program_id(0), me_ref, len(outs) == 2)
-    groups = cum_ref.shape[1] // LANES
-    rows = cum_ref.shape[0]
+    length, channels = cum_ref.shape
+    groups = channels // LANES
+    rows = length // BLOCKS
     per_block = SEGMENTS // BLOCKS
     seg_rows = rows // per_block
 
-    @pl.when(pl.program_id(0) == 0)
-    def _():
-        def join(j, state):
-            return arrived_ref[j, 0:groups, :] * state + arrived_ref[j, groups : 2 * groups, :]
-
-        state = lax.fori_loop(0, me_ref[1], join, jnp.zeros((groups, LANES), jnp.float32))
-        for g in range(groups):
-            lanes = slice(g * LANES, (g + 1) * LANES)
-            now = state[g : g + 1, :]
-            for s in range(SEGMENTS):
-                carry[s, 0:1, lanes] = now
-                now = seg_ref[0, s : s + 1, lanes] * now + seg_ref[1, s : s + 1, lanes]
-
-    for part in range(per_block):
-        at = slice(part * seg_rows, (part + 1) * seg_rows)
-        state = loc_ref[at, :] + cum_ref[at, :] * carry[block * per_block + part, 0:1, :]
-        branch[at, :] = state
-    gate = gate_ref[...].astype(jnp.float32)
-    out = (branch[...] * gelu(gate)).astype(jnp.bfloat16)
-    share = jnp.dot(out, w_ref[...], preferred_element_type=jnp.float32).astype(jnp.bfloat16)
-    put(outs, share)
-
-
-def row_block_at(step, me_ref, opposite):
-    turned = 2 if opposite else 1 + (step * (5 - step) >> 1)
-    return lax.rem(me_ref[0] + turned, BLOCKS)
+    def join(j, state):
+        return arrived_ref[j, 0:groups, :] * state + arrived_ref[j, groups : 2 * groups, :]
+
+    state = lax.fori_loop(0, me_ref[1], join, jnp.zeros((groups, LANES), jnp.float32))
+    for g in range(groups):
+        lanes = slice(g * LANES, (g + 1) * LANES)
+        now = state[g : g + 1, :]
+        for s in range(SEGMENTS):
+            carry[s, 0:1, lanes] = now
+            now = seg_ref[0, s : s + 1, lanes] * now + seg_ref[1, s : s + 1, lanes]
+
+    for b, steps in enumerate((2,) if len(outs) == 2 else (1, 3, 0)):
+        block = lax.rem(me_ref[0] + steps, BLOCKS)
+        first = pl.multiple_of(block * rows, rows)
+        for part in range(per_block):
+            at = pl.ds(pl.multiple_of(first + part * seg_rows, 8), seg_rows)
+            state = loc_ref[at, :] + cum_ref[at, :] * carry[block * per_block + part, 0:1, :]
+            branch[part * seg_rows : (part + 1) * seg_rows, :] = state
+        gate = gate_ref[pl.ds(first, rows), :].astype(jnp.float32)
+        out = (branch[...] * gelu(gate)).astype(jnp.bfloat16)
+        share = jnp.dot(out, w_ref[...], preferred_element_type=jnp.float32).astype(jnp.bfloat16)
+        if len(outs) == 2:
+            put(outs, share)
+        else:
+            outs[0][b] = share
 
 
 def put(outs, share):
-    if len(outs) == 1:
-        outs[0][0] = share
-    else:
-        half = share.shape[1] // 2
-        outs[0][...] = share[:, :half]
-        outs[1][...] = share[:, half:]
-
-
-def share_outputs(count, rows, width, halves):
-    if halves:
-        return (
-            [pl.BlockSpec((rows, width // 2), lambda b, *_: (0, 0))] * 2,
-            [jax.ShapeDtypeStruct((rows, width // 2), jnp.bfloat16)] * 2,
-        )
-    return (
-        [pl.BlockSpec((1, rows, width), lambda b, *_: (b, 0, 0))],
-        [jax.ShapeDtypeStruct((count, rows, width), jnp.bfloat16)],
-    )
+    half = share.shape[1] // 2
+    outs[0][...] = share[:, :half]
+    outs[1][...] = share[:, half:]
+
+
+VMEM = pl.BlockSpec(memory_space=pltpu.VMEM)
+
+
+def vm(value):
+    return pltpu.with_memory_space_constraint(value, pltpu.VMEM)
+
+
+def vm_out(shape):
+    return pltpu.VMEM(shape, jnp.bfloat16)
+
+
+def share_shapes(count, rows, width, halves):
+    return [vm_out((rows, width // 2))] * 2 if halves else [vm_out((count, rows, width))]
 
 
 def branch_shares(me, arrived, seg, cum, loc, gate, weight, halves):
@@ -178,42 +179,42 @@
     width = weight.shape[1]
     rows = length // BLOCKS
     count = 1 if halves else BLOCKS - 1
-    row_block = pl.BlockSpec((rows, channels), lambda b, me: (row_block_at(b, me, halves), 0))
-    whole = lambda a: pl.BlockSpec(a.shape, lambda b, me: (0,) * a.ndim)
-    out_specs, out_shape = share_outputs(count, rows, width, halves)
+    out_shape = share_shapes(count, rows, width, halves)
     return pl.pallas_call(
         branch_kernel,
-        grid_spec=pltpu.PrefetchScalarGridSpec(
-            num_scalar_prefetch=1,
-            grid=(count,),
-            in_specs=[whole(arrived), whole(seg), row_block, row_block, row_block, whole(weight)],
-            out_specs=out_specs,
-            scratch_shapes=[
-                pltpu.VMEM((SEGMENTS, 1, channels), jnp.float32),
-                pltpu.VMEM((rows, channels), jnp.float32),
-            ],
-        ),
+        in_specs=[pl.BlockSpec(memory_space=pltpu.SMEM), *[VMEM] * 6],
+        out_specs=[VMEM] * len(out_shape),
         out_shape=out_shape,
+        scratch_shapes=[
+            pltpu.VMEM((SEGMENTS, 1, channels), jnp.float32),
+            pltpu.VMEM((rows, channels), jnp.float32),
+        ],
         cost_estimate=pl.CostEstimate(
             flops=2 * count * rows * channels * width,
             bytes_accessed=count * rows * (10 * channels + 2 * width) + 2 * channels * width,
             transcendentals=count * rows * channels,
         ),
+        compiler_params=pltpu.CompilerParams(vmem_limit_bytes=20 * MIB),
         name="branch_first" if halves else "branch_rest",
-    )(me, arrived, seg, cum, loc, gate, weight)
+    )(me, *map(vm, (arrived, seg, cum, loc)), gate, weight)
 
 
 def feed_kernel(*refs, names, first):
-    me_ref, outside, own, right, left, low, high, w_ref, w_all, gk_ref, vk_ref = refs[:11]
-    outs = refs[11:-5]
-    lhs, up, act, down, sem = refs[-5:]
-    chunk = pl.program_id(0)
+    me_ref, outside, own, right, left, low, high, weights, gk_ref, vk_ref = refs[:10]
+    outs = refs[10:-7]
+    lhs, up_a, up_b, act, ring, down, sems = refs[-7:]
     rows = own.shape[0]
     tall = rows + HALO
     taps = gk_ref.shape[0]
-    width, units = down.shape
+    shards, chunks, shard_rows, _ = down.shape
+    width = shards * shard_rows
     half = width // 2
-    fetch = pltpu.make_async_copy(w_all.at[:, pl.ds(2 * units, units)], down, sem)
+    slots = ring.shape[0]
+    get_down = pltpu.make_async_copy(weights.at[:, pl.ds(2 * chunks, chunks)], down, sems.at[slots])
+
+    def get(chunk):
+        slot = lax.rem(chunk, slots)
+        return pltpu.make_async_copy(weights.at[:, pl.ds(2 * chunk, 2)], ring.at[slot], sems.at[slot])
 
     def fill(b, name):
         at = b * tall
@@ -237,96 +238,120 @@
         else:
             lhs[at : at + rows, :] = {"own": own, "right": right, "left": left}[name][...]
 
-    @pl.when(chunk == 0)
-    def _():
-        fetch.start()
-        for b, name in enumerate(names):
-            fill(b, name)
-
-    up[...] = (
-        jnp.dot(lhs[...], w_ref[...], preferred_element_type=jnp.float32)
-        .astype(jnp.bfloat16)
-        .astype(jnp.float32)
-    )
-    gate_taps = gk_ref[...].astype(jnp.float32)
-    value_taps = vk_ref[...].astype(jnp.float32)
-    lanes = pl.ds(pl.multiple_of(chunk * LANES, LANES), LANES)
-    for b in range(len(names)):
-        gate = jnp.zeros((rows, LANES), jnp.float32)
-        value = jnp.zeros((rows, LANES), jnp.float32)
-        for k in range(taps):
-            at = b * tall + HALO - (taps - 1) + k
-            gate = gate + up[at : at + rows, 0:LANES] * gate_taps[k : k + 1, :]
-            value = value + up[at : at + rows, LANES : 2 * LANES] * value_taps[k : k + 1, :]
-        act[b * rows : (b + 1) * rows, lanes] = (gelu(gate) * value).astype(jnp.bfloat16)
-
-    @pl.when(chunk == pl.num_programs(0) - 1)
-    def _():
-        fetch.wait()
+    def activate(chunk, up):
+        lanes = pl.ds(pl.multiple_of(chunk * LANES, LANES), LANES)
+        gate_taps = gk_ref[:, lanes].astype(jnp.float32)
+        value_taps = vk_ref[:, lanes].astype(jnp.float32)
         for b in range(len(names)):
-            share = lax.dot_general(
-                act[b * rows : (b + 1) * rows, :],
-                down[...],
-                (((1,), (1,)), ((), ())),
-                preferred_element_type=jnp.float32,
-            ).astype(jnp.bfloat16)
-            if first:
-                put(outs, share)
-            else:
-                outs[0][b] = share
+            gate = jnp.zeros((rows, LANES), jnp.float32)
+            value = jnp.zeros((rows, LANES), jnp.float32)
+            for k in range(taps):
+                at = b * tall + HALO - (taps - 1) + k
+                gate = gate + up[at : at + rows, 0:LANES] * gate_taps[k : k + 1, :]
+                value = value + up[at : at + rows, LANES : 2 * LANES] * value_taps[k : k + 1, :]
+            act[b * rows : (b + 1) * rows, lanes] = (gelu(gate) * value).astype(jnp.bfloat16)
+
+    def project(chunk, up):
+        slot = lax.rem(chunk, slots)
+        sides = [ring[slot, :, side].reshape(width, LANES) for side in range(2)]
+        up[...] = (
+            jnp.dot(lhs[...], jnp.concatenate(sides, axis=1), preferred_element_type=jnp.float32)
+            .astype(jnp.bfloat16)
+            .astype(jnp.float32)
+        )
+
+    for chunk in range(slots - 1):
+        get(jnp.int32(chunk)).start()
+    get_down.start()
+    for b, name in enumerate(names):
+        fill(b, name)
+    get(jnp.int32(0)).wait()
+    project(jnp.int32(0), up_a)
+
+    def ahead(chunk):
+        @pl.when(chunk < chunks)
+        def _():
+            get(chunk).start()
+
+    def pair(i, carry):
+        chunk = 2 * i
+        ahead(chunk + 3)
+        ahead(chunk + 4)
+        get(chunk + 1).wait()
+        get(chunk + 2).wait()
+        activate(chunk, up_a)
+        project(chunk + 1, up_b)
+        activate(chunk + 1, up_b)
+        project(chunk + 2, up_a)
+        return carry
+
+    lax.fori_loop(0, chunks // 2, pair, 0)
+    get_down.wait()
+    activate(jnp.int32(chunks - 1), up_a)
+    turned = jnp.concatenate([down[:, c].reshape(width, LANES) for c in range(chunks)], axis=1)
+    share = lax.dot_general(
+        act[...], turned, (((1,), (1,)), ((), ())), preferred_element_type=jnp.float32
+    ).astype(jnp.bfloat16)
+    if first:
+        put(outs, share)
+    else:
+        for b in range(len(names)):
+            outs[0][b] = share[b * rows : (b + 1) * rows, :]
 
 
 def feed(me, outside, blocks, weights, gate_kernel, value_kernel, names, first):
     count = len(names)
     rows, width = blocks[0].shape
     units = gate_kernel.shape[1]
-    chunks = units // LANES
-    taps = gate_kernel.shape[0]
-    out_specs, out_shape = share_outputs(count, rows, width, first)
-    if not first:
-        out_specs = [pl.BlockSpec((count, rows, width), lambda c: (0, 0, 0))]
+    assert units // LANES % 2 == 1
+    shards, _, shard_rows, _ = weights.shape
+    tall = count * (rows + HALO)
+    out_shape = share_shapes(count, rows, width, first)
     return pl.pallas_call(
         functools.partial(feed_kernel, names=names, first=first),
-        grid=(chunks,),
         in_specs=[
             pl.BlockSpec(memory_space=pltpu.SMEM),
-            *[pl.BlockSpec(memory_space=pltpu.VMEM)] * (1 + len(blocks)),
-            pl.BlockSpec((width, 2 * LANES), lambda c: (0, c)),
+            *[VMEM] * (1 + len(blocks)),
             pl.BlockSpec(memory_space=pl.ANY),
-            pl.BlockSpec((taps, LANES), lambda c: (0, c)),
-            pl.BlockSpec((taps, LANES), lambda c: (0, c)),
-        ],
-        out_specs=out_specs,
+            VMEM,
+            VMEM,
+        ],
+        out_specs=[VMEM] * len(out_shape),
         out_shape=out_shape,
         scratch_shapes=[
-            pltpu.VMEM((count * (rows + HALO), width), jnp.bfloat16),
-            pltpu.VMEM((count * (rows + HALO), 2 * LANES), jnp.float32),
+            pltpu.VMEM((tall, width), jnp.bfloat16),
+            pltpu.VMEM((tall, 2 * LANES), jnp.float32),
+            pltpu.VMEM((tall, 2 * LANES), jnp.float32),
             pltpu.VMEM((count * rows, units), jnp.bfloat16),
-            pltpu.VMEM((width, units), jnp.bfloat16),
-            pltpu.SemaphoreType.DMA,
+            pltpu.VMEM((4, shards, 2, shard_rows, LANES), jnp.bfloat16),
+            pltpu.VMEM((shards, units // LANES, shard_rows, LANES), jnp.bfloat16),
+            pltpu.SemaphoreType.DMA((5,)),
         ],
         cost_estimate=pl.CostEstimate(
             flops=6 * count * rows * width * units,
             bytes_accessed=6 * width * units + 4 * count * rows * width,
             transcendentals=count * rows * units,
         ),
+        compiler_params=pltpu.CompilerParams(vmem_limit_bytes=36 * MIB),
         name="feed_first" if first else "feed_rest",
-    )(me, outside, *blocks, weights, weights, gate_kernel, value_kernel)
+    )(me, vm(outside), *map(vm, blocks), weights, gate_kernel, value_kernel)
 
 
 def pack_kernel(gate_ref, value_ref, turned_ref, out_ref):
-    units = gate_ref.shape[1]
-    for at in range(0, units, LANES):
-        out_ref[:, 2 * at : 2 * at + LANES] = gate_ref[:, at : at + LANES]
-        out_ref[:, 2 * at + LANES : 2 * at + 2 * LANES] = value_ref[:, at : at + LANES]
-    out_ref[:, 2 * units :] = turned_ref[...]
+    chunks = gate_ref.shape[1] // LANES
+    for c in range(chunks):
+        lanes = slice(c * LANES, (c + 1) * LANES)
+        out_ref[2 * c] = gate_ref[:, lanes]
+        out_ref[2 * c + 1] = value_ref[:, lanes]
+        out_ref[2 * chunks + c] = turned_ref[:, lanes]
 
 
 def packed(gate, value, turned):
     rows, units = gate.shape
     return pl.pallas_call(
         pack_kernel,
-        out_shape=jax.ShapeDtypeStruct((rows, 3 * units), jnp.bfloat16),
+        out_shape=jax.ShapeDtypeStruct((3 * units // LANES, rows, LANES), jnp.bfloat16),
+        compiler_params=pltpu.CompilerParams(vmem_limit_bytes=8 * MIB),
         name="pack",
     )(gate, value, turned)
 
@@ -371,9 +396,6 @@
     by_rows(rows, body)
 
 
-VMEM = pl.BlockSpec(memory_space=pltpu.VMEM)
-
-
 def mid(me, rest, left, right, residual, mix_gain, inner_gain):
     rows, width = left.shape
     return pl.pallas_call(
@@ -385,10 +407,11 @@
             VMEM, VMEM,
         ],
         out_specs=[VMEM, VMEM],
-        out_shape=[jax.ShapeDtypeStruct((rows, width), jnp.bfloat16)] * 2,
+        out_shape=[vm_out((rows, width))] * 2,
         scratch_shapes=[pltpu.VMEM((rows, width), jnp.bfloat16), pltpu.SemaphoreType.DMA],
+        compiler_params=pltpu.CompilerParams(vmem_limit_bytes=12 * MIB),
         name="mid",
-    )(me, rest, left, right, residual, mix_gain, inner_gain)
+    )(me, vm(rest), vm(left), vm(right), residual, mix_gain, inner_gain)
 
 
 def last_kernel(rest_ref, left_ref, right_ref, hidden_ref, gain_ref, out_ref):
@@ -409,8 +432,9 @@
         in_specs=[VMEM] * 5,
         out_specs=VMEM,
         out_shape=jax.ShapeDtypeStruct(hidden.shape, jnp.bfloat16),
+        compiler_params=pltpu.CompilerParams(vmem_limit_bytes=12 * MIB),
         name="last",
-    )(rest, left, right, hidden, gain)
+    )(*map(vm, (rest, left, right, hidden)), gain)
 
 
 def join_kernel(rest_ref, low_ref, high_ref, right_ref, left_ref):
@@ -432,9 +456,10 @@
         join_kernel,
         in_specs=[VMEM] * 3,
         out_specs=[VMEM] * 2,
-        out_shape=[jax.ShapeDtypeStruct((rows, width), jnp.bfloat16)] * 2,
+        out_shape=[vm_out((rows, width))] * 2,
+        compiler_params=pltpu.CompilerParams(vmem_limit_bytes=12 * MIB),
         name="join",
-    )(rest, low, high)
+    )(*map(vm, (rest, low, high)))
 
 
 def turn(value, axis, steps):
@@ -482,7 +507,8 @@
     me = jnp.stack([tp_me, lax.axis_index("sp").astype(jnp.int32)])
 
     edge = from_behind(mix_input[mix_input.shape[0] - 8 :], "sp")
-    weights = lax.all_gather(packed(gate_weight, value_weight, down_weight.T), "sp", axis=0, tiled=True)
+    shard = packed(gate_weight, value_weight, down_weight.T)
+    weights = lax.all_gather(shard, "sp", axis=0, tiled=True).reshape(n_sp, *shard.shape)
 
     cum, loc, seg, ends = local_scan(
         mix_input, edge, mix_kernel, recur_gate_map, input_gate_map, decay_param[None], jump_log, n_sp

time: 222 us -> 204 us (0.919)
  Pallas kernels: 75 us -> 44.4 us
  local copies, waits for them, and re-layouts: 7.79 us -> 17.1 us
  waiting for transfers between devices: 88.1 us -> 91 us
    pallas_call x2, Pallas kernels: 38.1 us -> 28 us  [feed(): pl.pallas_call(functools.partial(feed_kernel, names=names, first=first),...]
    pallas_call x3, Pallas kernels: 12.4 us -> 4.97 us  [the longest x2 4.08 us: branch_shares(): pl.pallas_call(branch_kernel, in_specs=[pl.BlockSpec(memory_space=pltpu.S...]
    unnamed x30 -> x46, local copies, waits for them, and re-layouts: 7.03 us -> 14.1 us
    pallas_call x2, Pallas kernels: 6.16 us -> 0.44 us  [join(): pl.pallas_call(join_kernel, in_specs=[VMEM] * 3, out_specs=[VMEM] * 2, ou...]
    pallas_call x1, Pallas kernels: 6.92 us -> 3.55 us  [mid(): pl.pallas_call(mid_kernel, in_specs=[pl.BlockSpec(memory_space=pltpu.SMEM...]
    ppermute x12, waiting for transfers between devices: 52.2 us -> 54.9 us  [turn(): lax.ppermute(value, axis, [(i, (i + steps) % count) for i in range(count)])]
  transfers between devices with their start and end apart: 16 -> 16, of which waited for: 8 -> 8; matrix products, arithmetic and copies ran while one was open for 1% -> 2% of each run, Pallas kernels for 22% -> 15%
where the time goes in v3:
time: 204 us; the launch traced here: 202 us
  waiting for transfers between devices  91 us (45%)
  Pallas kernels  44.4 us (22%)
  starting transfers between devices  36.1 us (18%)
  local copies, waits for them, and re-layouts  17.1 us (8%)
  between operations  13.6 us (7%)
    ppermute x12, waiting for transfers between devices, turn(): lax.ppermute(value, axis, [(i, (i + steps) % count) for i in range(count)])  54.9 us
    pallas_call x2, Pallas kernels, feed(): pl.pallas_call(functools.partial(feed_kernel, names=names, first=first),...  28 us
    ppermute x2, waiting for transfers between devices, from_behind(): return lax.ppermute(value, axis, [(i, i + 1) for i in range(count - 1)])  18.1 us
    all_to_all x1, waiting for transfers between devices, exchanged(): return lax.all_to_all(tiles, axis, split_axis=0, concat_axis=0, tiled=True)  17.9 us
    ppermute x12, starting transfers between devices, turn(): lax.ppermute(value, axis, [(i, (i + steps) % count) for i in range(count)])  17.8 us
    unnamed x46, local copies, waits for them, and re-layouts  14.1 us
    ppermute x2, starting transfers between devices, from_behind(): return lax.ppermute(value, axis, [(i, i + 1) for i in range(count - 1)])  10.2 us
    all_to_all x1, starting transfers between devices, exchanged(): return lax.all_to_all(tiles, axis, split_axis=0, concat_axis=0, tiled=True)  8.11 us
  transfers between devices with their start and end apart: 16, of which 8 were waited for; matrix products, arithmetic and copies ran while one was open for 2% of the time, Pallas kernels for 15%

profile of v3, /device:TPU:33, one launch (start us, length us, event | category | flops | bytes accessed | tf_op | source)
XLA Modules:
  0.0 202.4 jit_solution(5186026379813111283)
XLA Ops:
  6.6 0.9 copy-done.7
  7.5 0.9 copy-done.8
  8.4 0.9 copy-done.9
  9.3 0.9 pack.1
  10.2 0.1 all-gather.2.cloned.1.call-update
  10.3 0.7 slice.24
  11.0 5.7 %collective-permute-start = (bf16[8,512]{1,0:T(8,128)(2,1)S(1)}, bf16[8,512]{1,0:T(8,128)(2,1)S(1)}, u32[]{:S(2)}, u32[]{:S(2)}) collective-permute-start(bf16[8,512]{1,0:T(8,128)(2,1)S(1)} %slice.24), channel_id=1, source_target_pairs={{0,4},{4,8},{8,12},{12,16},{16,20},{20,24},{24,28},{28,32},{32,36}... | collective-permute-start | bytes 24584 | tf_op jit(solution)/shard_map/ppermute | solution.py:478
  16.7 16.6 %collective-permute-done.edge_ref = bf16[8,512]{1,0:T(8,128)(2,1)S(1)} collective-permute-done((bf16[8,512]{1,0:T(8,128)(2,1)S(1)}, bf16[8,512]{1,0:T(8,128)(2,1)S(1)}, u32[]{:S(2)}, u32[]{:S(2)}) %collective-permute-start) | collective-permute-done | bytes 8224 | tf_op jit(solution)/shard_map/ppermute | solution.py:478
  33.3 1.4 copy-done.5
  34.7 1.1 copy-done.6
  35.8 0.9 copy-done.13
  36.7 0.9 copy-done.14
  37.6 0.7 copy-done.21
  38.3 0.7 copy-done.22
  39.0 5.0 %local_scan.1 = (f32[704,512]{1,0:T(8,128)S(1)}, f32[704,512]{1,0:T(8,128)S(1)}, f32[2,8,512]{2,1,0:T(8,128)S(1)}, f32[32,8,128]{2,1,0:T(8,128)S(1)}) custom-call(bf16[704,512]{1,0:T(8,128)(2,1)S(1)} %copy-done.6, bf16[8,512]{1,0:T(8,128)(2,1)S(1)} %collective-permute-done.edge_ref, bf16[4,512]{1,0:T(4,128)(2,1)S(1)} %copy-done.21, ...), custom_call_target="tpu_custom_call" | custom-call | tf_op jit(solution)/shard_map/local_scan/pallas_call | solution.py:95
  44.0 1.1 copy-done.1
  45.1 0.6 copy-done.10
  45.7 0.7 copy-done.15
  46.4 8.1 %all-to-all-start = ((f32[32,8,128]{2,1,0:T(8,128)}), f32[32,8,128]{2,1,0:T(8,128)}, u32[]{:S(2)}, u32[]{:S(2)}) async-start(f32[32,8,128]{2,1,0:T(8,128)} %copy-done.15), calls=%async_computation | async-start | bytes 262144 | tf_op jit(solution)/shard_map/all_to_all | solution.py:482
  54.5 0.1 pad_add_fusion.me_ref.refs_0_
  54.6 17.9 %all-to-all-done.arrived_ref = f32[32,8,128]{2,1,0:T(8,128)} async-done(((f32[32,8,128]{2,1,0:T(8,128)}), f32[32,8,128]{2,1,0:T(8,128)}, u32[]{:S(2)}, u32[]{:S(2)}) %all-to-all-start) | async-done | bytes 131104 | tf_op jit(solution)/shard_map/all_to_all | solution.py:482
  72.5 1.4 copy-done.2
  73.9 1.1 copy-done.4
  75.0 0.8 copy-done.11
  75.8 1.6 branch_first.1
  77.4 1.4 collective-permute-start.1
  78.9 1.7 collective-permute-start.2
  80.6 2.5 %branch_rest.1.rest_ref = bf16[3,176,2048]{2,1,0:T(8,128)(2,1)S(1)} custom-call(s32[2]{0:T(128)S(1)} %pad_add_fusion.me_ref.refs_0_, f32[32,8,128]{2,1,0:T(8,128)} %all-to-all-done.arrived_ref, f32[2,8,512]{2,1,0:T(8,128)S(1)} %copy-done.12, f32[704,512]{1,0:T(8,128)S(1)} %get-tuple-element.21.cum_ref, f32[704,512]{1,0:T(8,128)S(1)} %copy-done.2, ...), custom_call_target="tpu_custom_call" | custom-call | flops 1107296256 | bytes 6963200 | tf_op jit(solution)/shard_map/branch_rest/pallas_call | solution.py:183
  83.1 0.0 copy-start.3
  83.1 5.2 %collective-permute-done.1.low_ref = bf16[176,1024]{1,0:T(8,128)(2,1)S(1)} collective-permute-done((bf16[176,1024]{1,0:T(8,128)(2,1)S(1)}, bf16[176,1024]{1,0:T(8,128)(2,1)S(1)}, u32[]{:S(2)}, u32[]{:S(2)}) %collective-permute-start.1) | collective-permute-done | bytes 360480 | tf_op jit(solution)/shard_map/ppermute | solution.py:467
  88.3 0.0 collective-permute-done.2.high_ref
  88.3 0.2 join.2
  88.5 1.0 collective-permute-start.3
  89.5 1.8 collective-permute-start.4
  91.3 14.8 %collective-permute-done.3.left_ref = bf16[176,2048]{1,0:T(8,128)(2,1)S(1)} collective-permute-done((bf16[176,2048]{1,0:T(8,128)(2,1)S(1)}, bf16[176,2048]{1,0:T(8,128)(2,1)S(1)}, u32[]{:S(2)}, u32[]{:S(2)}) %collective-permute-start.3) | collective-permute-done | bytes 720928 | tf_op jit(solution)/shard_map/ppermute | solution.py:467
  106.1 0.0 collective-permute-done.4.right_ref
  106.1 0.0 copy-start.16
  106.1 0.0 copy-start.17
  106.1 3.5 %mid.1 = (bf16[176,2048]{1,0:T(8,128)(2,1)S(1)}, bf16[176,2048]{1,0:T(8,128)(2,1)S(1)}) custom-call(s32[2]{0:T(128)S(1)} %pad_add_fusion.me_ref.refs_0_, bf16[3,176,2048]{2,1,0:T(8,128)(2,1)S(1)} %branch_rest.1.rest_ref, bf16[176,2048]{1,0:T(8,128)(2,1)S(1)} %collective-permute-done.3.left_ref, bf16[176,2048]{1,0:T(8,128)(2,1)S(1)} %collective-permute-done.4.right_ref, ...), custom_call_target="tpu_custom_call" | custom-call | tf_op jit(solution)/shard_map/mid/pallas_call | solution.py:401
  109.7 0.1 collective-permute-start.6
  109.8 2.6 %collective-permute-start.5 = (bf16[176,2048]{1,0:T(8,128)(2,1)S(1)}, bf16[176,2048]{1,0:T(8,128)(2,1)S(1)}, u32[]{:S(2)}, u32[]{:S(2)}) collective-permute-start(bf16[176,2048]{1,0:T(8,128)(2,1)S(1)} %get-tuple-element.27.refs_2_), channel_id=1, source_target_pairs={{0,3},{1,0},{2,1},{3,2},{4,7},{5,4},{6,5},{7,6},{8,11},{9,8},{10,9... | collective-permute-start | bytes 2162696 | tf_op jit(solution)/shard_map/ppermute | solution.py:467
  112.5 14.0 %collective-permute-done.6.refs_4_ = bf16[176,2048]{1,0:T(8,128)(2,1)S(1)} collective-permute-done((bf16[176,2048]{1,0:T(8,128)(2,1)S(1)}, bf16[176,2048]{1,0:T(8,128)(2,1)S(1)}, u32[]{:S(2)}, u32[]{:S(2)}) %collective-permute-start.6) | collective-permute-done | bytes 720928 | tf_op jit(solution)/shard_map/ppermute | solution.py:467
  126.5 0.8 slice.33
  127.3 0.0 collective-permute-start.7
  127.3 0.0 collective-permute-done.5.refs_3_
  127.3 0.8 slice.35
  128.1 2.7 %collective-permute-start.8 = (bf16[176,1024]{1,0:T(8,128)(2,1)}, bf16[176,1024]{1,0:T(8,128)(2,1)}, u32[]{:S(2)}, u32[]{:S(2)}) collective-permute-start(bf16[176,1024]{1,0:T(8,128)(2,1)} %slice.35), channel_id=1, source_target_pairs={{0,3},{1,0},{2,1},{3,2},{4,7},{5,4},{6,5},{7,6},{8,11},{9,8},{10,9... | collective-permute-start | bytes 1081352 | tf_op jit(solution)/shard_map/ppermute | solution.py:467
  130.8 5.0 %collective-permute-done.7.refs_5_ = bf16[176,1024]{1,0:T(8,128)(2,1)S(1)} collective-permute-done((bf16[176,1024]{1,0:T(8,128)(2,1)}, bf16[176,1024]{1,0:T(8,128)(2,1)S(1)}, u32[]{:S(2)}, u32[]{:S(2)}) %collective-permute-start.7) | collective-permute-done | bytes 360480 | tf_op jit(solution)/shard_map/ppermute | solution.py:467
  135.8 0.0 collective-permute-done.8.refs_6_
  135.8 0.8 slice.36
  136.6 4.4 %collective-permute-start.9 = (bf16[16,2048]{1,0:T(8,128)(2,1)S(1)}, bf16[16,2048]{1,0:T(8,128)(2,1)S(1)}, u32[]{:S(2)}, u32[]{:S(2)}) collective-permute-start(bf16[16,2048]{1,0:T(8,128)(2,1)S(1)} %fusion), channel_id=1, source_target_pairs={{0,4},{4,8},{8,12},{12,16},{16,20},{20,24},{24,28},{28,32},{32,36}... | collective-permute-start | bytes 196616 | tf_op jit(solution)/shard_map/ppermute | solution.py:478
  141.0 1.5 collective-permute-done.9.refs_1_
  142.5 11.3 %feed_first.1 = (bf16[176,1024]{1,0:T(8,128)(2,1)S(1)}, bf16[176,1024]{1,0:T(8,128)(2,1)S(1)}) custom-call(s32[2]{0:T(128)S(1)} %pad_add_fusion.me_ref.refs_0_, bf16[16,2048]{1,0:T(8,128)(2,1)S(1)} %collective-permute-done.9.refs_1_, bf16[176,2048]{1,0:T(8,128)(2,1)S(1)} %get-tuple-element.27.refs_2_, bf16[176,2048]{1,0:T(8,128)(2,1)S(1)} %collective-permute-done.5.refs_3_, ...), custom_call_target="tpu_custom_call" | custom-call | flops 3045064704 | bytes 18743296 | tf_op jit(solution)/shard_map/feed_first/pallas_call | solution.py:310
  153.8 0.1 collective-permute-start.10
  154.0 3.5 %collective-permute-start.11 = (bf16[176,1024]{1,0:T(8,128)(2,1)S(1)}, bf16[176,1024]{1,0:T(8,128)(2,1)S(1)}, u32[]{:S(2)}, u32[]{:S(2)}) collective-permute-start(bf16[176,1024]{1,0:T(8,128)(2,1)S(1)} %get-tuple-element.29), channel_id=1, source_target_pairs={{0,3},{1,0},{2,1},{3,2},{4,7},{5,4},{6,5},{7,6},{8,11},{9,8},{10,9... | collective-permute-start | bytes 1081352 | tf_op jit(solution)/shard_map/ppermute | solution.py:467
  157.5 16.7 %feed_rest.1.rest_ref = bf16[3,176,2048]{2,1,0:T(8,128)(2,1)S(1)} custom-call(s32[2]{0:T(128)S(1)} %pad_add_fusion.me_ref.refs_0_, bf16[16,2048]{1,0:T(8,128)(2,1)S(1)} %collective-permute-done.9.refs_1_, bf16[176,2048]{1,0:T(8,128)(2,1)S(1)} %get-tuple-element.27.refs_2_, bf16[176,2048]{1,0:T(8,128)(2,1)S(1)} %collective-permute-done.5.refs_3_, ...), custom_call_target="tpu_custom_call" | custom-call | flops 9135194112 | bytes 21626880 | tf_op jit(solution)/shard_map/feed_rest/pallas_call | solution.py:310
  174.2 0.0 copy-start.20
  174.2 0.0 collective-permute-done.11.high_ref
  174.3 0.2 join.3
  174.5 0.1 collective-permute-start.12
  174.6 2.6 %collective-permute-start.13 = (bf16[176,2048]{1,0:T(8,128)(2,1)S(1)}, bf16[176,2048]{1,0:T(8,128)(2,1)S(1)}, u32[]{:S(2)}, u32[]{:S(2)}) collective-permute-start(bf16[176,2048]{1,0:T(8,128)(2,1)S(1)} %get-tuple-element.31), channel_id=1, source_target_pairs={{0,3},{1,0},{2,1},{3,2},{4,7},{5,4},{6,5},{7,6},{8,11},{9,8},{10,9... | collective-permute-start | bytes 2162696 | tf_op jit(solution)/shard_map/ppermute | solution.py:467
  177.3 15.8 %collective-permute-done.12.left_ref = bf16[176,2048]{1,0:T(8,128)(2,1)S(1)} collective-permute-done((bf16[176,2048]{1,0:T(8,128)(2,1)S(1)}, bf16[176,2048]{1,0:T(8,128)(2,1)S(1)}, u32[]{:S(2)}, u32[]{:S(2)}) %collective-permute-start.12) | collective-permute-done | bytes 720928 | tf_op jit(solution)/shard_map/ppermute | solution.py:467
  193.1 0.0 collective-permute-done.13.right_ref
  193.1 2.4 %last.1 = bf16[176,2048]{1,0:T(8,128)(2,1)} custom-call(bf16[3,176,2048]{2,1,0:T(8,128)(2,1)S(1)} %feed_rest.1.rest_ref, bf16[176,2048]{1,0:T(8,128)(2,1)S(1)} %collective-permute-done.12.left_ref, bf16[176,2048]{1,0:T(8,128)(2,1)S(1)} %collective-permute-done.13.right_ref, bf16[176,2048]{1,0:T(8,128)(2,1)S(1)} %get-tuple-element.32.hidden_ref, ...), custom_call_target="tpu_custom_call" | custom-call | tf_op jit(solution)/shard_map/last/pallas_call | solution.py:430
  (32 shorter events, 0.1 us)
Async XLA Ops:
  6.5 136.0 %all-gather.2.cloned.1.call-start = ((), (), s32[]{:S(2)}) async-start(), calls=%async_computation.1 | async-start | bytes 17842176 | tf_op jit(solution)/shard_map/all_gather | solution.py:511
  6.6 0.9 copy-start.7
  7.5 0.9 copy-start.8
  8.4 0.9 copy-start.9
  9.3 63.2 %copy-start = (bf16[512,2048]{1,0:T(8,128)(2,1)S(1)}, bf16[512,2048]{1,0:T(8,128)(2,1)}, u32[]{:S(2)}) copy-start(bf16[512,2048]{1,0:T(8,128)(2,1)} %w_ref.3) | copy-start | bytes 6291460
  11.0 22.4 %collective-permute-start = (bf16[8,512]{1,0:T(8,128)(2,1)S(1)}, bf16[8,512]{1,0:T(8,128)(2,1)S(1)}, u32[]{:S(2)}, u32[]{:S(2)}) collective-permute-start(bf16[8,512]{1,0:T(8,128)(2,1)S(1)} %slice.24), channel_id=1, source_target_pairs={{0,4},{4,8},{8,12},{12,16},{16,20},{20,24},{24,28},{28,32},{32,36}... | collective-permute-start | bytes 24584 | tf_op jit(solution)/shard_map/ppermute | solution.py:478
  33.3 1.4 copy-start.5
  34.7 1.1 copy-start.6
  35.8 0.9 copy-start.13
  36.7 0.9 copy-start.14
  37.6 0.7 copy-start.21
  38.3 0.7 copy-start.22
  44.0 1.1 copy-start.1
  45.1 0.6 copy-start.10
  45.7 0.7 copy-start.15
  46.4 26.1 %all-to-all-start = ((f32[32,8,128]{2,1,0:T(8,128)}), f32[32,8,128]{2,1,0:T(8,128)}, u32[]{:S(2)}, u32[]{:S(2)}) async-start(f32[32,8,128]{2,1,0:T(8,128)} %copy-done.15), calls=%async_computation | async-start | bytes 262144 | tf_op jit(solution)/shard_map/all_to_all | solution.py:482
  72.5 1.4 copy-start.2
  73.9 1.1 copy-start.4
  75.0 0.8 copy-start.11
  75.8 4.8 %copy-start.12 = (f32[2,8,512]{2,1,0:T(8,128)S(1)}, f32[2,8,512]{2,1,0:T(8,128)}, u32[]{:S(2)}) copy-start(f32[2,8,512]{2,1,0:T(8,128)} %copy-done.10) | copy-start | bytes 98308
  77.4 10.9 %collective-permute-start.1 = (bf16[176,1024]{1,0:T(8,128)(2,1)S(1)}, bf16[176,1024]{1,0:T(8,128)(2,1)S(1)}, u32[]{:S(2)}, u32[]{:S(2)}) collective-permute-start(bf16[176,1024]{1,0:T(8,128)(2,1)S(1)} %get-tuple-element.23), channel_id=1, source_target_pairs={{0,1},{1,2},{2,3},{3,0},{4,5},{5,6},{6,7},{7,4},{8,9},{9,10},{10,1... | collective-permute-start | bytes 1081352 | tf_op jit(solution)/shard_map/ppermute | solution.py:467
  78.9 9.4 %collective-permute-start.2 = (bf16[176,1024]{1,0:T(8,128)(2,1)S(1)}, bf16[176,1024]{1,0:T(8,128)(2,1)S(1)}, u32[]{:S(2)}, u32[]{:S(2)}) collective-permute-start(bf16[176,1024]{1,0:T(8,128)(2,1)S(1)} %get-tuple-element.24), channel_id=1, source_target_pairs={{0,3},{1,0},{2,1},{3,2},{4,7},{5,4},{6,5},{7,6},{8,11},{9,8},{10,9... | collective-permute-start | bytes 1081352 | tf_op jit(solution)/shard_map/ppermute | solution.py:467
  80.6 25.5 %copy-start.18 = (f32[2048]{0:T(1024)S(1)}, f32[2048]{0:T(1024)}, u32[]{:S(2)}) copy-start(f32[2048]{0:T(1024)} %param.26) | copy-start | bytes 24580
  80.6 25.5 %copy-start.19 = (f32[2048]{0:T(1024)S(1)}, f32[2048]{0:T(1024)}, u32[]{:S(2)}) copy-start(f32[2048]{0:T(1024)} %param.27) | copy-start | bytes 24580
  83.1 23.0 %copy-start.3 = (bf16[704,2048]{1,0:T(8,128)(2,1)S(1)}, bf16[704,2048]{1,0:T(8,128)(2,1)}, u32[]{:S(2)}) copy-start(bf16[704,2048]{1,0:T(8,128)(2,1)} %res_ref.1) | copy-start | bytes 8650756
  88.5 17.6 %collective-permute-start.3 = (bf16[176,2048]{1,0:T(8,128)(2,1)S(1)}, bf16[176,2048]{1,0:T(8,128)(2,1)S(1)}, u32[]{:S(2)}, u32[]{:S(2)}) collective-permute-start(bf16[176,2048]{1,0:T(8,128)(2,1)S(1)} %get-tuple-element.25), channel_id=1, source_target_pairs={{0,1},{1,2},{2,3},{3,0},{4,5},{5,6},{6,7},{7,4},{8,9},{9,10},{10,1... | collective-permute-start | bytes 2162696 | tf_op jit(solution)/shard_map/ppermute | solution.py:467
  89.5 16.6 %collective-permute-start.4 = (bf16[176,2048]{1,0:T(8,128)(2,1)S(1)}, bf16[176,2048]{1,0:T(8,128)(2,1)S(1)}, u32[]{:S(2)}, u32[]{:S(2)}) collective-permute-start(bf16[176,2048]{1,0:T(8,128)(2,1)S(1)} %get-tuple-element.26), channel_id=1, source_target_pairs={{0,3},{1,0},{2,1},{3,2},{4,7},{5,4},{6,5},{7,6},{8,11},{9,8},{10,9... | collective-permute-start | bytes 2162696 | tf_op jit(solution)/shard_map/ppermute | solution.py:467
  106.1 36.4 %copy-start.16 = (bf16[3,1408]{1,0:T(4,128)(2,1)S(1)}, bf16[3,1408]{1,0:T(4,128)(2,1)}, u32[]{:S(2)}) copy-start(bf16[3,1408]{1,0:T(4,128)(2,1)} %refs_8_.3) | copy-start | bytes 25348
  106.1 36.4 %copy-start.17 = (bf16[3,1408]{1,0:T(4,128)(2,1)S(1)}, bf16[3,1408]{1,0:T(4,128)(2,1)}, u32[]{:S(2)}) copy-start(bf16[3,1408]{1,0:T(4,128)(2,1)} %refs_9_.3) | copy-start | bytes 25348
  109.7 16.8 %collective-permute-start.6 = (bf16[176,2048]{1,0:T(8,128)(2,1)S(1)}, bf16[176,2048]{1,0:T(8,128)(2,1)S(1)}, u32[]{:S(2)}, u32[]{:S(2)}) collective-permute-start(bf16[176,2048]{1,0:T(8,128)(2,1)S(1)} %get-tuple-element.27.refs_2_), channel_id=1, source_target_pairs={{0,1},{1,2},{2,3},{3,0},{4,5},{5,6},{6,7},{7,4},{8,9},{9,10},{10,1... | collective-permute-start | bytes 2162696 | tf_op jit(solution)/shard_map/ppermute | solution.py:467
  109.8 17.5 %collective-permute-start.5 = (bf16[176,2048]{1,0:T(8,128)(2,1)S(1)}, bf16[176,2048]{1,0:T(8,128)(2,1)S(1)}, u32[]{:S(2)}, u32[]{:S(2)}) collective-permute-start(bf16[176,2048]{1,0:T(8,128)(2,1)S(1)} %get-tuple-element.27.refs_2_), channel_id=1, source_target_pairs={{0,3},{1,0},{2,1},{3,2},{4,7},{5,4},{6,5},{7,6},{8,11},{9,8},{10,9... | collective-permute-start | bytes 2162696 | tf_op jit(solution)/shard_map/ppermute | solution.py:467
  127.3 8.5 %collective-permute-start.7 = (bf16[176,1024]{1,0:T(8,128)(2,1)}, bf16[176,1024]{1,0:T(8,128)(2,1)S(1)}, u32[]{:S(2)}, u32[]{:S(2)}) collective-permute-start(bf16[176,1024]{1,0:T(8,128)(2,1)} %slice.33), channel_id=1, source_target_pairs={{0,1},{1,2},{2,3},{3,0},{4,5},{5,6},{6,7},{7,4},{8,9},{9,10},{10,1... | collective-permute-start | bytes 1081352 | tf_op jit(solution)/shard_map/ppermute | solution.py:467
  128.1 7.7 %collective-permute-start.8 = (bf16[176,1024]{1,0:T(8,128)(2,1)}, bf16[176,1024]{1,0:T(8,128)(2,1)}, u32[]{:S(2)}, u32[]{:S(2)}) collective-permute-start(bf16[176,1024]{1,0:T(8,128)(2,1)} %slice.35), channel_id=1, source_target_pairs={{0,3},{1,0},{2,1},{3,2},{4,7},{5,4},{6,5},{7,6},{8,11},{9,8},{10,9... | collective-permute-start | bytes 1081352 | tf_op jit(solution)/shard_map/ppermute | solution.py:467
  136.6 6.0 %collective-permute-start.9 = (bf16[16,2048]{1,0:T(8,128)(2,1)S(1)}, bf16[16,2048]{1,0:T(8,128)(2,1)S(1)}, u32[]{:S(2)}, u32[]{:S(2)}) collective-permute-start(bf16[16,2048]{1,0:T(8,128)(2,1)S(1)} %fusion), channel_id=1, source_target_pairs={{0,4},{4,8},{8,12},{12,16},{16,20},{20,24},{24,28},{28,32},{32,36}... | collective-permute-start | bytes 196616 | tf_op jit(solution)/shard_map/ppermute | solution.py:478
  153.8 20.4 %collective-permute-start.10 = (bf16[176,1024]{1,0:T(8,128)(2,1)S(1)}, bf16[176,1024]{1,0:T(8,128)(2,1)S(1)}, u32[]{:S(2)}, u32[]{:S(2)}) collective-permute-start(bf16[176,1024]{1,0:T(8,128)(2,1)S(1)} %get-tuple-element.28), channel_id=1, source_target_pairs={{0,1},{1,2},{2,3},{3,0},{4,5},{5,6},{6,7},{7,4},{8,9},{9,10},{10,1... | collective-permute-start | bytes 1081352 | tf_op jit(solution)/shard_map/ppermute | solution.py:467
  154.0 20.3 %collective-permute-start.11 = (bf16[176,1024]{1,0:T(8,128)(2,1)S(1)}, bf16[176,1024]{1,0:T(8,128)(2,1)S(1)}, u32[]{:S(2)}, u32[]{:S(2)}) collective-permute-start(bf16[176,1024]{1,0:T(8,128)(2,1)S(1)} %get-tuple-element.29), channel_id=1, source_target_pairs={{0,3},{1,0},{2,1},{3,2},{4,7},{5,4},{6,5},{7,6},{8,11},{9,8},{10,9... | collective-permute-start | bytes 1081352 | tf_op jit(solution)/shard_map/ppermute | solution.py:467
  174.2 18.9 %copy-start.20 = (f32[2048]{0:T(1024)S(1)}, f32[2048]{0:T(1024)}, u32[]{:S(2)}) copy-start(f32[2048]{0:T(1024)} %param.28) | copy-start | bytes 24580
  174.5 18.6 %collective-permute-start.12 = (bf16[176,2048]{1,0:T(8,128)(2,1)S(1)}, bf16[176,2048]{1,0:T(8,128)(2,1)S(1)}, u32[]{:S(2)}, u32[]{:S(2)}) collective-permute-start(bf16[176,2048]{1,0:T(8,128)(2,1)S(1)} %get-tuple-element.30), channel_id=1, source_target_pairs={{0,1},{1,2},{2,3},{3,0},{4,5},{5,6},{6,7},{7,4},{8,9},{9,10},{10,1... | collective-permute-start | bytes 2162696 | tf_op jit(solution)/shard_map/ppermute | solution.py:467
  174.6 18.4 %collective-permute-start.13 = (bf16[176,2048]{1,0:T(8,128)(2,1)S(1)}, bf16[176,2048]{1,0:T(8,128)(2,1)S(1)}, u32[]{:S(2)}, u32[]{:S(2)}) collective-permute-start(bf16[176,2048]{1,0:T(8,128)(2,1)S(1)} %get-tuple-element.31), channel_id=1, source_target_pairs={{0,3},{1,0},{2,1},{3,2},{4,7},{5,4},{6,5},{7,6},{8,11},{9,8},{10,9... | collective-permute-start | bytes 2162696 | tf_op jit(solution)/shard_map/ppermute | solution.py:467
Sparse Core Ops, SparseCore 0:
  10.4 128.0 all-gather.1

commit v4 on v3

v4 whole, which is shorter than its diff:
```python
import functools

import jax
import jax.numpy as jnp
from jax import lax
from jax.experimental import pallas as pl
from jax.experimental.pallas import tpu as pltpu
from jax.sharding import PartitionSpec as P

EPS = 1e-06
GATE_SCALE = 8.0
SEGMENTS = 8
LANES = 128
BLOCKS = 4
HALO = 16
MIB = 1 << 20
GELU_A = 0.7978845608028654
GELU_B = 0.044715


def gelu(v):
    return 0.5 * v * (1.0 + jnp.tanh(GELU_A * (v + GELU_B * (v * v * v))))


def minus_expm1(y):
    series = 1.0 + y * (1.0 / 7.0)
    for n in (6.0, 5.0, 4.0, 3.0, 2.0):
        series = 1.0 + y * (1.0 / n) * series
    return jnp.where(y > -0.3, -y * series, 1.0 - jnp.exp(y))


def sigmoid(v):
    return 0.5 * jnp.tanh(0.5 * v) + 0.5


def scan_kernel(
    x_ref, edge_ref, taps_ref, rmap_ref, imap_ref, soft_ref, jump_ref,
    cum_ref, loc_ref, seg_ref, ends_ref,
    xs, decay, drive,
):
    group = pl.program_id(0)
    groups = pl.num_programs(0)
    length = x_ref.shape[0]
    taps = taps_ref.shape[0]
    xs[0:8, :] = edge_ref[...].astype(jnp.float32)
    xs[8 : 8 + length, :] = x_ref[...].astype(jnp.float32)
    rows = length // 4
    kernel = taps_ref[...].astype(jnp.float32)
    v = -soft_ref[...]
    soft = jnp.maximum(v, 0.0) + jnp.log1p(jnp.exp(-jnp.abs(v)))
    for at in range(0, length, rows):
        conv = jnp.zeros((rows, LANES), jnp.float32)
        for k in range(taps):
            first = 8 + at - (taps - 1) + k
            conv = conv + xs[first : first + rows, :] * kernel[k : k + 1, :]
        conv = conv.astype(jnp.bfloat16)
        rgate = sigmoid(jnp.dot(conv, rmap_ref[0], preferred_element_type=jnp.float32))
        igate = sigmoid(jnp.dot(conv, imap_ref[0], preferred_element_type=jnp.float32))
        log_decay = -GATE_SCALE * rgate * soft + jump_ref[at : at + rows, :]
        decay[at : at + rows, :] = jnp.exp(log_decay)
        drive[at : at + rows, :] = (
            jnp.sqrt(minus_expm1(2.0 * log_decay)) * igate * conv.astype(jnp.float32)
        )
    steps = length // SEGMENTS

    def step(i, carry):
        state, product = carry
        where = pl.ds(i, SEGMENTS, steps)
        a = decay[where, :]
        state = a * state + drive[where, :]
        product = a * product
        loc_ref[where, :] = state
        cum_ref[where, :] = product
        return state, product

    zero = jnp.zeros((SEGMENTS, LANES), jnp.float32)
    state, product = lax.fori_loop(0, steps, step, (zero, zero + 1.0), unroll=8)
    seg_ref[0, :, :] = product
    seg_ref[1, :, :] = state
    all_state = state[0:1]
    all_product = product[0:1]
    for s in range(1, SEGMENTS):
        all_state = product[s : s + 1] * all_state + state[s : s + 1]
        all_product = product[s : s + 1] * all_product
    count = ends_ref.shape[0]
    ends_ref[:, pl.ds(group, 1), :] = jnp.broadcast_to(all_product[None], (count, 1, LANES))
    ends_ref[:, pl.ds(groups + group, 1), :] = jnp.broadcast_to(all_state[None], (count, 1, LANES))


def local_scan(x, edge, taps, rmap, imap, soft, jump, copies):
    length, channels = x.shape
    groups = channels // LANES
    column = lambda rows: pl.BlockSpec((rows, LANES), lambda g: (0, g))
    square = pl.BlockSpec((1, LANES, LANES), lambda g: (g, 0, 0))
    return pl.pallas_call(
        scan_kernel,
        grid=(groups,),
        in_specs=[column(length), column(8), column(taps.shape[0]), square, square, column(1), column(length)],
        out_specs=[
            column(length),
            column(length),
            pl.BlockSpec((2, SEGMENTS, LANES), lambda g: (0, 0, g)),
            pl.BlockSpec((copies, 2 * groups, LANES), lambda g: (0, 0, 0)),
        ],
        out_shape=[
            jax.ShapeDtypeStruct((length, channels), jnp.float32),
            jax.ShapeDtypeStruct((length, channels), jnp.float32),
            jax.ShapeDtypeStruct((2, SEGMENTS, channels), jnp.float32),
            jax.ShapeDtypeStruct((copies, 2 * groups, LANES), jnp.float32),
        ],
        scratch_shapes=[
            pltpu.VMEM((length + 8, LANES), jnp.float32),
            pltpu.VMEM((length, LANES), jnp.float32),
            pltpu.VMEM((length, LANES), jnp.float32),
        ],
        name="local_scan",
    )(x, edge, taps, rmap, imap, soft, jump)


def branch_kernel(
    me_ref, arrived, seg, cum_hbm, loc_hbm, gate_hbm, w_ref, *rest, turns
):
    outs, (cum, loc, gates, carry, state, sems) = rest[:-6], rest[-6:]
    rows, channels = state.shape
    groups = channels // LANES
    per_block = SEGMENTS // BLOCKS
    seg_rows = rows // per_block
    starts = [lax.rem(me_ref[0] + steps, BLOCKS) for steps in turns]
    copies = []
    for b, block in enumerate(starts):
        at = pl.ds(pl.multiple_of(block * rows, rows), rows)
        for k, (source, target) in enumerate(((cum_hbm, cum), (loc_hbm, loc), (gate_hbm, gates))):
            copies.append(pltpu.make_async_copy(source.at[at, :], target.at[b], sems.at[3 * b + k]))
    for copy in copies:
        copy.start()

    def join(j, state):
        return arrived[j, 0:groups, :] * state + arrived[j, groups : 2 * groups, :]

    before = lax.fori_loop(0, me_ref[1], join, jnp.zeros((groups, LANES), jnp.float32))
    for g in range(groups):
        lanes = slice(g * LANES, (g + 1) * LANES)
        now = before[g : g + 1, :]
        for s in range(SEGMENTS):
            carry[s, 0:1, lanes] = now
            now = seg[0, s : s + 1, lanes] * now + seg[1, s : s + 1, lanes]
    for copy in copies:
        copy.wait()

    for b, block in enumerate(starts):
        for part in range(per_block):
            at = slice(part * seg_rows, (part + 1) * seg_rows)
            state[at, :] = loc[b, at, :] + cum[b, at, :] * carry[block * per_block + part, 0:1, :]
        out = (state[...] * gelu(gates[b].astype(jnp.float32))).astype(jnp.bfloat16)
        put(outs, b, jnp.dot(out, w_ref[...], preferred_element_type=jnp.float32))


def put(outs, block, share):
    share = share.astype(jnp.bfloat16)
    half = share.shape[1] // 2
    if block < 2:
        outs[2 * block][...] = share[:, :half]
        outs[2 * block + 1][...] = share[:, half:]
    else:
        outs[4][...] = share


VMEM = pl.BlockSpec(memory_space=pltpu.VMEM)
HERE = pl.BlockSpec(memory_space=pltpu.HBM)
OPPOSITE, OTHERS = (2,), (1, 3, 0)


def vm(value):
    return pltpu.with_memory_space_constraint(value, pltpu.VMEM)


def hbm(value):
    return pltpu.with_memory_space_constraint(value, pltpu.HBM)


def vm_out(shape):
    return pltpu.VMEM(shape, jnp.bfloat16)


def share_shapes(turns, rows, width):
    half = vm_out((rows, width // 2))
    return [half] * 2 if len(turns) == 1 else [half] * 4 + [vm_out((rows, width))]


def branch_shares(me, arrived, seg, cum, loc, gate, weight, turns):
    length, channels = cum.shape
    width = weight.shape[1]
    rows = length // BLOCKS
    count = len(turns)
    out_shape = share_shapes(turns, rows, width)
    return pl.pallas_call(
        functools.partial(branch_kernel, turns=turns),
        in_specs=[pl.BlockSpec(memory_space=pltpu.SMEM), VMEM, VMEM, *[HERE] * 3, VMEM],
        out_specs=[VMEM] * len(out_shape),
        out_shape=out_shape,
        scratch_shapes=[
            pltpu.VMEM((count, rows, channels), jnp.float32),
            pltpu.VMEM((count, rows, channels), jnp.float32),
            pltpu.VMEM((count, rows, channels), jnp.bfloat16),
            pltpu.VMEM((SEGMENTS, 1, channels), jnp.float32),
            pltpu.VMEM((rows, channels), jnp.float32),
            pltpu.SemaphoreType.DMA((3 * count,)),
        ],
        cost_estimate=pl.CostEstimate(
            flops=2 * count * rows * channels * width,
            bytes_accessed=count * rows * (10 * channels + 2 * width) + 2 * channels * width,
            transcendentals=count * rows * channels,
        ),
        compiler_params=pltpu.CompilerParams(vmem_limit_bytes=16 * MIB),
        name="branch_first" if count == 1 else "branch_rest",
    )(me, arrived, seg, hbm(cum), hbm(loc), hbm(gate), weight)


def feed_kernel(*refs, turns):
    first = len(turns) == 1
    me_ref, outside = refs[:2]
    halves = {0: refs[2:4], 1: refs[4:6], 2: refs[6:8], 3: refs[8:10]}
    if first:
        weights, gk_ref, vk_ref, *outs, ring, down, lhs, up_a, up_b, act, sems = refs[10:]
    else:
        ring, down, gk_ref, vk_ref, *outs, lhs, up_a, up_b, act = refs[10:]
    rows = halves[0][0].shape[0]
    tall = rows + HALO
    taps = gk_ref.shape[0]
    shards, chunks, shard_rows, _ = down.shape
    width = shards * shard_rows
    half = width // 2
    columns = (slice(0, half), slice(half, width))

    def get(chunk):
        return pltpu.make_async_copy(weights.at[:, pl.ds(2 * chunk, 2)], ring.at[chunk], sems.at[chunk])

    def fill(b, steps):
        at = b * tall
        for part, behind in zip(columns, halves[(steps - 1) % BLOCKS]):
            lhs[at : at + HALO, part] = behind[rows - HALO : rows, :]

        @pl.when(lax.rem(me_ref[0] + steps, BLOCKS) == 0)
        def _():
            lhs[at : at + HALO, :] = outside[...]

        for part, own in zip(columns, halves[steps]):
            lhs[at + HALO : at + tall, part] = own[...]

    def activate(chunk, up):
        lanes = pl.ds(pl.multiple_of(chunk * LANES, LANES), LANES)
        gate_taps = gk_ref[:, lanes].astype(jnp.float32)
        value_taps = vk_ref[:, lanes].astype(jnp.float32)
        for b in range(len(turns)):
            gate = jnp.zeros((rows, LANES), jnp.float32)
            value = jnp.zeros((rows, LANES), jnp.float32)
            for k in range(taps):
                at = b * tall + HALO - (taps - 1) + k
                gate = gate + up[at : at + rows, 0:LANES] * gate_taps[k : k + 1, :]
                value = value + up[at : at + rows, LANES : 2 * LANES] * value_taps[k : k + 1, :]
            act[b * rows : (b + 1) * rows, lanes] = (gelu(gate) * value).astype(jnp.bfloat16)

    def project(chunk, up):
        sides = [ring[chunk, :, side].reshape(width, LANES) for side in range(2)]
        up[...] = (
            jnp.dot(lhs[...], jnp.concatenate(sides, axis=1), preferred_element_type=jnp.float32)
            .astype(jnp.bfloat16)
            .astype(jnp.float32)
        )

    if first:
        get_down = pltpu.make_async_copy(weights.at[:, pl.ds(2 * chunks, chunks)], down, sems.at[chunks])
        for chunk in range(chunks):
            get(jnp.int32(chunk)).start()
        get_down.start()
    for b, steps in enumerate(turns):
        fill(b, steps)
    if first:
        get(jnp.int32(0)).wait()
    project(jnp.int32(0), up_a)

    def pair(i, carry):
        chunk = 2 * i
        if first:
            get(chunk + 1).wait()
            get(chunk + 2).wait()
        activate(chunk, up_a)
        project(chunk + 1, up_b)
        activate(chunk + 1, up_b)
        project(chunk + 2, up_a)
        return carry

    lax.fori_loop(0, chunks // 2, pair, 0)
    if first:
        get_down.wait()
    activate(jnp.int32(chunks - 1), up_a)
    turned = jnp.concatenate([down[:, c].reshape(width, LANES) for c in range(chunks)], axis=1)
    share = lax.dot_general(
        act[...], turned, (((1,), (1,)), ((), ())), preferred_element_type=jnp.float32
    )
    for b in range(len(turns)):
        put(outs, b, share[b * rows : (b + 1) * rows, :])


def feed(me, outside, halves, weights, gate_kernel, value_kernel, turns):
    first = len(turns) == 1
    count = len(turns)
    rows, half = halves[0].shape
    width, units = 2 * half, gate_kernel.shape[1]
    chunks = units // LANES
    assert chunks % 2 == 1
    tall = count * (rows + HALO)
    out_shape = share_shapes(turns, rows, width)
    scratch = [
        pltpu.VMEM((tall, width), jnp.bfloat16),
        pltpu.VMEM((tall, 2 * LANES), jnp.float32),
        pltpu.VMEM((tall, 2 * LANES), jnp.float32),
        pltpu.VMEM((count * rows, units), jnp.bfloat16),
    ]
    if first:
        shards, _, shard_rows, _ = weights[0].shape
        out_shape += [
            vm_out((chunks, shards, 2, shard_rows, LANES)),
            vm_out((shards, chunks, shard_rows, LANES)),
        ]
        scratch += [pltpu.SemaphoreType.DMA((chunks + 1,))]
    else:
        weights = map(vm, weights)
    return pl.pallas_call(
        functools.partial(feed_kernel, turns=turns),
        in_specs=[
            pl.BlockSpec(memory_space=pltpu.SMEM),
            *[VMEM] * (1 + len(halves)),
            *([HERE] if first else [VMEM] * 2),
            VMEM,
            VMEM,
        ],
        out_specs=[VMEM] * len(out_shape),
        out_shape=out_shape,
        scratch_shapes=scratch,
        cost_estimate=pl.CostEstimate(
            flops=6 * count * rows * width * units,
            bytes_accessed=6 * width * units + 4 * count * rows * width,
            transcendentals=count * rows * units,
        ),
        compiler_params=pltpu.CompilerParams(vmem_limit_bytes=12 * MIB),
        name="feed_first" if first else "feed_rest",
    )(me, vm(outside), *map(vm, halves), *weights, gate_kernel, value_kernel)


def pack_kernel(gate_ref, value_ref, turned_ref, out_ref):
    chunks = gate_ref.shape[1] // LANES
    for c in range(chunks):
        lanes = slice(c * LANES, (c + 1) * LANES)
        out_ref[2 * c] = gate_ref[:, lanes]
        out_ref[2 * c + 1] = value_ref[:, lanes]
        out_ref[2 * chunks + c] = turned_ref[:, lanes]


def packed(gate, value, turned):
    rows, units = gate.shape
    return pl.pallas_call(
        pack_kernel,
        out_shape=jax.ShapeDtypeStruct((3 * units // LANES, rows, LANES), jnp.bfloat16),
        name="pack",
    )(gate, value, turned)


def scaled(v, gain):
    return v * lax.rsqrt(jnp.mean(v * v, axis=-1, keepdims=True) + EPS) * gain


def shares_sum(refs, at):
    own, left_low, left_high, right_low, right_high = refs
    half = left_low.shape[1]
    parts = []
    for part, left, right in (
        (slice(0, half), left_low, right_low),
        (slice(half, 2 * half), left_high, right_high),
    ):
        total = own[at, part].astype(jnp.float32) + left[at, :].astype(jnp.float32)
        total = total + right[at, :].astype(jnp.float32)
        parts.append(total.astype(jnp.bfloat16).astype(jnp.float32))
    return jnp.concatenate(parts, axis=1)


def by_rows(rows, body):
    def step(i, carry):
        body(pl.ds(pl.multiple_of(i * HALO, HALO), HALO))
        return carry

    lax.fori_loop(0, rows // HALO, step, 0)


def mid_kernel(me_ref, *refs):
    shares, (res_hbm, mix_ref, inner_ref, hidden_ref, low_ref, high_ref, res, sem) = refs[:5], refs[5:]
    rows, half = low_ref.shape
    first = pl.multiple_of(me_ref[0] * rows, rows)
    fetch = pltpu.make_async_copy(res_hbm.at[pl.ds(first, rows), :], res, sem)
    fetch.start()
    mix, inner = mix_ref[...], inner_ref[...]
    fetch.wait()

    def body(at):
        hidden = (
            res[at, :].astype(jnp.float32) + scaled(shares_sum(shares, at), mix)
        ).astype(jnp.bfloat16)
        hidden_ref[at, :] = hidden
        normed = scaled(hidden.astype(jnp.float32), inner).astype(jnp.bfloat16)
        low_ref[at, :] = normed[:, :half]
        high_ref[at, :] = normed[:, half:]

    by_rows(rows, body)


def mid(me, shares, residual, mix_gain, inner_gain):
    rows, width = shares[0].shape
    return pl.pallas_call(
        mid_kernel,
        in_specs=[pl.BlockSpec(memory_space=pltpu.SMEM), *[VMEM] * 5, HERE, VMEM, VMEM],
        out_specs=[VMEM] * 3,
        out_shape=[
            jax.ShapeDtypeStruct((rows, width), jnp.bfloat16),
            *[vm_out((rows, width // 2))] * 2,
        ],
        scratch_shapes=[pltpu.VMEM((rows, width), jnp.bfloat16), pltpu.SemaphoreType.DMA],
        compiler_params=pltpu.CompilerParams(vmem_limit_bytes=12 * MIB),
        name="mid",
    )(me, *map(vm, shares), hbm(residual), mix_gain, inner_gain)


def last_kernel(*refs):
    shares, (hidden_ref, gain_ref, out_ref) = refs[:5], refs[5:]
    gain = gain_ref[...]

    def body(at):
        out_ref[at, :] = (
            hidden_ref[at, :].astype(jnp.float32) + scaled(shares_sum(shares, at), gain)
        ).astype(jnp.bfloat16)

    by_rows(hidden_ref.shape[0], body)


def last(shares, hidden, gain):
    return pl.pallas_call(
        last_kernel,
        in_specs=[VMEM] * 7,
        out_specs=VMEM,
        out_shape=jax.ShapeDtypeStruct(hidden.shape, jnp.bfloat16),
        compiler_params=pltpu.CompilerParams(vmem_limit_bytes=12 * MIB),
        name="last",
    )(*map(vm, shares), hidden, gain)


def join_kernel(right_low, low_ref, left_high, high_ref, right_ref, left_ref):
    def body(at):
        for own, other, out in ((right_low, low_ref, right_ref), (left_high, high_ref, left_ref)):
            total = own[at, :].astype(jnp.float32) + other[at, :].astype(jnp.float32)
            out[at, :] = total.astype(jnp.bfloat16)

    by_rows(low_ref.shape[0], body)


def join(right_low, low, left_high, high):
    return pl.pallas_call(
        join_kernel,
        in_specs=[VMEM] * 4,
        out_specs=[VMEM] * 2,
        out_shape=[vm_out(low.shape)] * 2,
        compiler_params=pltpu.CompilerParams(vmem_limit_bytes=12 * MIB),
        name="join",
    )(*map(vm, (right_low, low, left_high, high)))


def turn(value, axis, steps):
    count = lax.axis_size(axis)
    return lax.ppermute(value, axis, [(i, (i + steps) % count) for i in range(count)])


def ring_sum(first, rest):
    low, high = turn(first[0], "tp", 1), turn(first[1], "tp", -1)
    right_low, right_high, left_low, left_high, own = rest
    from_left_high, from_right_low = turn(right_high, "tp", 1), turn(left_low, "tp", -1)
    right_low, left_high = join(right_low, low, left_high, high)
    from_left_low, from_right_high = turn(right_low, "tp", 1), turn(left_high, "tp", -1)
    return own, from_left_low, from_left_high, from_right_low, from_right_high


def from_behind(value, axis):
    count = lax.axis_size(axis)
    return lax.ppermute(value, axis, [(i, i + 1) for i in range(count - 1)])


def exchanged(tiles, axis):
    return lax.all_to_all(tiles, axis, split_axis=0, concat_axis=0, tiled=True)


def local(
    residual,
    mix_input,
    gate_input,
    mix_kernel,
    recur_gate_map,
    input_gate_map,
    decay_param,
    jump_log,
    out_weight,
    mix_gain,
    inner_gain,
    final_gain,
    gate_weight,
    value_weight,
    gate_kernel,
    value_kernel,
    down_weight,
):
    n_tp, n_sp = lax.axis_size("tp"), lax.axis_size("sp")
    assert n_tp == BLOCKS
    tp_me = lax.axis_index("tp").astype(jnp.int32)
    me = jnp.stack([tp_me, lax.axis_index("sp").astype(jnp.int32)])

    edge = from_behind(mix_input[mix_input.shape[0] - 8 :], "sp")
    shard = packed(gate_weight, value_weight, down_weight.T)
    weights = lax.all_gather(shard, "sp", axis=0, tiled=True).reshape(n_sp, *shard.shape)

    cum, loc, seg, ends = local_scan(
        mix_input, edge, mix_kernel, recur_gate_map, input_gate_map, decay_param[None], jump_log, n_sp
    )
    arrived = exchanged(ends, "sp")
    shares = functools.partial(
        branch_shares, arrived=arrived, seg=seg, cum=cum, loc=loc, gate=gate_input, weight=out_weight
    )
    first = shares(me, turns=OPPOSITE)
    rest = shares(me, turns=OTHERS)
    hidden_state, own_low, own_high = mid(
        me, ring_sum(first, rest), residual, mix_gain[None], inner_gain[None]
    )
    left_low, right_high = turn(own_low, "tp", 1), turn(own_high, "tp", -1)
    left_high, right_low = turn(own_high, "tp", 1), turn(own_low, "tp", -1)
    opposite_low, opposite_high = turn(left_low, "tp", 1), turn(right_high, "tp", -1)

    tail = lambda low, high: jnp.concatenate([low[-HALO:], high[-HALO:]], axis=1)
    own_tail = tail(own_low, own_high)
    final_tail = jnp.where(
        tp_me == n_tp - 1,
        own_tail,
        jnp.where(tp_me == 0, tail(left_low, left_high), tail(right_low, right_high)),
    )
    places = range(n_sp - 1)
    outside = jnp.where(
        tp_me == 1,
        lax.ppermute(own_tail, ("sp", "tp"), [(s * n_tp + n_tp - 1, (s + 1) * n_tp + 1) for s in places]),
        lax.ppermute(
            final_tail,
            ("sp", "tp"),
            [(s * n_tp + t, (s + 1) * n_tp + t) for s in places for t in (0, 2, 3)],
        ),
    )
    halves = (own_low, own_high, right_low, right_high, opposite_low, opposite_high, left_low, left_high)
    *first, ring, down = feed(
        me, outside, halves, (hbm(weights),), gate_kernel, value_kernel, turns=OPPOSITE
    )
    rest = feed(me, outside, halves, (ring, down), gate_kernel, value_kernel, turns=OTHERS)
    return last(ring_sum(first, rest), hidden_state, final_gain[None])


def solution(mesh):
    return jax.shard_map(
        local,
        mesh=mesh,
        in_specs=(
            P(("grp", "sp"), None),
            P(("grp", "sp"), "tp"),
            P(("grp", "sp"), "tp"),
            P(None, "tp"),
            P("tp", None, None),
            P("tp", None, None),
            P("tp"),
            P(("grp", "sp"), "tp"),
            P("tp", None),
            P(),
            P(),
            P(),
            P("sp", "tp"),
            P("sp", "tp"),
            P(None, "tp"),
            P(None, "tp"),
            P("tp", "sp"),
        ),
        out_specs=P(("grp", "sp", "tp"), None),
        check_vma=False,
    )
```

time: 204 us -> 193 us (0.946)
  local copies, waits for them, and re-layouts: 17.1 us -> 3.83 us
  starting transfers between devices: 36.1 us -> 43.3 us
  waiting for transfers between devices: 91 us -> 85.3 us
    unnamed x46 -> x20, local copies, waits for them, and re-layouts: 14.1 us -> 3.11 us
    ppermute x12 -> x18, starting transfers between devices: 17.8 us -> 25.3 us  [turn(): lax.ppermute(value, axis, [(i, (i + steps) % count) for i in range(count)])]
    ppermute x12 -> x18, waiting for transfers between devices: 54.9 us -> 49 us  [turn(): lax.ppermute(value, axis, [(i, (i + steps) % count) for i in range(count)])]
    ppermute x2 -> x1, starting transfers between devices: 10.2 us -> 5.73 us  [from_behind(): return lax.ppermute(value, axis, [(i, i + 1) for i in range(count - 1)])]
    ppermute x0 -> x2, starting transfers between devices: none -> 4.01 us  [the longest x1 3.35 us: local(): lax.ppermute(final_tail, ('sp', 'tp'), [(s * n_tp + t, (s + 1) * n_tp + t...]
    pallas_call x7, Pallas kernels: 34.9 us -> 32.5 us  [the longest x2 23.5 us: feed(): pl.pallas_call(functools.partial(feed_kernel, turns=turns), in_specs=[pl....]
    ppermute x2 -> x1, waiting for transfers between devices: 18.1 us -> 16.6 us  [from_behind(): return lax.ppermute(value, axis, [(i, i + 1) for i in range(count - 1)])]
  transfers between devices with their start and end apart: 16 -> 23, of which waited for: 8 -> 13; matrix products, arithmetic and copies ran while one was open for 2% -> 0% of each run, Pallas kernels for 15% -> 17%
where the time goes in v4:
time: 193 us; the launch traced here: 192 us
  waiting for transfers between devices  85.3 us (44%)
  Pallas kernels  45.9 us (24%)
  starting transfers between devices  43.3 us (22%)
  between operations  13.6 us (7%)
  local copies, waits for them, and re-layouts  3.83 us (2%)
    ppermute x18, waiting for transfers between devices, turn(): lax.ppermute(value, axis, [(i, (i + steps) % count) for i in range(count)])  49 us
    ppermute x18, starting transfers between devices, turn(): lax.ppermute(value, axis, [(i, (i + steps) % count) for i in range(count)])  25.3 us
    pallas_call x2, Pallas kernels, feed(): pl.pallas_call(functools.partial(feed_kernel, turns=turns), in_specs=[pl....  23.5 us
    all_to_all x1, waiting for transfers between devices, exchanged(): return lax.all_to_all(tiles, axis, split_axis=0, concat_axis=0, tiled=True)  17.8 us
    ppermute x1, waiting for transfers between devices, from_behind(): return lax.ppermute(value, axis, [(i, i + 1) for i in range(count - 1)])  16.6 us
    all_to_all x1, starting transfers between devices, exchanged(): return lax.all_to_all(tiles, axis, split_axis=0, concat_axis=0, tiled=True)  8.28 us
    pallas_call x1, Pallas kernels, local_scan(): pl.pallas_call(scan_kernel, grid=(groups,), in_specs=[column(length), col...  6.83 us
    pallas_call x2, Pallas kernels, branch_shares(): pl.pallas_call(functools.partial(branch_kernel, turns=turns), in_specs=[p...  6.25 us
  transfers between devices with their start and end apart: 23, of which 13 were waited for; matrix products, arithmetic and copies ran while one was open for 0% of the time, Pallas kernels for 17%

profile of v4, /device:TPU:33, one launch (start us, length us, event | category | flops | bytes accessed | tf_op | source)
XLA Modules:
  0.0 192.1 jit_solution(13519038848347921312)
XLA Ops:
  6.6 2.1 %pack.1 = bf16[33,64,128]{2,1,0:T(8,128)(2,1)} custom-call(bf16[64,1408]{1,0:T(8,128)(2,1)} %gate_ref.1, bf16[64,1408]{1,0:T(8,128)(2,1)} %value_ref.1, bf16[64,1408]{1,0:T(8,128)(2,1)} %bitcast.12), custom_call_target="tpu_custom_call" | custom-call | tf_op jit(solution)/shard_map/pack/pallas_call | solution.py:362
  8.7 0.1 all-gather.2.cloned.1.call-update
  8.7 0.7 slice.21
  9.4 5.7 %collective-permute-start = (bf16[8,512]{1,0:T(8,128)(2,1)S(1)}, bf16[8,512]{1,0:T(8,128)(2,1)S(1)}, u32[]{:S(2)}, u32[]{:S(2)}) collective-permute-start(bf16[8,512]{1,0:T(8,128)(2,1)S(1)} %slice.21), channel_id=1, source_target_pairs={{0,4},{4,8},{8,12},{12,16},{16,20},{20,24},{24,28},{28,32},{32,36}... | collective-permute-start | bytes 24584 | tf_op jit(solution)/shard_map/ppermute | solution.py:491
  15.2 16.6 %collective-permute-done.edge_ref = bf16[8,512]{1,0:T(8,128)(2,1)S(1)} collective-permute-done((bf16[8,512]{1,0:T(8,128)(2,1)S(1)}, bf16[8,512]{1,0:T(8,128)(2,1)S(1)}, u32[]{:S(2)}, u32[]{:S(2)}) %collective-permute-start) | collective-permute-done | bytes 8224 | tf_op jit(solution)/shard_map/ppermute | solution.py:491
  31.8 0.6 copy-done.9
  32.4 6.8 %local_scan.1 = (f32[704,512]{1,0:T(8,128)}, f32[704,512]{1,0:T(8,128)}, f32[2,8,512]{2,1,0:T(8,128)}, f32[32,8,128]{2,1,0:T(8,128)}) custom-call(bf16[704,512]{1,0:T(8,128)(2,1)} %x_ref.1, bf16[8,512]{1,0:T(8,128)(2,1)} %copy-done.9, bf16[4,512]{1,0:T(4,128)(2,1)} %taps_ref.1, bf16[4,128,128]{2,1,0:T(8,128)(2,1)} %rmap_ref.1, ...), custom_call_target="tpu_custom_call" | custom-call | tf_op jit(solution)/shard_map/local_scan/pallas_call | solution.py:95
  39.2 8.3 %all-to-all-start = ((f32[32,8,128]{2,1,0:T(8,128)}), f32[32,8,128]{2,1,0:T(8,128)S(1)}, u32[]{:S(2)}, u32[]{:S(2)}) async-start(f32[32,8,128]{2,1,0:T(8,128)} %get-tuple-element.32), calls=%async_computation | async-start | bytes 262144 | tf_op jit(solution)/shard_map/all_to_all | solution.py:495
  47.5 0.1 pad_add_fusion.me_ref.refs_0_
  47.6 17.8 %all-to-all-done.arrived = f32[32,8,128]{2,1,0:T(8,128)S(1)} async-done(((f32[32,8,128]{2,1,0:T(8,128)}), f32[32,8,128]{2,1,0:T(8,128)S(1)}, u32[]{:S(2)}, u32[]{:S(2)}) %all-to-all-start) | async-done | bytes 131104 | tf_op jit(solution)/shard_map/all_to_all | solution.py:495
  65.4 0.8 copy-done.3
  66.2 2.4 %branch_first.1 = (bf16[176,1024]{1,0:T(8,128)(2,1)S(1)}, bf16[176,1024]{1,0:T(8,128)(2,1)S(1)}) custom-call(s32[2]{0:T(128)S(1)} %pad_add_fusion.me_ref.refs_0_, f32[32,8,128]{2,1,0:T(8,128)S(1)} %all-to-all-done.arrived, f32[2,8,512]{2,1,0:T(8,128)S(1)} %copy-done.3, f32[704,512]{1,0:T(8,128)} %get-tuple-element.34.cum_hbm, ...), custom_call_target="tpu_custom_call" | custom-call | flops 369098752 | bytes 3719168 | tf_op jit(solution)/shard_map/branch_first/pallas_call | solution.py:196
  68.5 1.5 collective-permute-start.1
  70.0 1.6 collective-permute-start.2
  71.6 3.9 %branch_rest.1 = (bf16[176,1024]{1,0:T(8,128)(2,1)S(1)}, bf16[176,1024]{1,0:T(8,128)(2,1)S(1)}, bf16[176,1024]{1,0:T(8,128)(2,1)S(1)}, bf16[176,1024]{1,0:T(8,128)(2,1)S(1)}, bf16[176,2048]{1,0:T(8,128)(2,1)S(1)}) custom-call(s32[2]{0:T(128)S(1)} %pad_add_fusion.me_ref.refs_0_, f32[32,8,128]{2,1,0:T(8,128)S(1)} %all-to-all-done.arrived, ...), custom_call_target="tpu_custom_call" | custom-call | flops 1107296256 | bytes 6963200 | tf_op jit(solution)/shard_map/branch_rest/pallas_call | solution.py:196
  75.5 0.1 collective-permute-start.4
  75.6 2.6 %collective-permute-start.5 = (bf16[176,1024]{1,0:T(8,128)(2,1)S(1)}, bf16[176,1024]{1,0:T(8,128)(2,1)S(1)}, u32[]{:S(2)}, u32[]{:S(2)}) collective-permute-start(bf16[176,1024]{1,0:T(8,128)(2,1)S(1)} %get-tuple-element.43), channel_id=1, source_target_pairs={{0,3},{1,0},{2,1},{3,2},{4,7},{5,4},{6,5},{7,6},{8,11},{9,8},{10,9... | collective-permute-start | bytes 1081352 | tf_op jit(solution)/shard_map/ppermute | solution.py:477
  78.3 0.9 collective-permute-done.1.low_ref
  79.2 0.0 collective-permute-done.2.high_ref
  79.2 0.2 join.2
  79.4 1.0 collective-permute-start.3
  80.4 1.9 collective-permute-start.6
  82.3 5.0 %collective-permute-done.4.refs_2_ = bf16[176,1024]{1,0:T(8,128)(2,1)S(1)} collective-permute-done((bf16[176,1024]{1,0:T(8,128)(2,1)S(1)}, bf16[176,1024]{1,0:T(8,128)(2,1)S(1)}, u32[]{:S(2)}, u32[]{:S(2)}) %collective-permute-start.4) | collective-permute-done | bytes 360480 | tf_op jit(solution)/shard_map/ppermute | solution.py:477
  87.3 0.0 collective-permute-done.5.refs_3_
  87.3 7.7 %collective-permute-done.3.refs_1_ = bf16[176,1024]{1,0:T(8,128)(2,1)S(1)} collective-permute-done((bf16[176,1024]{1,0:T(8,128)(2,1)S(1)}, bf16[176,1024]{1,0:T(8,128)(2,1)S(1)}, u32[]{:S(2)}, u32[]{:S(2)}) %collective-permute-start.3) | collective-permute-done | bytes 360480 | tf_op jit(solution)/shard_map/ppermute | solution.py:477
  95.1 0.0 collective-permute-done.6.refs_4_
  95.1 0.0 copy-start.4
  95.1 0.0 copy-start.5
  95.1 4.4 %mid.1 = (bf16[176,2048]{1,0:T(8,128)(2,1)S(1)}, bf16[176,1024]{1,0:T(8,128)(2,1)S(1)}, bf16[176,1024]{1,0:T(8,128)(2,1)S(1)}) custom-call(s32[2]{0:T(128)S(1)} %pad_add_fusion.me_ref.refs_0_, bf16[176,2048]{1,0:T(8,128)(2,1)S(1)} %get-tuple-element.36.refs_0_, bf16[176,1024]{1,0:T(8,128)(2,1)S(1)} %collective-permute-done.3.refs_1_, ...), custom_call_target="tpu_custom_call" | custom-call | tf_op jit(solution)/shard_map/mid/pallas_call | solution.py:418
  99.5 2.8 %collective-permute-start.10 = (bf16[176,1024]{1,0:T(8,128)(2,1)S(1)}, bf16[176,1024]{1,0:T(8,128)(2,1)S(1)}, u32[]{:S(2)}, u32[]{:S(2)}) collective-permute-start(bf16[176,1024]{1,0:T(8,128)(2,1)S(1)} %get-tuple-element.45.refs_2_), channel_id=1, source_target_pairs={{0,3},{1,0},{2,1},{3,2},{4,7},{5,4},{6,5},{7,6},{8,11},{9,8},{10,9... | collective-permute-start | bytes 1081352 | tf_op jit(solution)/shard_map/ppermute | solution.py:477
  102.2 0.0 collective-permute-start.8
  102.2 2.7 %collective-permute-start.11 = (bf16[176,1024]{1,0:T(8,128)(2,1)S(1)}, bf16[176,1024]{1,0:T(8,128)(2,1)S(1)}, u32[]{:S(2)}, u32[]{:S(2)}) collective-permute-start(bf16[176,1024]{1,0:T(8,128)(2,1)S(1)} %get-tuple-element.46.refs_3_), channel_id=1, source_target_pairs={{0,3},{1,0},{2,1},{3,2},{4,7},{5,4},{6,5},{7,6},{8,11},{9,8},{10,9... | collective-permute-start | bytes 1081352 | tf_op jit(solution)/shard_map/ppermute | solution.py:477
  104.9 0.0 collective-permute-start.9
  104.9 3.8 %collective-permute-done.10.refs_4_ = bf16[176,1024]{1,0:T(8,128)(2,1)S(1)} collective-permute-done((bf16[176,1024]{1,0:T(8,128)(2,1)S(1)}, bf16[176,1024]{1,0:T(8,128)(2,1)S(1)}, u32[]{:S(2)}, u32[]{:S(2)}) %collective-permute-start.10) | collective-permute-done | bytes 360480 | tf_op jit(solution)/shard_map/ppermute | solution.py:477
  108.7 3.2 %collective-permute-done.8.refs_8_ = bf16[176,1024]{1,0:T(8,128)(2,1)S(1)} collective-permute-done((bf16[176,1024]{1,0:T(8,128)(2,1)S(1)}, bf16[176,1024]{1,0:T(8,128)(2,1)S(1)}, u32[]{:S(2)}, u32[]{:S(2)}) %collective-permute-start.8) | collective-permute-done | bytes 360480 | tf_op jit(solution)/shard_map/ppermute | solution.py:477
  111.9 4.5 %collective-permute-done.11.refs_5_ = bf16[176,1024]{1,0:T(8,128)(2,1)S(1)} collective-permute-done((bf16[176,1024]{1,0:T(8,128)(2,1)S(1)}, bf16[176,1024]{1,0:T(8,128)(2,1)S(1)}, u32[]{:S(2)}, u32[]{:S(2)}) %collective-permute-start.11) | collective-permute-done | bytes 360480 | tf_op jit(solution)/shard_map/ppermute | solution.py:477
  116.4 3.2 %collective-permute-done.9.refs_9_ = bf16[176,1024]{1,0:T(8,128)(2,1)S(1)} collective-permute-done((bf16[176,1024]{1,0:T(8,128)(2,1)S(1)}, bf16[176,1024]{1,0:T(8,128)(2,1)S(1)}, u32[]{:S(2)}, u32[]{:S(2)}) %collective-permute-start.9) | collective-permute-done | bytes 360480 | tf_op jit(solution)/shard_map/ppermute | solution.py:477
  119.7 3.3 %collective-permute-start.12 = (bf16[16,2048]{1,0:T(8,128)(2,1)S(1)}, bf16[16,2048]{1,0:T(8,128)(2,1)S(1)}, u32[]{:S(2)}, u32[]{:S(2)}) collective-permute-start(bf16[16,2048]{1,0:T(8,128)(2,1)S(1)} %get-tuple-element.59), channel_id=1, source_target_pairs={{0,4},{2,6},{3,7},{4,8},{6,10},{7,11},{8,12},{10,14},{11,15},{12,1... | collective-permute-start | bytes 196616 | tf_op jit(solution)/shard_map/ppermute | solution.py:553
  123.0 0.7 collective-permute-start.7
  123.7 0.1 collective-permute-start.13
  123.8 2.6 %collective-permute-start.14 = (bf16[176,1024]{1,0:T(8,128)(2,1)S(1)}, bf16[176,1024]{1,0:T(8,128)(2,1)S(1)}, u32[]{:S(2)}, u32[]{:S(2)}) collective-permute-start(bf16[176,1024]{1,0:T(8,128)(2,1)S(1)} %collective-permute-done.11.refs_5_), channel_id=1, source_target_pairs={{0,3},{1,0},{2,1},{3,2},{4,7},{5,4},{6,5},{7,6},{8,11},{9,8},{10,9... | collective-permute-start | bytes 1081352 | tf_op jit(solution)/shard_map/ppermute | solution.py:477
  126.5 0.0 collective-permute-done.12
  126.5 0.0 collective-permute-done.7
  126.5 8.3 %collective-permute-done.13.refs_6_ = bf16[176,1024]{1,0:T(8,128)(2,1)S(1)} collective-permute-done((bf16[176,1024]{1,0:T(8,128)(2,1)S(1)}, bf16[176,1024]{1,0:T(8,128)(2,1)S(1)}, u32[]{:S(2)}, u32[]{:S(2)}) %collective-permute-start.13) | collective-permute-done | bytes 360480 | tf_op jit(solution)/shard_map/ppermute | solution.py:477
  134.8 0.0 collective-permute-done.14.refs_7_
  134.8 0.7 copy-done.1
  135.5 1.8 all-gather.2.cloned.1.call-done
  137.3 1.0 copy-done.2
  138.3 8.8 %feed_first.1 = (bf16[176,1024]{1,0:T(8,128)(2,1)S(1)}, bf16[176,1024]{1,0:T(8,128)(2,1)S(1)}, bf16[11,32,2,64,128]{4,3,2,1,0:T(8,128)(2,1)S(1)}, bf16[32,11,64,128]{3,2,1,0:T(8,128)(2,1)S(1)}) custom-call(s32[2]{0:T(128)S(1)} %pad_add_fusion.me_ref.refs_0_, bf16[16,2048]{1,0:T(8,128)(2,1)S(1)} %broadcast_select_fusion.refs_1_, ...), custom_call_target="tpu_custom_call" | custom-call | flops 3045064704 | bytes 18743296 | tf_op jit(solution)/shard_map/feed_first/pallas_call | solution.py:329
  147.1 1.3 collective-permute-start.15
  148.4 1.5 collective-permute-start.16
  149.9 14.7 %feed_rest.1 = (bf16[176,1024]{1,0:T(8,128)(2,1)S(1)}, bf16[176,1024]{1,0:T(8,128)(2,1)S(1)}, bf16[176,1024]{1,0:T(8,128)(2,1)S(1)}, bf16[176,1024]{1,0:T(8,128)(2,1)S(1)}, bf16[176,2048]{1,0:T(8,128)(2,1)S(1)}) custom-call(s32[2]{0:T(128)S(1)} %pad_add_fusion.me_ref.refs_0_, bf16[16,2048]{1,0:T(8,128)(2,1)S(1)} %broadcast_select_fusion.refs_1_, ...), custom_call_target="tpu_custom_call" | custom-call | flops 9135194112 | bytes 21626880 | tf_op jit(solution)/shard_map/feed_rest/pallas_call | solution.py:329
  164.6 0.1 collective-permute-start.18
  164.7 2.6 %collective-permute-start.19 = (bf16[176,1024]{1,0:T(8,128)(2,1)S(1)}, bf16[176,1024]{1,0:T(8,128)(2,1)S(1)}, u32[]{:S(2)}, u32[]{:S(2)}) collective-permute-start(bf16[176,1024]{1,0:T(8,128)(2,1)S(1)} %get-tuple-element.56), channel_id=1, source_target_pairs={{0,3},{1,0},{2,1},{3,2},{4,7},{5,4},{6,5},{7,6},{8,11},{9,8},{10,9... | collective-permute-start | bytes 1081352 | tf_op jit(solution)/shard_map/ppermute | solution.py:477
  167.4 0.0 collective-permute-done.15.low_ref
  167.4 0.0 collective-permute-done.16.high_ref
  167.4 0.2 join.3
  167.6 0.1 collective-permute-start.17
  167.8 2.6 %collective-permute-start.20 = (bf16[176,1024]{1,0:T(8,128)(2,1)S(1)}, bf16[176,1024]{1,0:T(8,128)(2,1)S(1)}, u32[]{:S(2)}, u32[]{:S(2)}) collective-permute-start(bf16[176,1024]{1,0:T(8,128)(2,1)S(1)} %get-tuple-element.57), channel_id=1, source_target_pairs={{0,3},{1,0},{2,1},{3,2},{4,7},{5,4},{6,5},{7,6},{8,11},{9,8},{10,9... | collective-permute-start | bytes 1081352 | tf_op jit(solution)/shard_map/ppermute | solution.py:477
  170.4 4.7 %collective-permute-done.18.refs_2_ = bf16[176,1024]{1,0:T(8,128)(2,1)S(1)} collective-permute-done((bf16[176,1024]{1,0:T(8,128)(2,1)S(1)}, bf16[176,1024]{1,0:T(8,128)(2,1)S(1)}, u32[]{:S(2)}, u32[]{:S(2)}) %collective-permute-start.18) | collective-permute-done | bytes 360480 | tf_op jit(solution)/shard_map/ppermute | solution.py:477
  175.1 0.0 collective-permute-done.19.refs_3_
  175.1 7.7 %collective-permute-done.17.refs_1_ = bf16[176,1024]{1,0:T(8,128)(2,1)S(1)} collective-permute-done((bf16[176,1024]{1,0:T(8,128)(2,1)S(1)}, bf16[176,1024]{1,0:T(8,128)(2,1)S(1)}, u32[]{:S(2)}, u32[]{:S(2)}) %collective-permute-start.17) | collective-permute-done | bytes 360480 | tf_op jit(solution)/shard_map/ppermute | solution.py:477
  182.8 0.0 collective-permute-done.20.refs_4_
  182.8 2.4 %last.1 = bf16[176,2048]{1,0:T(8,128)(2,1)} custom-call(bf16[176,2048]{1,0:T(8,128)(2,1)S(1)} %get-tuple-element.49.refs_0_, bf16[176,1024]{1,0:T(8,128)(2,1)S(1)} %collective-permute-done.17.refs_1_, bf16[176,1024]{1,0:T(8,128)(2,1)S(1)} %collective-permute-done.18.refs_2_, bf16[176,1024]{1,0:T(8,128)(2,1)S(1)} %collective-permute-done.19.refs_3_, ...), custom_call_target="tpu_custom_call" | custom-call | tf_op jit(solution)/shard_map/last/pallas_call | solution.py:445
  (23 shorter events, 0.1 us)
Async XLA Ops:
  6.5 58.9 %copy-start = (bf16[512,2048]{1,0:T(8,128)(2,1)S(1)}, bf16[512,2048]{1,0:T(8,128)(2,1)}, u32[]{:S(2)}) copy-start(bf16[512,2048]{1,0:T(8,128)(2,1)} %w_ref.3) | copy-start | bytes 6291460
  6.5 130.8 %all-gather.2.cloned.1.call-start = ((), (), s32[]{:S(2)}) async-start(), calls=%async_computation.1 | async-start | bytes 17842176 | tf_op jit(solution)/shard_map/all_gather | solution.py:524
  9.4 22.4 %collective-permute-start = (bf16[8,512]{1,0:T(8,128)(2,1)S(1)}, bf16[8,512]{1,0:T(8,128)(2,1)S(1)}, u32[]{:S(2)}, u32[]{:S(2)}) collective-permute-start(bf16[8,512]{1,0:T(8,128)(2,1)S(1)} %slice.21), channel_id=1, source_target_pairs={{0,4},{4,8},{8,12},{12,16},{16,20},{20,24},{24,28},{28,32},{32,36}... | collective-permute-start | bytes 24584 | tf_op jit(solution)/shard_map/ppermute | solution.py:491
  31.8 0.6 copy-start.9
  39.2 26.2 %all-to-all-start = ((f32[32,8,128]{2,1,0:T(8,128)}), f32[32,8,128]{2,1,0:T(8,128)S(1)}, u32[]{:S(2)}, u32[]{:S(2)}) async-start(f32[32,8,128]{2,1,0:T(8,128)} %get-tuple-element.32), calls=%async_computation | async-start | bytes 262144 | tf_op jit(solution)/shard_map/all_to_all | solution.py:495
  65.4 0.8 copy-start.3
  68.5 10.6 %collective-permute-start.1 = (bf16[176,1024]{1,0:T(8,128)(2,1)S(1)}, bf16[176,1024]{1,0:T(8,128)(2,1)S(1)}, u32[]{:S(2)}, u32[]{:S(2)}) collective-permute-start(bf16[176,1024]{1,0:T(8,128)(2,1)S(1)} %get-tuple-element.38), channel_id=1, source_target_pairs={{0,1},{1,2},{2,3},{3,0},{4,5},{5,6},{6,7},{7,4},{8,9},{9,10},{10,1... | collective-permute-start | bytes 1081352 | tf_op jit(solution)/shard_map/ppermute | solution.py:477
  70.0 25.1 %copy-start.6 = (f32[2048]{0:T(1024)S(1)}, f32[2048]{0:T(1024)}, u32[]{:S(2)}) copy-start(f32[2048]{0:T(1024)} %param.26) | copy-start | bytes 24580
  70.0 25.1 %copy-start.7 = (f32[2048]{0:T(1024)S(1)}, f32[2048]{0:T(1024)}, u32[]{:S(2)}) copy-start(f32[2048]{0:T(1024)} %param.27) | copy-start | bytes 24580
  70.0 9.2 %collective-permute-start.2 = (bf16[176,1024]{1,0:T(8,128)(2,1)S(1)}, bf16[176,1024]{1,0:T(8,128)(2,1)S(1)}, u32[]{:S(2)}, u32[]{:S(2)}) collective-permute-start(bf16[176,1024]{1,0:T(8,128)(2,1)S(1)} %get-tuple-element.40), channel_id=1, source_target_pairs={{0,3},{1,0},{2,1},{3,2},{4,7},{5,4},{6,5},{7,6},{8,11},{9,8},{10,9... | collective-permute-start | bytes 1081352 | tf_op jit(solution)/shard_map/ppermute | solution.py:477
  75.5 11.9 %collective-permute-start.4 = (bf16[176,1024]{1,0:T(8,128)(2,1)S(1)}, bf16[176,1024]{1,0:T(8,128)(2,1)S(1)}, u32[]{:S(2)}, u32[]{:S(2)}) collective-permute-start(bf16[176,1024]{1,0:T(8,128)(2,1)S(1)} %get-tuple-element.42), channel_id=1, source_target_pairs={{0,1},{1,2},{2,3},{3,0},{4,5},{5,6},{6,7},{7,4},{8,9},{9,10},{10,1... | collective-permute-start | bytes 1081352 | tf_op jit(solution)/shard_map/ppermute | solution.py:477
  75.6 11.7 %collective-permute-start.5 = (bf16[176,1024]{1,0:T(8,128)(2,1)S(1)}, bf16[176,1024]{1,0:T(8,128)(2,1)S(1)}, u32[]{:S(2)}, u32[]{:S(2)}) collective-permute-start(bf16[176,1024]{1,0:T(8,128)(2,1)S(1)} %get-tuple-element.43), channel_id=1, source_target_pairs={{0,3},{1,0},{2,1},{3,2},{4,7},{5,4},{6,5},{7,6},{8,11},{9,8},{10,9... | collective-permute-start | bytes 1081352 | tf_op jit(solution)/shard_map/ppermute | solution.py:477
  79.4 15.7 %collective-permute-start.3 = (bf16[176,1024]{1,0:T(8,128)(2,1)S(1)}, bf16[176,1024]{1,0:T(8,128)(2,1)S(1)}, u32[]{:S(2)}, u32[]{:S(2)}) collective-permute-start(bf16[176,1024]{1,0:T(8,128)(2,1)S(1)} %get-tuple-element.41), channel_id=1, source_target_pairs={{0,1},{1,2},{2,3},{3,0},{4,5},{5,6},{6,7},{7,4},{8,9},{9,10},{10,1... | collective-permute-start | bytes 1081352 | tf_op jit(solution)/shard_map/ppermute | solution.py:477
  80.4 14.7 %collective-permute-start.6 = (bf16[176,1024]{1,0:T(8,128)(2,1)S(1)}, bf16[176,1024]{1,0:T(8,128)(2,1)S(1)}, u32[]{:S(2)}, u32[]{:S(2)}) collective-permute-start(bf16[176,1024]{1,0:T(8,128)(2,1)S(1)} %get-tuple-element.44), channel_id=1, source_target_pairs={{0,3},{1,0},{2,1},{3,2},{4,7},{5,4},{6,5},{7,6},{8,11},{9,8},{10,9... | collective-permute-start | bytes 1081352 | tf_op jit(solution)/shard_map/ppermute | solution.py:477
  95.1 42.3 %copy-start.4 = (bf16[3,1408]{1,0:T(4,128)(2,1)S(1)}, bf16[3,1408]{1,0:T(4,128)(2,1)}, u32[]{:S(2)}) copy-start(bf16[3,1408]{1,0:T(4,128)(2,1)} %refs_12_.3) | copy-start | bytes 25348
  95.1 42.3 %copy-start.5 = (bf16[3,1408]{1,0:T(4,128)(2,1)S(1)}, bf16[3,1408]{1,0:T(4,128)(2,1)}, u32[]{:S(2)}) copy-start(bf16[3,1408]{1,0:T(4,128)(2,1)} %refs_13_.1) | copy-start | bytes 25348
  99.5 9.2 %collective-permute-start.10 = (bf16[176,1024]{1,0:T(8,128)(2,1)S(1)}, bf16[176,1024]{1,0:T(8,128)(2,1)S(1)}, u32[]{:S(2)}, u32[]{:S(2)}) collective-permute-start(bf16[176,1024]{1,0:T(8,128)(2,1)S(1)} %get-tuple-element.45.refs_2_), channel_id=1, source_target_pairs={{0,3},{1,0},{2,1},{3,2},{4,7},{5,4},{6,5},{7,6},{8,11},{9,8},{10,9... | collective-permute-start | bytes 1081352 | tf_op jit(solution)/shard_map/ppermute | solution.py:477
  102.2 9.7 %collective-permute-start.8 = (bf16[176,1024]{1,0:T(8,128)(2,1)S(1)}, bf16[176,1024]{1,0:T(8,128)(2,1)S(1)}, u32[]{:S(2)}, u32[]{:S(2)}) collective-permute-start(bf16[176,1024]{1,0:T(8,128)(2,1)S(1)} %get-tuple-element.45.refs_2_), channel_id=1, source_target_pairs={{0,1},{1,2},{2,3},{3,0},{4,5},{5,6},{6,7},{7,4},{8,9},{9,10},{10,1... | collective-permute-start | bytes 1081352 | tf_op jit(solution)/shard_map/ppermute | solution.py:477
  102.2 14.2 %collective-permute-start.11 = (bf16[176,1024]{1,0:T(8,128)(2,1)S(1)}, bf16[176,1024]{1,0:T(8,128)(2,1)S(1)}, u32[]{:S(2)}, u32[]{:S(2)}) collective-permute-start(bf16[176,1024]{1,0:T(8,128)(2,1)S(1)} %get-tuple-element.46.refs_3_), channel_id=1, source_target_pairs={{0,3},{1,0},{2,1},{3,2},{4,7},{5,4},{6,5},{7,6},{8,11},{9,8},{10,9... | collective-permute-start | bytes 1081352 | tf_op jit(solution)/shard_map/ppermute | solution.py:477
  104.9 14.7 %collective-permute-start.9 = (bf16[176,1024]{1,0:T(8,128)(2,1)S(1)}, bf16[176,1024]{1,0:T(8,128)(2,1)S(1)}, u32[]{:S(2)}, u32[]{:S(2)}) collective-permute-start(bf16[176,1024]{1,0:T(8,128)(2,1)S(1)} %get-tuple-element.46.refs_3_), channel_id=1, source_target_pairs={{0,1},{1,2},{2,3},{3,0},{4,5},{5,6},{6,7},{7,4},{8,9},{9,10},{10,1... | collective-permute-start | bytes 1081352 | tf_op jit(solution)/shard_map/ppermute | solution.py:477
  119.7 6.8 %collective-permute-start.12 = (bf16[16,2048]{1,0:T(8,128)(2,1)S(1)}, bf16[16,2048]{1,0:T(8,128)(2,1)S(1)}, u32[]{:S(2)}, u32[]{:S(2)}) collective-permute-start(bf16[16,2048]{1,0:T(8,128)(2,1)S(1)} %get-tuple-element.59), channel_id=1, source_target_pairs={{0,4},{2,6},{3,7},{4,8},{6,10},{7,11},{8,12},{10,14},{11,15},{12,1... | collective-permute-start | bytes 196616 | tf_op jit(solution)/shard_map/ppermute | solution.py:553
  123.0 3.5 %collective-permute-start.7 = (bf16[16,2048]{1,0:T(8,128)(2,1)S(1)}, bf16[16,2048]{1,0:T(8,128)(2,1)S(1)}, u32[]{:S(2)}, u32[]{:S(2)}) collective-permute-start(bf16[16,2048]{1,0:T(8,128)(2,1)S(1)} %get-tuple-element.60), channel_id=1, source_target_pairs={{3,5},{7,9},{11,13},{15,17},{19,21},{23,25},{27,29},{31,33},{35,37... | collective-permute-start | bytes 196616 | tf_op jit(solution)/shard_map/ppermute | solution.py:552
  123.7 11.1 %collective-permute-start.13 = (bf16[176,1024]{1,0:T(8,128)(2,1)S(1)}, bf16[176,1024]{1,0:T(8,128)(2,1)S(1)}, u32[]{:S(2)}, u32[]{:S(2)}) collective-permute-start(bf16[176,1024]{1,0:T(8,128)(2,1)S(1)} %collective-permute-done.8.refs_8_), channel_id=1, source_target_pairs={{0,1},{1,2},{2,3},{3,0},{4,5},{5,6},{6,7},{7,4},{8,9},{9,10},{10,1... | collective-permute-start | bytes 1081352 | tf_op jit(solution)/shard_map/ppermute | solution.py:477
  123.8 10.9 %collective-permute-start.14 = (bf16[176,1024]{1,0:T(8,128)(2,1)S(1)}, bf16[176,1024]{1,0:T(8,128)(2,1)S(1)}, u32[]{:S(2)}, u32[]{:S(2)}) collective-permute-start(bf16[176,1024]{1,0:T(8,128)(2,1)S(1)} %collective-permute-done.11.refs_5_), channel_id=1, source_target_pairs={{0,3},{1,0},{2,1},{3,2},{4,7},{5,4},{6,5},{7,6},{8,11},{9,8},{10,9... | collective-permute-start | bytes 1081352 | tf_op jit(solution)/shard_map/ppermute | solution.py:477
  134.8 0.7 copy-start.1
  137.3 1.0 copy-start.2
  147.1 20.3 %collective-permute-start.15 = (bf16[176,1024]{1,0:T(8,128)(2,1)S(1)}, bf16[176,1024]{1,0:T(8,128)(2,1)S(1)}, u32[]{:S(2)}, u32[]{:S(2)}) collective-permute-start(bf16[176,1024]{1,0:T(8,128)(2,1)S(1)} %get-tuple-element.51), channel_id=1, source_target_pairs={{0,1},{1,2},{2,3},{3,0},{4,5},{5,6},{6,7},{7,4},{8,9},{9,10},{10,1... | collective-permute-start | bytes 1081352 | tf_op jit(solution)/shard_map/ppermute | solution.py:477
  148.4 19.0 %collective-permute-start.16 = (bf16[176,1024]{1,0:T(8,128)(2,1)S(1)}, bf16[176,1024]{1,0:T(8,128)(2,1)S(1)}, u32[]{:S(2)}, u32[]{:S(2)}) collective-permute-start(bf16[176,1024]{1,0:T(8,128)(2,1)S(1)} %get-tuple-element.53), channel_id=1, source_target_pairs={{0,3},{1,0},{2,1},{3,2},{4,7},{5,4},{6,5},{7,6},{8,11},{9,8},{10,9... | collective-permute-start | bytes 1081352 | tf_op jit(solution)/shard_map/ppermute | solution.py:477
  149.9 32.9 %copy-start.8 = (f32[2048]{0:T(1024)S(1)}, f32[2048]{0:T(1024)}, u32[]{:S(2)}) copy-start(f32[2048]{0:T(1024)} %param.28) | copy-start | bytes 24580
  164.6 10.5 %collective-permute-start.18 = (bf16[176,1024]{1,0:T(8,128)(2,1)S(1)}, bf16[176,1024]{1,0:T(8,128)(2,1)S(1)}, u32[]{:S(2)}, u32[]{:S(2)}) collective-permute-start(bf16[176,1024]{1,0:T(8,128)(2,1)S(1)} %get-tuple-element.55), channel_id=1, source_target_pairs={{0,1},{1,2},{2,3},{3,0},{4,5},{5,6},{6,7},{7,4},{8,9},{9,10},{10,1... | collective-permute-start | bytes 1081352 | tf_op jit(solution)/shard_map/ppermute | solution.py:477
  164.7 10.3 %collective-permute-start.19 = (bf16[176,1024]{1,0:T(8,128)(2,1)S(1)}, bf16[176,1024]{1,0:T(8,128)(2,1)S(1)}, u32[]{:S(2)}, u32[]{:S(2)}) collective-permute-start(bf16[176,1024]{1,0:T(8,128)(2,1)S(1)} %get-tuple-element.56), channel_id=1, source_target_pairs={{0,3},{1,0},{2,1},{3,2},{4,7},{5,4},{6,5},{7,6},{8,11},{9,8},{10,9... | collective-permute-start | bytes 1081352 | tf_op jit(solution)/shard_map/ppermute | solution.py:477
  167.6 15.2 %collective-permute-start.17 = (bf16[176,1024]{1,0:T(8,128)(2,1)S(1)}, bf16[176,1024]{1,0:T(8,128)(2,1)S(1)}, u32[]{:S(2)}, u32[]{:S(2)}) collective-permute-start(bf16[176,1024]{1,0:T(8,128)(2,1)S(1)} %get-tuple-element.54), channel_id=1, source_target_pairs={{0,1},{1,2},{2,3},{3,0},{4,5},{5,6},{6,7},{7,4},{8,9},{9,10},{10,1... | collective-permute-start | bytes 1081352 | tf_op jit(solution)/shard_map/ppermute | solution.py:477
  167.8 15.0 %collective-permute-start.20 = (bf16[176,1024]{1,0:T(8,128)(2,1)S(1)}, bf16[176,1024]{1,0:T(8,128)(2,1)S(1)}, u32[]{:S(2)}, u32[]{:S(2)}) collective-permute-start(bf16[176,1024]{1,0:T(8,128)(2,1)S(1)} %get-tuple-element.57), channel_id=1, source_target_pairs={{0,3},{1,0},{2,1},{3,2},{4,7},{5,4},{6,5},{7,6},{8,11},{9,8},{10,9... | collective-permute-start | bytes 1081352 | tf_op jit(solution)/shard_map/ppermute | solution.py:477
Sparse Core Ops, SparseCore 0:
  9.2 128.0 all-gather.1

commit v5 on v4

--- a/solution.py
+++ b/solution.py
@@ -152,22 +152,22 @@
             at = slice(part * seg_rows, (part + 1) * seg_rows)
             state[at, :] = loc[b, at, :] + cum[b, at, :] * carry[block * per_block + part, 0:1, :]
         out = (state[...] * gelu(gates[b].astype(jnp.float32))).astype(jnp.bfloat16)
-        put(outs, b, jnp.dot(out, w_ref[...], preferred_element_type=jnp.float32))
-
-
-def put(outs, block, share):
+        put(outs, b, turns[b], jnp.dot(out, w_ref[...], preferred_element_type=jnp.float32))
+
+
+def put(outs, at, steps, share):
     share = share.astype(jnp.bfloat16)
     half = share.shape[1] // 2
-    if block < 2:
-        outs[2 * block][...] = share[:, :half]
-        outs[2 * block + 1][...] = share[:, half:]
+    if steps:
+        outs[2 * at][...] = share[:, :half]
+        outs[2 * at + 1][...] = share[:, half:]
     else:
-        outs[4][...] = share
+        outs[2 * at][...] = share
 
 
 VMEM = pl.BlockSpec(memory_space=pltpu.VMEM)
 HERE = pl.BlockSpec(memory_space=pltpu.HBM)
-OPPOSITE, OTHERS = (2,), (1, 3, 0)
+OPPOSITE, SIDES, OTHERS, OWN = (2,), (1, 3), (1, 3, 0), (0,)
 
 
 def vm(value):
@@ -178,13 +178,17 @@
     return pltpu.with_memory_space_constraint(value, pltpu.HBM)
 
 
+def hbm_out(shape):
+    return pltpu.HBM(shape, jnp.bfloat16)
+
+
 def vm_out(shape):
     return pltpu.VMEM(shape, jnp.bfloat16)
 
 
 def share_shapes(turns, rows, width):
     half = vm_out((rows, width // 2))
-    return [half] * 2 if len(turns) == 1 else [half] * 4 + [vm_out((rows, width))]
+    return sum(([half] * 2 if steps else [vm_out((rows, width))] for steps in turns), [])
 
 
 def branch_shares(me, arrived, seg, cum, loc, gate, weight, turns):
@@ -217,13 +221,13 @@
 
 
 def feed_kernel(*refs, turns):
-    first = len(turns) == 1
+    first = turns == OPPOSITE
     me_ref, outside = refs[:2]
     halves = {0: refs[2:4], 1: refs[4:6], 2: refs[6:8], 3: refs[8:10]}
     if first:
-        weights, gk_ref, vk_ref, *outs, ring, down, lhs, up_a, up_b, act, sems = refs[10:]
+        weights, gk_ref, vk_ref, *outs, ring, down, lhs, up, act, sems = refs[10:]
     else:
-        ring, down, gk_ref, vk_ref, *outs, lhs, up_a, up_b, act = refs[10:]
+        ring, down, gk_ref, vk_ref, *outs, lhs, up, act = refs[10:]
     rows = halves[0][0].shape[0]
     tall = rows + HALO
     taps = gk_ref.shape[0]
@@ -247,7 +251,8 @@
         for part, own in zip(columns, halves[steps]):
             lhs[at + HALO : at + tall, part] = own[...]
 
-    def activate(chunk, up):
+    def activate(chunk):
+        side = lax.rem(chunk, 2)
         lanes = pl.ds(pl.multiple_of(chunk * LANES, LANES), LANES)
         gate_taps = gk_ref[:, lanes].astype(jnp.float32)
         value_taps = vk_ref[:, lanes].astype(jnp.float32)
@@ -256,13 +261,13 @@
             value = jnp.zeros((rows, LANES), jnp.float32)
             for k in range(taps):
                 at = b * tall + HALO - (taps - 1) + k
-                gate = gate + up[at : at + rows, 0:LANES] * gate_taps[k : k + 1, :]
-                value = value + up[at : at + rows, LANES : 2 * LANES] * value_taps[k : k + 1, :]
+                gate = gate + up[side, at : at + rows, 0:LANES] * gate_taps[k : k + 1, :]
+                value = value + up[side, at : at + rows, LANES : 2 * LANES] * value_taps[k : k + 1, :]
             act[b * rows : (b + 1) * rows, lanes] = (gelu(gate) * value).astype(jnp.bfloat16)
 
-    def project(chunk, up):
+    def project(chunk):
         sides = [ring[chunk, :, side].reshape(width, LANES) for side in range(2)]
-        up[...] = (
+        up[lax.rem(chunk, 2)] = (
             jnp.dot(lhs[...], jnp.concatenate(sides, axis=1), preferred_element_type=jnp.float32)
             .astype(jnp.bfloat16)
             .astype(jnp.float32)
@@ -277,44 +282,38 @@
         fill(b, steps)
     if first:
         get(jnp.int32(0)).wait()
-    project(jnp.int32(0), up_a)
-
-    def pair(i, carry):
-        chunk = 2 * i
+    project(jnp.int32(0))
+
+    def step(chunk, carry):
         if first:
             get(chunk + 1).wait()
-            get(chunk + 2).wait()
-        activate(chunk, up_a)
-        project(chunk + 1, up_b)
-        activate(chunk + 1, up_b)
-        project(chunk + 2, up_a)
+        activate(chunk)
+        project(chunk + 1)
         return carry
 
-    lax.fori_loop(0, chunks // 2, pair, 0)
+    lax.fori_loop(0, chunks - 1, step, 0)
     if first:
         get_down.wait()
-    activate(jnp.int32(chunks - 1), up_a)
+    activate(jnp.int32(chunks - 1))
     turned = jnp.concatenate([down[:, c].reshape(width, LANES) for c in range(chunks)], axis=1)
     share = lax.dot_general(
         act[...], turned, (((1,), (1,)), ((), ())), preferred_element_type=jnp.float32
     )
     for b in range(len(turns)):
-        put(outs, b, share[b * rows : (b + 1) * rows, :])
+        put(outs, b, turns[b], share[b * rows : (b + 1) * rows, :])
 
 
 def feed(me, outside, halves, weights, gate_kernel, value_kernel, turns):
-    first = len(turns) == 1
+    first = turns == OPPOSITE
     count = len(turns)
     rows, half = halves[0].shape
     width, units = 2 * half, gate_kernel.shape[1]
     chunks = units // LANES
-    assert chunks % 2 == 1
     tall = count * (rows + HALO)
     out_shape = share_shapes(turns, rows, width)
     scratch = [
         pltpu.VMEM((tall, width), jnp.bfloat16),
-        pltpu.VMEM((tall, 2 * LANES), jnp.float32),
-        pltpu.VMEM((tall, 2 * LANES), jnp.float32),
+        pltpu.VMEM((2, tall, 2 * LANES), jnp.float32),
         pltpu.VMEM((count * rows, units), jnp.bfloat16),
     ]
     if first:
@@ -344,8 +343,8 @@
             transcendentals=count * rows * units,
         ),
         compiler_params=pltpu.CompilerParams(vmem_limit_bytes=12 * MIB),
-        name="feed_first" if first else "feed_rest",
-    )(me, vm(outside), *map(vm, halves), *weights, gate_kernel, value_kernel)
+        name={OPPOSITE: "feed_first", SIDES: "feed_sides", OWN: "feed_own"}[turns],
+    )(me, outside, *map(vm, halves[:4]), *halves[4:6], *map(vm, halves[6:]), *weights, gate_kernel, value_kernel)
 
 
 def pack_kernel(gate_ref, value_ref, turned_ref, out_ref):
@@ -420,7 +419,7 @@
         in_specs=[pl.BlockSpec(memory_space=pltpu.SMEM), *[VMEM] * 5, HERE, VMEM, VMEM],
         out_specs=[VMEM] * 3,
         out_shape=[
-            jax.ShapeDtypeStruct((rows, width), jnp.bfloat16),
+            hbm_out((rows, width)),
             *[vm_out((rows, width // 2))] * 2,
         ],
         scratch_shapes=[pltpu.VMEM((rows, width), jnp.bfloat16), pltpu.SemaphoreType.DMA],
@@ -560,7 +559,8 @@
     *first, ring, down = feed(
         me, outside, halves, (hbm(weights),), gate_kernel, value_kernel, turns=OPPOSITE
     )
-    rest = feed(me, outside, halves, (ring, down), gate_kernel, value_kernel, turns=OTHERS)
+    given = (me, outside, halves, (ring, down), gate_kernel, value_kernel)
+    rest = feed(*given, turns=SIDES) + feed(*given, turns=OWN)
     return last(ring_sum(first, rest), hidden_state, final_gain[None])
 
 

time: 193 us -> 187 us (0.969)
  waiting for transfers between devices: 85.3 us -> 78.3 us
  Pallas kernels: 45.9 us -> 49.4 us
    ppermute x18, waiting for transfers between devices: 49 us -> 42 us  [turn(): lax.ppermute(value, axis, [(i, (i + steps) % count) for i in range(count)])]
    pallas_call x2 -> x3, Pallas kernels: 23.5 us -> 26.3 us  [feed(): pl.pallas_call(functools.partial(feed_kernel, turns=turns), in_specs=[pl....]
  transfers between devices with their start and end apart: 23 -> 23, of which waited for: 13 -> 12; matrix products, arithmetic and copies ran while one was open for 0% -> 0% of each run, Pallas kernels for 17% -> 19%
where the time goes in v5:
time: 187 us
  waiting for transfers between devices  78.3 us (42%)
  Pallas kernels  49.4 us (26%)
  starting transfers between devices  43.4 us (23%)
  between operations  13.6 us (7%)
  local copies, waits for them, and re-layouts  2.11 us (1%)
    ppermute x18, waiting for transfers between devices, turn(): lax.ppermute(value, axis, [(i, (i + steps) % count) for i in range(count)])  42 us
    pallas_call x3, Pallas kernels, feed(): pl.pallas_call(functools.partial(feed_kernel, turns=turns), in_specs=[pl....  26.3 us
    ppermute x18, starting transfers between devices, turn(): lax.ppermute(value, axis, [(i, (i + steps) % count) for i in range(count)])  25.3 us
    all_to_all x1, waiting for transfers between devices, exchanged(): return lax.all_to_all(tiles, axis, split_axis=0, concat_axis=0, tiled=True)  17.8 us
    ppermute x1, waiting for transfers between devices, from_behind(): return lax.ppermute(value, axis, [(i, i + 1) for i in range(count - 1)])  16.6 us
    all_to_all x1, starting transfers between devices, exchanged(): return lax.all_to_all(tiles, axis, split_axis=0, concat_axis=0, tiled=True)  8.28 us
    pallas_call x1, Pallas kernels, local_scan(): pl.pallas_call(scan_kernel, grid=(groups,), in_specs=[column(length), col...  6.78 us
    pallas_call x2, Pallas kernels, branch_shares(): pl.pallas_call(functools.partial(branch_kernel, turns=turns), in_specs=[p...  6.28 us
  transfers between devices with their start and end apart: 23, of which 12 were waited for; matrix products, arithmetic and copies ran while one was open for 0% of the time, Pallas kernels for 19%

profile of v5, /device:TPU:33, one launch (start us, length us, event | category | flops | bytes accessed | tf_op | source)
XLA Modules:
  0.0 186.9 jit_solution(5274130676353622028)
XLA Ops:
  6.6 2.1 %pack.1 = bf16[33,64,128]{2,1,0:T(8,128)(2,1)} custom-call(bf16[64,1408]{1,0:T(8,128)(2,1)} %gate_ref.1, bf16[64,1408]{1,0:T(8,128)(2,1)} %value_ref.1, bf16[64,1408]{1,0:T(8,128)(2,1)} %bitcast.12), custom_call_target="tpu_custom_call" | custom-call | tf_op jit(solution)/shard_map/pack/pallas_call | solution.py:361
  8.7 0.1 all-gather.2.cloned.1.call-update
  8.7 0.7 slice.21
  9.4 5.7 %collective-permute-start = (bf16[8,512]{1,0:T(8,128)(2,1)S(1)}, bf16[8,512]{1,0:T(8,128)(2,1)S(1)}, u32[]{:S(2)}, u32[]{:S(2)}) collective-permute-start(bf16[8,512]{1,0:T(8,128)(2,1)S(1)} %slice.21), channel_id=1, source_target_pairs={{0,4},{4,8},{8,12},{12,16},{16,20},{20,24},{24,28},{28,32},{32,36}... | collective-permute-start | bytes 24584 | tf_op jit(solution)/shard_map/ppermute | solution.py:490
  15.2 16.6 %collective-permute-done.edge_ref = bf16[8,512]{1,0:T(8,128)(2,1)S(1)} collective-permute-done((bf16[8,512]{1,0:T(8,128)(2,1)S(1)}, bf16[8,512]{1,0:T(8,128)(2,1)S(1)}, u32[]{:S(2)}, u32[]{:S(2)}) %collective-permute-start) | collective-permute-done | bytes 8224 | tf_op jit(solution)/shard_map/ppermute | solution.py:490
  31.8 0.6 copy-done.8
  32.4 6.8 %local_scan.1 = (f32[704,512]{1,0:T(8,128)}, f32[704,512]{1,0:T(8,128)}, f32[2,8,512]{2,1,0:T(8,128)}, f32[32,8,128]{2,1,0:T(8,128)}) custom-call(bf16[704,512]{1,0:T(8,128)(2,1)} %x_ref.1, bf16[8,512]{1,0:T(8,128)(2,1)} %copy-done.8, bf16[4,512]{1,0:T(4,128)(2,1)} %taps_ref.1, bf16[4,128,128]{2,1,0:T(8,128)(2,1)} %rmap_ref.1, ...), custom_call_target="tpu_custom_call" | custom-call | tf_op jit(solution)/shard_map/local_scan/pallas_call | solution.py:95
  39.2 8.3 %all-to-all-start = ((f32[32,8,128]{2,1,0:T(8,128)}), f32[32,8,128]{2,1,0:T(8,128)S(1)}, u32[]{:S(2)}, u32[]{:S(2)}) async-start(f32[32,8,128]{2,1,0:T(8,128)} %get-tuple-element.31), calls=%async_computation | async-start | bytes 262144 | tf_op jit(solution)/shard_map/all_to_all | solution.py:494
  47.5 0.1 pad_add_fusion.me_ref.refs_0_
  47.5 17.8 %all-to-all-done.arrived = f32[32,8,128]{2,1,0:T(8,128)S(1)} async-done(((f32[32,8,128]{2,1,0:T(8,128)}), f32[32,8,128]{2,1,0:T(8,128)S(1)}, u32[]{:S(2)}, u32[]{:S(2)}) %all-to-all-start) | async-done | bytes 131104 | tf_op jit(solution)/shard_map/all_to_all | solution.py:494
  65.4 0.8 copy-done.2
  66.1 2.4 %branch_first.1 = (bf16[176,1024]{1,0:T(8,128)(2,1)S(1)}, bf16[176,1024]{1,0:T(8,128)(2,1)S(1)}) custom-call(s32[2]{0:T(128)S(1)} %pad_add_fusion.me_ref.refs_0_, f32[32,8,128]{2,1,0:T(8,128)S(1)} %all-to-all-done.arrived, f32[2,8,512]{2,1,0:T(8,128)S(1)} %copy-done.2, f32[704,512]{1,0:T(8,128)} %get-tuple-element.33.cum_hbm, ...), custom_call_target="tpu_custom_call" | custom-call | flops 369098752 | bytes 3719168 | tf_op jit(solution)/shard_map/branch_first/pallas_call | solution.py:200
  68.5 1.5 collective-permute-start.1
  70.0 1.6 collective-permute-start.2
  71.5 3.9 %branch_rest.1 = (bf16[176,1024]{1,0:T(8,128)(2,1)S(1)}, bf16[176,1024]{1,0:T(8,128)(2,1)S(1)}, bf16[176,1024]{1,0:T(8,128)(2,1)S(1)}, bf16[176,1024]{1,0:T(8,128)(2,1)S(1)}, bf16[176,2048]{1,0:T(8,128)(2,1)S(1)}) custom-call(s32[2]{0:T(128)S(1)} %pad_add_fusion.me_ref.refs_0_, f32[32,8,128]{2,1,0:T(8,128)S(1)} %all-to-all-done.arrived, ...), custom_call_target="tpu_custom_call" | custom-call | flops 1107296256 | bytes 6963200 | tf_op jit(solution)/shard_map/branch_rest/pallas_call | solution.py:200
  75.5 0.1 collective-permute-start.4
  75.6 2.6 %collective-permute-start.5 = (bf16[176,1024]{1,0:T(8,128)(2,1)S(1)}, bf16[176,1024]{1,0:T(8,128)(2,1)S(1)}, u32[]{:S(2)}, u32[]{:S(2)}) collective-permute-start(bf16[176,1024]{1,0:T(8,128)(2,1)S(1)} %get-tuple-element.42), channel_id=1, source_target_pairs={{0,3},{1,0},{2,1},{3,2},{4,7},{5,4},{6,5},{7,6},{8,11},{9,8},{10,9... | collective-permute-start | bytes 1081352 | tf_op jit(solution)/shard_map/ppermute | solution.py:476
  78.2 0.9 collective-permute-done.1.low_ref
  79.1 0.0 collective-permute-done.2.high_ref
  79.1 0.2 join.2
  79.3 1.0 collective-permute-start.3
  80.4 1.9 %collective-permute-start.6 = (bf16[176,1024]{1,0:T(8,128)(2,1)S(1)}, bf16[176,1024]{1,0:T(8,128)(2,1)S(1)}, u32[]{:S(2)}, u32[]{:S(2)}) collective-permute-start(bf16[176,1024]{1,0:T(8,128)(2,1)S(1)} %get-tuple-element.43), channel_id=1, source_target_pairs={{0,3},{1,0},{2,1},{3,2},{4,7},{5,4},{6,5},{7,6},{8,11},{9,8},{10,9... | collective-permute-start | bytes 1081352 | tf_op jit(solution)/shard_map/ppermute | solution.py:476
  82.3 5.0 %collective-permute-done.4.refs_2_ = bf16[176,1024]{1,0:T(8,128)(2,1)S(1)} collective-permute-done((bf16[176,1024]{1,0:T(8,128)(2,1)S(1)}, bf16[176,1024]{1,0:T(8,128)(2,1)S(1)}, u32[]{:S(2)}, u32[]{:S(2)}) %collective-permute-start.4) | collective-permute-done | bytes 360480 | tf_op jit(solution)/shard_map/ppermute | solution.py:476
  87.3 0.0 collective-permute-done.5.refs_3_
  87.3 7.7 %collective-permute-done.3.refs_1_ = bf16[176,1024]{1,0:T(8,128)(2,1)S(1)} collective-permute-done((bf16[176,1024]{1,0:T(8,128)(2,1)S(1)}, bf16[176,1024]{1,0:T(8,128)(2,1)S(1)}, u32[]{:S(2)}, u32[]{:S(2)}) %collective-permute-start.3) | collective-permute-done | bytes 360480 | tf_op jit(solution)/shard_map/ppermute | solution.py:476
  95.0 0.0 collective-permute-done.6.refs_4_
  95.0 0.0 copy-start.3
  95.0 0.0 copy-start.4
  95.0 5.1 %mid.1 = (bf16[176,2048]{1,0:T(8,128)(2,1)}, bf16[176,1024]{1,0:T(8,128)(2,1)S(1)}, bf16[176,1024]{1,0:T(8,128)(2,1)S(1)}) custom-call(s32[2]{0:T(128)S(1)} %pad_add_fusion.me_ref.refs_0_, bf16[176,2048]{1,0:T(8,128)(2,1)S(1)} %get-tuple-element.35.refs_0_, bf16[176,1024]{1,0:T(8,128)(2,1)S(1)} %collective-permute-done.3.refs_1_, ...), custom_call_target="tpu_custom_call" | custom-call | tf_op jit(solution)/shard_map/mid/pallas_call | solution.py:417
  100.2 2.8 %collective-permute-start.10 = (bf16[176,1024]{1,0:T(8,128)(2,1)S(1)}, bf16[176,1024]{1,0:T(8,128)(2,1)S(1)}, u32[]{:S(2)}, u32[]{:S(2)}) collective-permute-start(bf16[176,1024]{1,0:T(8,128)(2,1)S(1)} %get-tuple-element.44.refs_2_), channel_id=1, source_target_pairs={{0,3},{1,0},{2,1},{3,2},{4,7},{5,4},{6,5},{7,6},{8,11},{9,8},{10,9... | collective-permute-start | bytes 1081352 | tf_op jit(solution)/shard_map/ppermute | solution.py:476
  102.9 0.0 collective-permute-start.8
  102.9 2.7 %collective-permute-start.11 = (bf16[176,1024]{1,0:T(8,128)(2,1)S(1)}, bf16[176,1024]{1,0:T(8,128)(2,1)S(1)}, u32[]{:S(2)}, u32[]{:S(2)}) collective-permute-start(bf16[176,1024]{1,0:T(8,128)(2,1)S(1)} %get-tuple-element.45.refs_3_), channel_id=1, source_target_pairs={{0,3},{1,0},{2,1},{3,2},{4,7},{5,4},{6,5},{7,6},{8,11},{9,8},{10,9... | collective-permute-start | bytes 1081352 | tf_op jit(solution)/shard_map/ppermute | solution.py:476
  105.6 0.0 collective-permute-start.9
  105.6 3.7 %collective-permute-done.10.refs_4_ = bf16[176,1024]{1,0:T(8,128)(2,1)S(1)} collective-permute-done((bf16[176,1024]{1,0:T(8,128)(2,1)S(1)}, bf16[176,1024]{1,0:T(8,128)(2,1)S(1)}, u32[]{:S(2)}, u32[]{:S(2)}) %collective-permute-start.10) | collective-permute-done | bytes 360480 | tf_op jit(solution)/shard_map/ppermute | solution.py:476
  109.4 3.2 %collective-permute-done.8.refs_8_ = bf16[176,1024]{1,0:T(8,128)(2,1)S(1)} collective-permute-done((bf16[176,1024]{1,0:T(8,128)(2,1)S(1)}, bf16[176,1024]{1,0:T(8,128)(2,1)S(1)}, u32[]{:S(2)}, u32[]{:S(2)}) %collective-permute-start.8) | collective-permute-done | bytes 360480 | tf_op jit(solution)/shard_map/ppermute | solution.py:476
  112.6 4.5 %collective-permute-done.11.refs_5_ = bf16[176,1024]{1,0:T(8,128)(2,1)S(1)} collective-permute-done((bf16[176,1024]{1,0:T(8,128)(2,1)S(1)}, bf16[176,1024]{1,0:T(8,128)(2,1)S(1)}, u32[]{:S(2)}, u32[]{:S(2)}) %collective-permute-start.11) | collective-permute-done | bytes 360480 | tf_op jit(solution)/shard_map/ppermute | solution.py:476
  117.1 3.2 %collective-permute-done.9.refs_9_ = bf16[176,1024]{1,0:T(8,128)(2,1)S(1)} collective-permute-done((bf16[176,1024]{1,0:T(8,128)(2,1)S(1)}, bf16[176,1024]{1,0:T(8,128)(2,1)S(1)}, u32[]{:S(2)}, u32[]{:S(2)}) %collective-permute-start.9) | collective-permute-done | bytes 360480 | tf_op jit(solution)/shard_map/ppermute | solution.py:476
  120.4 3.4 %collective-permute-start.12 = (bf16[16,2048]{1,0:T(8,128)(2,1)S(1)}, bf16[16,2048]{1,0:T(8,128)(2,1)S(1)}, u32[]{:S(2)}, u32[]{:S(2)}) collective-permute-start(bf16[16,2048]{1,0:T(8,128)(2,1)S(1)} %get-tuple-element.57), channel_id=1, source_target_pairs={{0,4},{2,6},{3,7},{4,8},{6,10},{7,11},{8,12},{10,14},{11,15},{12,1... | collective-permute-start | bytes 196616 | tf_op jit(solution)/shard_map/ppermute | solution.py:552
  123.8 0.7 collective-permute-start.7
  124.4 0.1 collective-permute-start.13
  124.6 2.6 %collective-permute-start.14 = (bf16[176,1024]{1,0:T(8,128)(2,1)S(1)}, bf16[176,1024]{1,0:T(8,128)(2,1)S(1)}, u32[]{:S(2)}, u32[]{:S(2)}) collective-permute-start(bf16[176,1024]{1,0:T(8,128)(2,1)S(1)} %collective-permute-done.11.refs_5_), channel_id=1, source_target_pairs={{0,3},{1,0},{2,1},{3,2},{4,7},{5,4},{6,5},{7,6},{8,11},{9,8},{10,9... | collective-permute-start | bytes 1081352 | tf_op jit(solution)/shard_map/ppermute | solution.py:476
  127.2 0.0 collective-permute-done.12
  127.2 0.0 collective-permute-done.7
  127.2 8.3 %collective-permute-done.13.refs_6_ = bf16[176,1024]{1,0:T(8,128)(2,1)S(1)} collective-permute-done((bf16[176,1024]{1,0:T(8,128)(2,1)S(1)}, bf16[176,1024]{1,0:T(8,128)(2,1)S(1)}, u32[]{:S(2)}, u32[]{:S(2)}) %collective-permute-start.13) | collective-permute-done | bytes 360480 | tf_op jit(solution)/shard_map/ppermute | solution.py:476
  135.5 0.0 collective-permute-done.14.refs_7_
  135.5 1.8 all-gather.2.cloned.1.call-done
  137.3 8.8 %feed_first.1 = (bf16[176,1024]{1,0:T(8,128)(2,1)S(1)}, bf16[176,1024]{1,0:T(8,128)(2,1)S(1)}, bf16[11,32,2,64,128]{4,3,2,1,0:T(8,128)(2,1)S(1)}, bf16[32,11,64,128]{3,2,1,0:T(8,128)(2,1)S(1)}) custom-call(s32[2]{0:T(128)S(1)} %pad_add_fusion.me_ref.refs_0_, bf16[16,2048]{1,0:T(8,128)(2,1)S(1)} %broadcast_select_fusion.refs_1_, ...), custom_call_target="tpu_custom_call" | custom-call | flops 3045064704 | bytes 18743296 | tf_op jit(solution)/shard_map/feed_first/pallas_call | solution.py:328
  146.1 1.3 collective-permute-start.15
  147.4 1.5 collective-permute-start.16
  148.9 10.5 %feed_sides.1 = (bf16[176,1024]{1,0:T(8,128)(2,1)S(1)}, bf16[176,1024]{1,0:T(8,128)(2,1)S(1)}, bf16[176,1024]{1,0:T(8,128)(2,1)S(1)}, bf16[176,1024]{1,0:T(8,128)(2,1)S(1)}) custom-call(s32[2]{0:T(128)S(1)} %pad_add_fusion.me_ref.refs_0_, bf16[16,2048]{1,0:T(8,128)(2,1)S(1)} %broadcast_select_fusion.refs_1_, ...), custom_call_target="tpu_custom_call" | custom-call | flops 6090129408 | bytes 20185088 | tf_op jit(solution)/shard_map/feed_sides/pallas_call | solution.py:328
  159.5 0.1 collective-permute-start.18
  159.6 2.6 %collective-permute-start.19 = (bf16[176,1024]{1,0:T(8,128)(2,1)S(1)}, bf16[176,1024]{1,0:T(8,128)(2,1)S(1)}, u32[]{:S(2)}, u32[]{:S(2)}) collective-permute-start(bf16[176,1024]{1,0:T(8,128)(2,1)S(1)} %get-tuple-element.54), channel_id=1, source_target_pairs={{0,3},{1,0},{2,1},{3,2},{4,7},{5,4},{6,5},{7,6},{8,11},{9,8},{10,9... | collective-permute-start | bytes 1081352 | tf_op jit(solution)/shard_map/ppermute | solution.py:476
  162.2 0.0 collective-permute-done.15.low_ref
  162.2 0.0 collective-permute-done.16.high_ref
  162.2 0.2 join.3
  162.5 0.1 collective-permute-start.17
  162.6 0.0 copy-start.1
  162.6 0.0 copy-start.7
  162.6 2.6 %collective-permute-start.20 = (bf16[176,1024]{1,0:T(8,128)(2,1)S(1)}, bf16[176,1024]{1,0:T(8,128)(2,1)S(1)}, u32[]{:S(2)}, u32[]{:S(2)}) collective-permute-start(bf16[176,1024]{1,0:T(8,128)(2,1)S(1)} %get-tuple-element.55), channel_id=1, source_target_pairs={{0,3},{1,0},{2,1},{3,2},{4,7},{5,4},{6,5},{7,6},{8,11},{9,8},{10,9... | collective-permute-start | bytes 1081352 | tf_op jit(solution)/shard_map/ppermute | solution.py:476
  165.3 7.0 %feed_own.1.refs_0_ = bf16[176,2048]{1,0:T(8,128)(2,1)S(1)} custom-call(s32[2]{0:T(128)S(1)} %pad_add_fusion.me_ref.refs_0_, bf16[16,2048]{1,0:T(8,128)(2,1)S(1)} %broadcast_select_fusion.refs_1_, bf16[176,1024]{1,0:T(8,128)(2,1)S(1)} %get-tuple-element.44.refs_2_, bf16[176,1024]{1,0:T(8,128)(2,1)S(1)} %get-tuple-element.45.refs_3_, ...), custom_call_target="tpu_custom_call" | custom-call | flops 3045064704 | bytes 18743296 | tf_op jit(solution)/shard_map/feed_own/pallas_call | solution.py:328
  172.3 0.0 collective-permute-done.18.refs_2_
  172.3 0.0 collective-permute-done.19.refs_3_
  172.3 5.4 %collective-permute-done.17.refs_1_ = bf16[176,1024]{1,0:T(8,128)(2,1)S(1)} collective-permute-done((bf16[176,1024]{1,0:T(8,128)(2,1)S(1)}, bf16[176,1024]{1,0:T(8,128)(2,1)S(1)}, u32[]{:S(2)}, u32[]{:S(2)}) %collective-permute-start.17) | collective-permute-done | bytes 360480 | tf_op jit(solution)/shard_map/ppermute | solution.py:476
  177.7 2.4 %last.1 = bf16[176,2048]{1,0:T(8,128)(2,1)} custom-call(bf16[176,2048]{1,0:T(8,128)(2,1)S(1)} %feed_own.1.refs_0_, bf16[176,1024]{1,0:T(8,128)(2,1)S(1)} %collective-permute-done.17.refs_1_, bf16[176,1024]{1,0:T(8,128)(2,1)S(1)} %collective-permute-done.18.refs_2_, bf16[176,1024]{1,0:T(8,128)(2,1)S(1)} %collective-permute-done.19.refs_3_, ...), custom_call_target="tpu_custom_call" | custom-call | tf_op jit(solution)/shard_map/last/pallas_call | solution.py:444
  (22 shorter events, 0.1 us)
Async XLA Ops:
  6.5 58.8 %copy-start = (bf16[512,2048]{1,0:T(8,128)(2,1)S(1)}, bf16[512,2048]{1,0:T(8,128)(2,1)}, u32[]{:S(2)}) copy-start(bf16[512,2048]{1,0:T(8,128)(2,1)} %w_ref.3) | copy-start | bytes 6291460
  6.5 130.8 %all-gather.2.cloned.1.call-start = ((), (), s32[]{:S(2)}) async-start(), calls=%async_computation.1 | async-start | bytes 17842176 | tf_op jit(solution)/shard_map/all_gather | solution.py:523
  9.4 22.4 %collective-permute-start = (bf16[8,512]{1,0:T(8,128)(2,1)S(1)}, bf16[8,512]{1,0:T(8,128)(2,1)S(1)}, u32[]{:S(2)}, u32[]{:S(2)}) collective-permute-start(bf16[8,512]{1,0:T(8,128)(2,1)S(1)} %slice.21), channel_id=1, source_target_pairs={{0,4},{4,8},{8,12},{12,16},{16,20},{20,24},{24,28},{28,32},{32,36}... | collective-permute-start | bytes 24584 | tf_op jit(solution)/shard_map/ppermute | solution.py:490
  31.8 0.6 copy-start.8
  39.2 26.2 %all-to-all-start = ((f32[32,8,128]{2,1,0:T(8,128)}), f32[32,8,128]{2,1,0:T(8,128)S(1)}, u32[]{:S(2)}, u32[]{:S(2)}) async-start(f32[32,8,128]{2,1,0:T(8,128)} %get-tuple-element.31), calls=%async_computation | async-start | bytes 262144 | tf_op jit(solution)/shard_map/all_to_all | solution.py:494
  65.4 0.8 copy-start.2
  68.5 10.6 %collective-permute-start.1 = (bf16[176,1024]{1,0:T(8,128)(2,1)S(1)}, bf16[176,1024]{1,0:T(8,128)(2,1)S(1)}, u32[]{:S(2)}, u32[]{:S(2)}) collective-permute-start(bf16[176,1024]{1,0:T(8,128)(2,1)S(1)} %get-tuple-element.37), channel_id=1, source_target_pairs={{0,1},{1,2},{2,3},{3,0},{4,5},{5,6},{6,7},{7,4},{8,9},{9,10},{10,1... | collective-permute-start | bytes 1081352 | tf_op jit(solution)/shard_map/ppermute | solution.py:476
  70.0 25.1 %copy-start.5 = (f32[2048]{0:T(1024)S(1)}, f32[2048]{0:T(1024)}, u32[]{:S(2)}) copy-start(f32[2048]{0:T(1024)} %param.26) | copy-start | bytes 24580
  70.0 25.1 %copy-start.6 = (f32[2048]{0:T(1024)S(1)}, f32[2048]{0:T(1024)}, u32[]{:S(2)}) copy-start(f32[2048]{0:T(1024)} %param.27) | copy-start | bytes 24580
  70.0 9.2 %collective-permute-start.2 = (bf16[176,1024]{1,0:T(8,128)(2,1)S(1)}, bf16[176,1024]{1,0:T(8,128)(2,1)S(1)}, u32[]{:S(2)}, u32[]{:S(2)}) collective-permute-start(bf16[176,1024]{1,0:T(8,128)(2,1)S(1)} %get-tuple-element.39), channel_id=1, source_target_pairs={{0,3},{1,0},{2,1},{3,2},{4,7},{5,4},{6,5},{7,6},{8,11},{9,8},{10,9... | collective-permute-start | bytes 1081352 | tf_op jit(solution)/shard_map/ppermute | solution.py:476
  75.5 11.8 %collective-permute-start.4 = (bf16[176,1024]{1,0:T(8,128)(2,1)S(1)}, bf16[176,1024]{1,0:T(8,128)(2,1)S(1)}, u32[]{:S(2)}, u32[]{:S(2)}) collective-permute-start(bf16[176,1024]{1,0:T(8,128)(2,1)S(1)} %get-tuple-element.41), channel_id=1, source_target_pairs={{0,1},{1,2},{2,3},{3,0},{4,5},{5,6},{6,7},{7,4},{8,9},{9,10},{10,1... | collective-permute-start | bytes 1081352 | tf_op jit(solution)/shard_map/ppermute | solution.py:476
  75.6 11.7 %collective-permute-start.5 = (bf16[176,1024]{1,0:T(8,128)(2,1)S(1)}, bf16[176,1024]{1,0:T(8,128)(2,1)S(1)}, u32[]{:S(2)}, u32[]{:S(2)}) collective-permute-start(bf16[176,1024]{1,0:T(8,128)(2,1)S(1)} %get-tuple-element.42), channel_id=1, source_target_pairs={{0,3},{1,0},{2,1},{3,2},{4,7},{5,4},{6,5},{7,6},{8,11},{9,8},{10,9... | collective-permute-start | bytes 1081352 | tf_op jit(solution)/shard_map/ppermute | solution.py:476
  79.3 15.7 %collective-permute-start.3 = (bf16[176,1024]{1,0:T(8,128)(2,1)S(1)}, bf16[176,1024]{1,0:T(8,128)(2,1)S(1)}, u32[]{:S(2)}, u32[]{:S(2)}) collective-permute-start(bf16[176,1024]{1,0:T(8,128)(2,1)S(1)} %get-tuple-element.40), channel_id=1, source_target_pairs={{0,1},{1,2},{2,3},{3,0},{4,5},{5,6},{6,7},{7,4},{8,9},{9,10},{10,1... | collective-permute-start | bytes 1081352 | tf_op jit(solution)/shard_map/ppermute | solution.py:476
  80.4 14.6 %collective-permute-start.6 = (bf16[176,1024]{1,0:T(8,128)(2,1)S(1)}, bf16[176,1024]{1,0:T(8,128)(2,1)S(1)}, u32[]{:S(2)}, u32[]{:S(2)}) collective-permute-start(bf16[176,1024]{1,0:T(8,128)(2,1)S(1)} %get-tuple-element.43), channel_id=1, source_target_pairs={{0,3},{1,0},{2,1},{3,2},{4,7},{5,4},{6,5},{7,6},{8,11},{9,8},{10,9... | collective-permute-start | bytes 1081352 | tf_op jit(solution)/shard_map/ppermute | solution.py:476
  95.0 42.3 %copy-start.3 = (bf16[3,1408]{1,0:T(4,128)(2,1)S(1)}, bf16[3,1408]{1,0:T(4,128)(2,1)}, u32[]{:S(2)}) copy-start(bf16[3,1408]{1,0:T(4,128)(2,1)} %refs_12_.5) | copy-start | bytes 25348
  95.0 42.3 %copy-start.4 = (bf16[3,1408]{1,0:T(4,128)(2,1)S(1)}, bf16[3,1408]{1,0:T(4,128)(2,1)}, u32[]{:S(2)}) copy-start(bf16[3,1408]{1,0:T(4,128)(2,1)} %refs_13_.3) | copy-start | bytes 25348
  100.2 9.2 %collective-permute-start.10 = (bf16[176,1024]{1,0:T(8,128)(2,1)S(1)}, bf16[176,1024]{1,0:T(8,128)(2,1)S(1)}, u32[]{:S(2)}, u32[]{:S(2)}) collective-permute-start(bf16[176,1024]{1,0:T(8,128)(2,1)S(1)} %get-tuple-element.44.refs_2_), channel_id=1, source_target_pairs={{0,3},{1,0},{2,1},{3,2},{4,7},{5,4},{6,5},{7,6},{8,11},{9,8},{10,9... | collective-permute-start | bytes 1081352 | tf_op jit(solution)/shard_map/ppermute | solution.py:476
  102.9 9.7 %collective-permute-start.8 = (bf16[176,1024]{1,0:T(8,128)(2,1)S(1)}, bf16[176,1024]{1,0:T(8,128)(2,1)S(1)}, u32[]{:S(2)}, u32[]{:S(2)}) collective-permute-start(bf16[176,1024]{1,0:T(8,128)(2,1)S(1)} %get-tuple-element.44.refs_2_), channel_id=1, source_target_pairs={{0,1},{1,2},{2,3},{3,0},{4,5},{5,6},{6,7},{7,4},{8,9},{9,10},{10,1... | collective-permute-start | bytes 1081352 | tf_op jit(solution)/shard_map/ppermute | solution.py:476
  102.9 14.2 %collective-permute-start.11 = (bf16[176,1024]{1,0:T(8,128)(2,1)S(1)}, bf16[176,1024]{1,0:T(8,128)(2,1)S(1)}, u32[]{:S(2)}, u32[]{:S(2)}) collective-permute-start(bf16[176,1024]{1,0:T(8,128)(2,1)S(1)} %get-tuple-element.45.refs_3_), channel_id=1, source_target_pairs={{0,3},{1,0},{2,1},{3,2},{4,7},{5,4},{6,5},{7,6},{8,11},{9,8},{10,9... | collective-permute-start | bytes 1081352 | tf_op jit(solution)/shard_map/ppermute | solution.py:476
  105.6 14.7 %collective-permute-start.9 = (bf16[176,1024]{1,0:T(8,128)(2,1)S(1)}, bf16[176,1024]{1,0:T(8,128)(2,1)S(1)}, u32[]{:S(2)}, u32[]{:S(2)}) collective-permute-start(bf16[176,1024]{1,0:T(8,128)(2,1)S(1)} %get-tuple-element.45.refs_3_), channel_id=1, source_target_pairs={{0,1},{1,2},{2,3},{3,0},{4,5},{5,6},{6,7},{7,4},{8,9},{9,10},{10,1... | collective-permute-start | bytes 1081352 | tf_op jit(solution)/shard_map/ppermute | solution.py:476
  120.4 6.9 %collective-permute-start.12 = (bf16[16,2048]{1,0:T(8,128)(2,1)S(1)}, bf16[16,2048]{1,0:T(8,128)(2,1)S(1)}, u32[]{:S(2)}, u32[]{:S(2)}) collective-permute-start(bf16[16,2048]{1,0:T(8,128)(2,1)S(1)} %get-tuple-element.57), channel_id=1, source_target_pairs={{0,4},{2,6},{3,7},{4,8},{6,10},{7,11},{8,12},{10,14},{11,15},{12,1... | collective-permute-start | bytes 196616 | tf_op jit(solution)/shard_map/ppermute | solution.py:552
  123.8 3.5 %collective-permute-start.7 = (bf16[16,2048]{1,0:T(8,128)(2,1)S(1)}, bf16[16,2048]{1,0:T(8,128)(2,1)S(1)}, u32[]{:S(2)}, u32[]{:S(2)}) collective-permute-start(bf16[16,2048]{1,0:T(8,128)(2,1)S(1)} %get-tuple-element.58), channel_id=1, source_target_pairs={{3,5},{7,9},{11,13},{15,17},{19,21},{23,25},{27,29},{31,33},{35,37... | collective-permute-start | bytes 196616 | tf_op jit(solution)/shard_map/ppermute | solution.py:551
  124.4 11.1 %collective-permute-start.13 = (bf16[176,1024]{1,0:T(8,128)(2,1)S(1)}, bf16[176,1024]{1,0:T(8,128)(2,1)S(1)}, u32[]{:S(2)}, u32[]{:S(2)}) collective-permute-start(bf16[176,1024]{1,0:T(8,128)(2,1)S(1)} %collective-permute-done.8.refs_8_), channel_id=1, source_target_pairs={{0,1},{1,2},{2,3},{3,0},{4,5},{5,6},{6,7},{7,4},{8,9},{9,10},{10,1... | collective-permute-start | bytes 1081352 | tf_op jit(solution)/shard_map/ppermute | solution.py:476
  124.6 11.0 %collective-permute-start.14 = (bf16[176,1024]{1,0:T(8,128)(2,1)S(1)}, bf16[176,1024]{1,0:T(8,128)(2,1)S(1)}, u32[]{:S(2)}, u32[]{:S(2)}) collective-permute-start(bf16[176,1024]{1,0:T(8,128)(2,1)S(1)} %collective-permute-done.11.refs_5_), channel_id=1, source_target_pairs={{0,3},{1,0},{2,1},{3,2},{4,7},{5,4},{6,5},{7,6},{8,11},{9,8},{10,9... | collective-permute-start | bytes 1081352 | tf_op jit(solution)/shard_map/ppermute | solution.py:476
  146.1 16.1 %collective-permute-start.15 = (bf16[176,1024]{1,0:T(8,128)(2,1)S(1)}, bf16[176,1024]{1,0:T(8,128)(2,1)S(1)}, u32[]{:S(2)}, u32[]{:S(2)}) collective-permute-start(bf16[176,1024]{1,0:T(8,128)(2,1)S(1)} %get-tuple-element.49), channel_id=1, source_target_pairs={{0,1},{1,2},{2,3},{3,0},{4,5},{5,6},{6,7},{7,4},{8,9},{9,10},{10,1... | collective-permute-start | bytes 1081352 | tf_op jit(solution)/shard_map/ppermute | solution.py:476
  147.4 14.8 %collective-permute-start.16 = (bf16[176,1024]{1,0:T(8,128)(2,1)S(1)}, bf16[176,1024]{1,0:T(8,128)(2,1)S(1)}, u32[]{:S(2)}, u32[]{:S(2)}) collective-permute-start(bf16[176,1024]{1,0:T(8,128)(2,1)S(1)} %get-tuple-element.51), channel_id=1, source_target_pairs={{0,3},{1,0},{2,1},{3,2},{4,7},{5,4},{6,5},{7,6},{8,11},{9,8},{10,9... | collective-permute-start | bytes 1081352 | tf_op jit(solution)/shard_map/ppermute | solution.py:476
  159.5 12.8 %collective-permute-start.18 = (bf16[176,1024]{1,0:T(8,128)(2,1)S(1)}, bf16[176,1024]{1,0:T(8,128)(2,1)S(1)}, u32[]{:S(2)}, u32[]{:S(2)}) collective-permute-start(bf16[176,1024]{1,0:T(8,128)(2,1)S(1)} %get-tuple-element.53), channel_id=1, source_target_pairs={{0,1},{1,2},{2,3},{3,0},{4,5},{5,6},{6,7},{7,4},{8,9},{9,10},{10,1... | collective-permute-start | bytes 1081352 | tf_op jit(solution)/shard_map/ppermute | solution.py:476
  159.6 12.7 %collective-permute-start.19 = (bf16[176,1024]{1,0:T(8,128)(2,1)S(1)}, bf16[176,1024]{1,0:T(8,128)(2,1)S(1)}, u32[]{:S(2)}, u32[]{:S(2)}) collective-permute-start(bf16[176,1024]{1,0:T(8,128)(2,1)S(1)} %get-tuple-element.54), channel_id=1, source_target_pairs={{0,3},{1,0},{2,1},{3,2},{4,7},{5,4},{6,5},{7,6},{8,11},{9,8},{10,9... | collective-permute-start | bytes 1081352 | tf_op jit(solution)/shard_map/ppermute | solution.py:476
  162.5 15.2 %collective-permute-start.17 = (bf16[176,1024]{1,0:T(8,128)(2,1)S(1)}, bf16[176,1024]{1,0:T(8,128)(2,1)S(1)}, u32[]{:S(2)}, u32[]{:S(2)}) collective-permute-start(bf16[176,1024]{1,0:T(8,128)(2,1)S(1)} %get-tuple-element.52), channel_id=1, source_target_pairs={{0,1},{1,2},{2,3},{3,0},{4,5},{5,6},{6,7},{7,4},{8,9},{9,10},{10,1... | collective-permute-start | bytes 1081352 | tf_op jit(solution)/shard_map/ppermute | solution.py:476
  162.6 15.0 %copy-start.1 = (bf16[176,2048]{1,0:T(8,128)(2,1)S(1)}, bf16[176,2048]{1,0:T(8,128)(2,1)}, u32[]{:S(2)}) copy-start(bf16[176,2048]{1,0:T(8,128)(2,1)} %get-tuple-element.56.refs_5_) | copy-start | bytes 2162692
  162.6 15.0 %copy-start.7 = (f32[2048]{0:T(1024)S(1)}, f32[2048]{0:T(1024)}, u32[]{:S(2)}) copy-start(f32[2048]{0:T(1024)} %param.28) | copy-start | bytes 24580
  162.6 15.0 %collective-permute-start.20 = (bf16[176,1024]{1,0:T(8,128)(2,1)S(1)}, bf16[176,1024]{1,0:T(8,128)(2,1)S(1)}, u32[]{:S(2)}, u32[]{:S(2)}) collective-permute-start(bf16[176,1024]{1,0:T(8,128)(2,1)S(1)} %get-tuple-element.55), channel_id=1, source_target_pairs={{0,3},{1,0},{2,1},{3,2},{4,7},{5,4},{6,5},{7,6},{8,11},{9,8},{10,9... | collective-permute-start | bytes 1081352 | tf_op jit(solution)/shard_map/ppermute | solution.py:476
Sparse Core Ops, SparseCore 0:
  9.2 128.0 all-gather.1

commit v6 on v5

--- a/solution.py
+++ b/solution.py
@@ -6,6 +6,7 @@
 from jax.experimental import pallas as pl
 from jax.experimental.pallas import tpu as pltpu
 from jax.sharding import PartitionSpec as P
+
 
 EPS = 1e-06
 GATE_SCALE = 8.0
@@ -343,26 +344,33 @@
             transcendentals=count * rows * units,
         ),
         compiler_params=pltpu.CompilerParams(vmem_limit_bytes=12 * MIB),
-        name={OPPOSITE: "feed_first", SIDES: "feed_sides", OWN: "feed_own"}[turns],
     )(me, outside, *map(vm, halves[:4]), *halves[4:6], *map(vm, halves[6:]), *weights, gate_kernel, value_kernel)
 
 
-def pack_kernel(gate_ref, value_ref, turned_ref, out_ref):
+def pack_kernel(gate_ref, value_ref, turned_ref, out_ref, sems):
     chunks = gate_ref.shape[1] // LANES
+    copies = []
     for c in range(chunks):
-        lanes = slice(c * LANES, (c + 1) * LANES)
-        out_ref[2 * c] = gate_ref[:, lanes]
-        out_ref[2 * c + 1] = value_ref[:, lanes]
-        out_ref[2 * chunks + c] = turned_ref[:, lanes]
+        lanes = pl.ds(c * LANES, LANES)
+        for source, at in ((gate_ref, 2 * c), (value_ref, 2 * c + 1), (turned_ref, 2 * chunks + c)):
+            copies.append(pltpu.make_async_copy(source.at[:, lanes], out_ref.at[at], sems.at[at]))
+    for copy in copies:
+        copy.start()
+    for copy in copies:
+        copy.wait()
 
 
 def packed(gate, value, turned):
     rows, units = gate.shape
+    pieces = 3 * units // LANES
     return pl.pallas_call(
         pack_kernel,
-        out_shape=jax.ShapeDtypeStruct((3 * units // LANES, rows, LANES), jnp.bfloat16),
+        in_specs=[HERE] * 3,
+        out_specs=HERE,
+        out_shape=hbm_out((pieces, rows, LANES)),
+        scratch_shapes=[pltpu.SemaphoreType.DMA((pieces,))],
         name="pack",
-    )(gate, value, turned)
+    )(hbm(gate), hbm(value), hbm(turned))
 
 
 def scaled(v, gain):
@@ -392,17 +400,15 @@
 
 
 def mid_kernel(me_ref, *refs):
-    shares, (res_hbm, mix_ref, inner_ref, hidden_ref, low_ref, high_ref, res, sem) = refs[:5], refs[5:]
+    shares, (res_ref, mix_ref, inner_ref, hidden_ref, low_ref, high_ref) = refs[:5], refs[5:]
     rows, half = low_ref.shape
-    first = pl.multiple_of(me_ref[0] * rows, rows)
-    fetch = pltpu.make_async_copy(res_hbm.at[pl.ds(first, rows), :], res, sem)
-    fetch.start()
+    first = me_ref[0] * rows
     mix, inner = mix_ref[...], inner_ref[...]
-    fetch.wait()
 
     def body(at):
+        there = pl.ds(pl.multiple_of(first + at.start, HALO), HALO)
         hidden = (
-            res[at, :].astype(jnp.float32) + scaled(shares_sum(shares, at), mix)
+            res_ref[there, :].astype(jnp.float32) + scaled(shares_sum(shares, at), mix)
         ).astype(jnp.bfloat16)
         hidden_ref[at, :] = hidden
         normed = scaled(hidden.astype(jnp.float32), inner).astype(jnp.bfloat16)
@@ -416,16 +422,15 @@
     rows, width = shares[0].shape
     return pl.pallas_call(
         mid_kernel,
-        in_specs=[pl.BlockSpec(memory_space=pltpu.SMEM), *[VMEM] * 5, HERE, VMEM, VMEM],
+        in_specs=[pl.BlockSpec(memory_space=pltpu.SMEM), *[VMEM] * 8],
         out_specs=[VMEM] * 3,
         out_shape=[
             hbm_out((rows, width)),
             *[vm_out((rows, width // 2))] * 2,
         ],
-        scratch_shapes=[pltpu.VMEM((rows, width), jnp.bfloat16), pltpu.SemaphoreType.DMA],
         compiler_params=pltpu.CompilerParams(vmem_limit_bytes=12 * MIB),
         name="mid",
-    )(me, *map(vm, shares), hbm(residual), mix_gain, inner_gain)
+    )(me, *map(vm, shares), residual, mix_gain, inner_gain)
 
 
 def last_kernel(*refs):
@@ -488,6 +493,10 @@
 def from_behind(value, axis):
     count = lax.axis_size(axis)
     return lax.ppermute(value, axis, [(i, i + 1) for i in range(count - 1)])
+
+
+def tail_sent(value, pairs):
+    return lax.ppermute(value, ("sp", "tp"), pairs)
 
 
 def exchanged(tiles, axis):
@@ -548,10 +557,9 @@
     places = range(n_sp - 1)
     outside = jnp.where(
         tp_me == 1,
-        lax.ppermute(own_tail, ("sp", "tp"), [(s * n_tp + n_tp - 1, (s + 1) * n_tp + 1) for s in places]),
-        lax.ppermute(
+        tail_sent(own_tail, [(s * n_tp + n_tp - 1, (s + 1) * n_tp + 1) for s in places]),
+        tail_sent(
             final_tail,
-            ("sp", "tp"),
             [(s * n_tp + t, (s + 1) * n_tp + t) for s in places for t in (0, 2, 3)],
         ),
     )

time: 187 us -> 203 us (1.086)
  Pallas kernels: 49.4 us -> 64 us
    pallas_call x1, Pallas kernels: 2.12 us -> 17.8 us  [packed(): pl.pallas_call(pack_kernel, in_specs=[HERE] * 3, out_specs=HERE, out_shap...]
  transfers between devices with their start and end apart: 23 -> 23, of which waited for: 12 -> 12; matrix products, arithmetic and copies ran while one was open for 0% -> 0% of each run, Pallas kernels for 19% -> 17%
where the time goes in v6:
time: 203 us; the launch traced here: 202 us
  waiting for transfers between devices  78.9 us (39%)
  Pallas kernels  64 us (32%)
  starting transfers between devices  43.4 us (21%)
  between operations  13.7 us (7%)
  local copies, waits for them, and re-layouts  2.11 us (1%)
    ppermute x18, waiting for transfers between devices, turn(): lax.ppermute(value, axis, [(i, (i + steps) % count) for i in range(count)])  42.2 us
    pallas_call x3, Pallas kernels, feed(): pl.pallas_call(functools.partial(feed_kernel, turns=turns), in_specs=[pl....  26.3 us
    ppermute x18, starting transfers between devices, turn(): lax.ppermute(value, axis, [(i, (i + steps) % count) for i in range(count)])  25.3 us
    all_to_all x1, waiting for transfers between devices, exchanged(): return lax.all_to_all(tiles, axis, split_axis=0, concat_axis=0, tiled=True)  17.8 us
    pallas_call x1, Pallas kernels, packed(): pl.pallas_call(pack_kernel, in_specs=[HERE] * 3, out_specs=HERE, out_shap...  17.8 us
    ppermute x1, waiting for transfers between devices, from_behind(): return lax.ppermute(value, axis, [(i, i + 1) for i in range(count - 1)])  16.6 us
    all_to_all x1, starting transfers between devices, exchanged(): return lax.all_to_all(tiles, axis, split_axis=0, concat_axis=0, tiled=True)  8.19 us
    pallas_call x1, Pallas kernels, local_scan(): pl.pallas_call(scan_kernel, grid=(groups,), in_specs=[column(length), col...  6.79 us
  transfers between devices with their start and end apart: 23, of which 12 were waited for; matrix products, arithmetic and copies ran while one was open for 0% of the time, Pallas kernels for 17%

profile of v6, /device:TPU:33, one launch (start us, length us, event | category | flops | bytes accessed | tf_op | source)
XLA Modules:
  0.0 202.3 jit_solution(18233142235335360112)
XLA Ops:
  6.6 17.8 %pack.1 = bf16[33,64,128]{2,1,0:T(8,128)(2,1)} custom-call(bf16[64,1408]{1,0:T(8,128)(2,1)} %gate_ref.1, bf16[64,1408]{1,0:T(8,128)(2,1)} %value_ref.1, bf16[64,1408]{1,0:T(8,128)(2,1)} %bitcast.12), custom_call_target="tpu_custom_call" | custom-call | tf_op jit(solution)/shard_map/pack/pallas_call | solution.py:366
  24.3 0.1 all-gather.2.cloned.1.call-update
  24.4 0.7 slice.21
  25.1 5.7 %collective-permute-start = (bf16[8,512]{1,0:T(8,128)(2,1)S(1)}, bf16[8,512]{1,0:T(8,128)(2,1)S(1)}, u32[]{:S(2)}, u32[]{:S(2)}) collective-permute-start(bf16[8,512]{1,0:T(8,128)(2,1)S(1)} %slice.21), channel_id=1, source_target_pairs={{0,4},{4,8},{8,12},{12,16},{16,20},{20,24},{24,28},{28,32},{32,36}... | collective-permute-start | bytes 24584 | tf_op jit(solution)/shard_map/ppermute | solution.py:495
  30.8 16.6 %collective-permute-done.edge_ref = bf16[8,512]{1,0:T(8,128)(2,1)S(1)} collective-permute-done((bf16[8,512]{1,0:T(8,128)(2,1)S(1)}, bf16[8,512]{1,0:T(8,128)(2,1)S(1)}, u32[]{:S(2)}, u32[]{:S(2)}) %collective-permute-start) | collective-permute-done | bytes 8224 | tf_op jit(solution)/shard_map/ppermute | solution.py:495
  47.5 0.6 copy-done.9
  48.0 6.8 %local_scan.1 = (f32[704,512]{1,0:T(8,128)}, f32[704,512]{1,0:T(8,128)}, f32[2,8,512]{2,1,0:T(8,128)}, f32[32,8,128]{2,1,0:T(8,128)}) custom-call(bf16[704,512]{1,0:T(8,128)(2,1)} %x_ref.1, bf16[8,512]{1,0:T(8,128)(2,1)} %copy-done.9, bf16[4,512]{1,0:T(4,128)(2,1)} %taps_ref.1, bf16[4,128,128]{2,1,0:T(8,128)(2,1)} %rmap_ref.1, ...), custom_call_target="tpu_custom_call" | custom-call | tf_op jit(solution)/shard_map/local_scan/pallas_call | solution.py:96
  54.8 8.2 %all-to-all-start = ((f32[32,8,128]{2,1,0:T(8,128)}), f32[32,8,128]{2,1,0:T(8,128)S(1)}, u32[]{:S(2)}, u32[]{:S(2)}) async-start(f32[32,8,128]{2,1,0:T(8,128)} %get-tuple-element.31), calls=%async_computation | async-start | bytes 262144 | tf_op jit(solution)/shard_map/all_to_all | solution.py:503
  63.0 0.1 pad_add_fusion.me_ref.refs_0_
  63.1 17.8 %all-to-all-done.arrived = f32[32,8,128]{2,1,0:T(8,128)S(1)} async-done(((f32[32,8,128]{2,1,0:T(8,128)}), f32[32,8,128]{2,1,0:T(8,128)S(1)}, u32[]{:S(2)}, u32[]{:S(2)}) %all-to-all-start) | async-done | bytes 131104 | tf_op jit(solution)/shard_map/all_to_all | solution.py:503
  80.9 0.8 copy-done.3
  81.7 2.4 %branch_first.1 = (bf16[176,1024]{1,0:T(8,128)(2,1)S(1)}, bf16[176,1024]{1,0:T(8,128)(2,1)S(1)}) custom-call(s32[2]{0:T(128)S(1)} %pad_add_fusion.me_ref.refs_0_, f32[32,8,128]{2,1,0:T(8,128)S(1)} %all-to-all-done.arrived, f32[2,8,512]{2,1,0:T(8,128)S(1)} %copy-done.3, f32[704,512]{1,0:T(8,128)} %get-tuple-element.33.cum_hbm, ...), custom_call_target="tpu_custom_call" | custom-call | flops 369098752 | bytes 3719168 | tf_op jit(solution)/shard_map/branch_first/pallas_call | solution.py:201
  84.1 1.4 collective-permute-start.1
  85.5 1.8 collective-permute-start.2
  87.3 4.0 %branch_rest.1 = (bf16[176,1024]{1,0:T(8,128)(2,1)S(1)}, bf16[176,1024]{1,0:T(8,128)(2,1)S(1)}, bf16[176,1024]{1,0:T(8,128)(2,1)S(1)}, bf16[176,1024]{1,0:T(8,128)(2,1)S(1)}, bf16[176,2048]{1,0:T(8,128)(2,1)S(1)}) custom-call(s32[2]{0:T(128)S(1)} %pad_add_fusion.me_ref.refs_0_, f32[32,8,128]{2,1,0:T(8,128)S(1)} %all-to-all-done.arrived, ...), custom_call_target="tpu_custom_call" | custom-call | flops 1107296256 | bytes 6963200 | tf_op jit(solution)/shard_map/branch_rest/pallas_call | solution.py:201
  91.2 0.1 collective-permute-start.4
  91.4 2.6 %collective-permute-start.5 = (bf16[176,1024]{1,0:T(8,128)(2,1)S(1)}, bf16[176,1024]{1,0:T(8,128)(2,1)S(1)}, u32[]{:S(2)}, u32[]{:S(2)}) collective-permute-start(bf16[176,1024]{1,0:T(8,128)(2,1)S(1)} %get-tuple-element.42), channel_id=1, source_target_pairs={{0,3},{1,0},{2,1},{3,2},{4,7},{5,4},{6,5},{7,6},{8,11},{9,8},{10,9... | collective-permute-start | bytes 1081352 | tf_op jit(solution)/shard_map/ppermute | solution.py:481
  94.0 1.0 collective-permute-done.1.low_ref
  95.0 0.0 collective-permute-done.2.high_ref
  95.0 0.2 join.2
  95.2 0.9 collective-permute-start.3
  96.1 1.9 collective-permute-start.6
  98.0 4.9 %collective-permute-done.4.refs_2_ = bf16[176,1024]{1,0:T(8,128)(2,1)S(1)} collective-permute-done((bf16[176,1024]{1,0:T(8,128)(2,1)S(1)}, bf16[176,1024]{1,0:T(8,128)(2,1)S(1)}, u32[]{:S(2)}, u32[]{:S(2)}) %collective-permute-start.4) | collective-permute-done | bytes 360480 | tf_op jit(solution)/shard_map/ppermute | solution.py:481
  103.0 0.0 collective-permute-done.5.refs_3_
  103.0 7.7 %collective-permute-done.3.refs_1_ = bf16[176,1024]{1,0:T(8,128)(2,1)S(1)} collective-permute-done((bf16[176,1024]{1,0:T(8,128)(2,1)S(1)}, bf16[176,1024]{1,0:T(8,128)(2,1)S(1)}, u32[]{:S(2)}, u32[]{:S(2)}) %collective-permute-start.3) | collective-permute-done | bytes 360480 | tf_op jit(solution)/shard_map/ppermute | solution.py:481
  110.7 0.0 collective-permute-done.6.refs_4_
  110.7 0.0 copy-start.4
  110.7 0.0 copy-start.5
  110.7 4.0 %mid.1 = (bf16[176,2048]{1,0:T(8,128)(2,1)}, bf16[176,1024]{1,0:T(8,128)(2,1)S(1)}, bf16[176,1024]{1,0:T(8,128)(2,1)S(1)}) custom-call(s32[2]{0:T(128)S(1)} %pad_add_fusion.me_ref.refs_0_, bf16[176,2048]{1,0:T(8,128)(2,1)S(1)} %get-tuple-element.35.refs_0_, bf16[176,1024]{1,0:T(8,128)(2,1)S(1)} %collective-permute-done.3.refs_1_, ...), custom_call_target="tpu_custom_call" | custom-call | tf_op jit(solution)/shard_map/mid/pallas_call | solution.py:423
  114.7 2.7 %collective-permute-start.10 = (bf16[176,1024]{1,0:T(8,128)(2,1)S(1)}, bf16[176,1024]{1,0:T(8,128)(2,1)S(1)}, u32[]{:S(2)}, u32[]{:S(2)}) collective-permute-start(bf16[176,1024]{1,0:T(8,128)(2,1)S(1)} %get-tuple-element.44.refs_2_), channel_id=1, source_target_pairs={{0,3},{1,0},{2,1},{3,2},{4,7},{5,4},{6,5},{7,6},{8,11},{9,8},{10,9... | collective-permute-start | bytes 1081352 | tf_op jit(solution)/shard_map/ppermute | solution.py:481
  117.4 0.0 collective-permute-start.8
  117.4 2.7 %collective-permute-start.11 = (bf16[176,1024]{1,0:T(8,128)(2,1)S(1)}, bf16[176,1024]{1,0:T(8,128)(2,1)S(1)}, u32[]{:S(2)}, u32[]{:S(2)}) collective-permute-start(bf16[176,1024]{1,0:T(8,128)(2,1)S(1)} %get-tuple-element.45.refs_3_), channel_id=1, source_target_pairs={{0,3},{1,0},{2,1},{3,2},{4,7},{5,4},{6,5},{7,6},{8,11},{9,8},{10,9... | collective-permute-start | bytes 1081352 | tf_op jit(solution)/shard_map/ppermute | solution.py:481
  120.1 0.0 collective-permute-start.9
  120.1 3.7 %collective-permute-done.10.refs_4_ = bf16[176,1024]{1,0:T(8,128)(2,1)S(1)} collective-permute-done((bf16[176,1024]{1,0:T(8,128)(2,1)S(1)}, bf16[176,1024]{1,0:T(8,128)(2,1)S(1)}, u32[]{:S(2)}, u32[]{:S(2)}) %collective-permute-start.10) | collective-permute-done | bytes 360480 | tf_op jit(solution)/shard_map/ppermute | solution.py:481
  123.9 3.2 %collective-permute-done.8.refs_8_ = bf16[176,1024]{1,0:T(8,128)(2,1)S(1)} collective-permute-done((bf16[176,1024]{1,0:T(8,128)(2,1)S(1)}, bf16[176,1024]{1,0:T(8,128)(2,1)S(1)}, u32[]{:S(2)}, u32[]{:S(2)}) %collective-permute-start.8) | collective-permute-done | bytes 360480 | tf_op jit(solution)/shard_map/ppermute | solution.py:481
  127.1 4.5 %collective-permute-done.11.refs_5_ = bf16[176,1024]{1,0:T(8,128)(2,1)S(1)} collective-permute-done((bf16[176,1024]{1,0:T(8,128)(2,1)S(1)}, bf16[176,1024]{1,0:T(8,128)(2,1)S(1)}, u32[]{:S(2)}, u32[]{:S(2)}) %collective-permute-start.11) | collective-permute-done | bytes 360480 | tf_op jit(solution)/shard_map/ppermute | solution.py:481
  131.6 3.2 %collective-permute-done.9.refs_9_ = bf16[176,1024]{1,0:T(8,128)(2,1)S(1)} collective-permute-done((bf16[176,1024]{1,0:T(8,128)(2,1)S(1)}, bf16[176,1024]{1,0:T(8,128)(2,1)S(1)}, u32[]{:S(2)}, u32[]{:S(2)}) %collective-permute-start.9) | collective-permute-done | bytes 360480 | tf_op jit(solution)/shard_map/ppermute | solution.py:481
  134.9 3.6 %collective-permute-start.12 = (bf16[16,2048]{1,0:T(8,128)(2,1)S(1)}, bf16[16,2048]{1,0:T(8,128)(2,1)S(1)}, u32[]{:S(2)}, u32[]{:S(2)}) collective-permute-start(bf16[16,2048]{1,0:T(8,128)(2,1)S(1)} %get-tuple-element.57), channel_id=1, source_target_pairs={{0,4},{2,6},{3,7},{4,8},{6,10},{7,11},{8,12},{10,14},{11,15},{12,1... | collective-permute-start | bytes 196616 | tf_op jit(solution)/shard_map/ppermute | solution.py:499
  138.4 0.7 collective-permute-start.7
  139.1 0.1 collective-permute-start.13
  139.3 2.6 %collective-permute-start.14 = (bf16[176,1024]{1,0:T(8,128)(2,1)S(1)}, bf16[176,1024]{1,0:T(8,128)(2,1)S(1)}, u32[]{:S(2)}, u32[]{:S(2)}) collective-permute-start(bf16[176,1024]{1,0:T(8,128)(2,1)S(1)} %collective-permute-done.11.refs_5_), channel_id=1, source_target_pairs={{0,3},{1,0},{2,1},{3,2},{4,7},{5,4},{6,5},{7,6},{8,11},{9,8},{10,9... | collective-permute-start | bytes 1081352 | tf_op jit(solution)/shard_map/ppermute | solution.py:481
  141.9 0.0 collective-permute-done.12
  141.9 0.0 collective-permute-done.7
  141.9 8.5 %collective-permute-done.13.refs_6_ = bf16[176,1024]{1,0:T(8,128)(2,1)S(1)} collective-permute-done((bf16[176,1024]{1,0:T(8,128)(2,1)S(1)}, bf16[176,1024]{1,0:T(8,128)(2,1)S(1)}, u32[]{:S(2)}, u32[]{:S(2)}) %collective-permute-start.13) | collective-permute-done | bytes 360480 | tf_op jit(solution)/shard_map/ppermute | solution.py:481
  150.4 0.0 collective-permute-done.14.refs_7_
  150.4 2.2 %all-gather.2.cloned.1.call-done = bf16[1056,64,128]{2,1,0:T(8,128)(2,1)} async-done(((bf16[33,64,128]{2,1,0:T(8,128)(2,1)}), bf16[1056,64,128]{2,1,0:T(8,128)(2,1)}) %all-gather.2.cloned.1.call-update) | async-done | bytes 17301520 | tf_op jit(solution)/shard_map/all_gather | solution.py:532
  152.7 8.8 %shard_map.163 = (bf16[176,1024]{1,0:T(8,128)(2,1)S(1)}, bf16[176,1024]{1,0:T(8,128)(2,1)S(1)}, bf16[11,32,2,64,128]{4,3,2,1,0:T(8,128)(2,1)S(1)}, bf16[32,11,64,128]{3,2,1,0:T(8,128)(2,1)S(1)}) custom-call(s32[2]{0:T(128)S(1)} %pad_add_fusion.me_ref.refs_0_, bf16[16,2048]{1,0:T(8,128)(2,1)S(1)} %broadcast_select_fusion.refs_1_, ...), custom_call_target="tpu_custom_call" | custom-call | flops 3045064704 | bytes 18743296 | tf_op jit(solution)/shard_map/pallas_call | solution.py:329
  161.4 1.3 collective-permute-start.15
  162.7 1.5 collective-permute-start.16
  164.2 10.5 %shard_map.165 = (bf16[176,1024]{1,0:T(8,128)(2,1)S(1)}, bf16[176,1024]{1,0:T(8,128)(2,1)S(1)}, bf16[176,1024]{1,0:T(8,128)(2,1)S(1)}, bf16[176,1024]{1,0:T(8,128)(2,1)S(1)}) custom-call(s32[2]{0:T(128)S(1)} %pad_add_fusion.me_ref.refs_0_, bf16[16,2048]{1,0:T(8,128)(2,1)S(1)} %broadcast_select_fusion.refs_1_, ...), custom_call_target="tpu_custom_call" | custom-call | flops 6090129408 | bytes 20185088 | tf_op jit(solution)/shard_map/pallas_call | solution.py:329
  174.8 0.1 collective-permute-start.18
  174.9 2.6 %collective-permute-start.19 = (bf16[176,1024]{1,0:T(8,128)(2,1)S(1)}, bf16[176,1024]{1,0:T(8,128)(2,1)S(1)}, u32[]{:S(2)}, u32[]{:S(2)}) collective-permute-start(bf16[176,1024]{1,0:T(8,128)(2,1)S(1)} %get-tuple-element.54), channel_id=1, source_target_pairs={{0,3},{1,0},{2,1},{3,2},{4,7},{5,4},{6,5},{7,6},{8,11},{9,8},{10,9... | collective-permute-start | bytes 1081352 | tf_op jit(solution)/shard_map/ppermute | solution.py:481
  177.6 0.0 collective-permute-done.15.low_ref
  177.6 0.0 collective-permute-done.16.high_ref
  177.6 0.2 join.3
  177.8 0.1 collective-permute-start.17
  177.9 0.0 copy-start.2
  177.9 0.0 copy-start.8
  178.0 2.6 %collective-permute-start.20 = (bf16[176,1024]{1,0:T(8,128)(2,1)S(1)}, bf16[176,1024]{1,0:T(8,128)(2,1)S(1)}, u32[]{:S(2)}, u32[]{:S(2)}) collective-permute-start(bf16[176,1024]{1,0:T(8,128)(2,1)S(1)} %get-tuple-element.55), channel_id=1, source_target_pairs={{0,3},{1,0},{2,1},{3,2},{4,7},{5,4},{6,5},{7,6},{8,11},{9,8},{10,9... | collective-permute-start | bytes 1081352 | tf_op jit(solution)/shard_map/ppermute | solution.py:481
  180.6 7.0 %shard_map.164.refs_0_ = bf16[176,2048]{1,0:T(8,128)(2,1)S(1)} custom-call(s32[2]{0:T(128)S(1)} %pad_add_fusion.me_ref.refs_0_, bf16[16,2048]{1,0:T(8,128)(2,1)S(1)} %broadcast_select_fusion.refs_1_, bf16[176,1024]{1,0:T(8,128)(2,1)S(1)} %get-tuple-element.44.refs_2_, bf16[176,1024]{1,0:T(8,128)(2,1)S(1)} %get-tuple-element.45.refs_3_, ...), custom_call_target="tpu_custom_call" | custom-call | flops 3045064704 | bytes 18743296 | tf_op jit(solution)/shard_map/pallas_call | solution.py:329
  187.6 0.0 collective-permute-done.18.refs_2_
  187.6 0.0 collective-permute-done.19.refs_3_
  187.6 5.4 %collective-permute-done.17.refs_1_ = bf16[176,1024]{1,0:T(8,128)(2,1)S(1)} collective-permute-done((bf16[176,1024]{1,0:T(8,128)(2,1)S(1)}, bf16[176,1024]{1,0:T(8,128)(2,1)S(1)}, u32[]{:S(2)}, u32[]{:S(2)}) %collective-permute-start.17) | collective-permute-done | bytes 360480 | tf_op jit(solution)/shard_map/ppermute | solution.py:481
  193.0 2.4 %last.1 = bf16[176,2048]{1,0:T(8,128)(2,1)} custom-call(bf16[176,2048]{1,0:T(8,128)(2,1)S(1)} %shard_map.164.refs_0_, bf16[176,1024]{1,0:T(8,128)(2,1)S(1)} %collective-permute-done.17.refs_1_, bf16[176,1024]{1,0:T(8,128)(2,1)S(1)} %collective-permute-done.18.refs_2_, bf16[176,1024]{1,0:T(8,128)(2,1)S(1)} %collective-permute-done.19.refs_3_, ...), custom_call_target="tpu_custom_call" | custom-call | tf_op jit(solution)/shard_map/last/pallas_call | solution.py:449
  (24 shorter events, 0.1 us)
Async XLA Ops:
  6.5 74.4 %copy-start = (bf16[512,2048]{1,0:T(8,128)(2,1)S(1)}, bf16[512,2048]{1,0:T(8,128)(2,1)}, u32[]{:S(2)}) copy-start(bf16[512,2048]{1,0:T(8,128)(2,1)} %w_ref.3) | copy-start | bytes 6291460
  6.5 146.1 %all-gather.2.cloned.1.call-start = ((), (), s32[]{:S(2)}) async-start(), calls=%async_computation.1 | async-start | bytes 17842176 | tf_op jit(solution)/shard_map/all_gather | solution.py:532
  25.1 22.4 %collective-permute-start = (bf16[8,512]{1,0:T(8,128)(2,1)S(1)}, bf16[8,512]{1,0:T(8,128)(2,1)S(1)}, u32[]{:S(2)}, u32[]{:S(2)}) collective-permute-start(bf16[8,512]{1,0:T(8,128)(2,1)S(1)} %slice.21), channel_id=1, source_target_pairs={{0,4},{4,8},{8,12},{12,16},{16,20},{20,24},{24,28},{28,32},{32,36}... | collective-permute-start | bytes 24584 | tf_op jit(solution)/shard_map/ppermute | solution.py:495
  47.5 0.6 copy-start.9
  54.8 26.1 %all-to-all-start = ((f32[32,8,128]{2,1,0:T(8,128)}), f32[32,8,128]{2,1,0:T(8,128)S(1)}, u32[]{:S(2)}, u32[]{:S(2)}) async-start(f32[32,8,128]{2,1,0:T(8,128)} %get-tuple-element.31), calls=%async_computation | async-start | bytes 262144 | tf_op jit(solution)/shard_map/all_to_all | solution.py:503
  80.9 0.8 copy-start.3
  84.1 10.9 %collective-permute-start.1 = (bf16[176,1024]{1,0:T(8,128)(2,1)S(1)}, bf16[176,1024]{1,0:T(8,128)(2,1)S(1)}, u32[]{:S(2)}, u32[]{:S(2)}) collective-permute-start(bf16[176,1024]{1,0:T(8,128)(2,1)S(1)} %get-tuple-element.37), channel_id=1, source_target_pairs={{0,1},{1,2},{2,3},{3,0},{4,5},{5,6},{6,7},{7,4},{8,9},{9,10},{10,1... | collective-permute-start | bytes 1081352 | tf_op jit(solution)/shard_map/ppermute | solution.py:481
  85.5 25.2 %copy-start.1 = (bf16[704,2048]{1,0:T(8,128)(2,1)S(1)}, bf16[704,2048]{1,0:T(8,128)(2,1)}, u32[]{:S(2)}) copy-start(bf16[704,2048]{1,0:T(8,128)(2,1)} %refs_5_.1) | copy-start | bytes 8650756
  85.5 25.2 %copy-start.6 = (f32[2048]{0:T(1024)S(1)}, f32[2048]{0:T(1024)}, u32[]{:S(2)}) copy-start(f32[2048]{0:T(1024)} %param.26) | copy-start | bytes 24580
  85.5 25.2 %copy-start.7 = (f32[2048]{0:T(1024)S(1)}, f32[2048]{0:T(1024)}, u32[]{:S(2)}) copy-start(f32[2048]{0:T(1024)} %param.27) | copy-start | bytes 24580
  85.5 9.5 %collective-permute-start.2 = (bf16[176,1024]{1,0:T(8,128)(2,1)S(1)}, bf16[176,1024]{1,0:T(8,128)(2,1)S(1)}, u32[]{:S(2)}, u32[]{:S(2)}) collective-permute-start(bf16[176,1024]{1,0:T(8,128)(2,1)S(1)} %get-tuple-element.39), channel_id=1, source_target_pairs={{0,3},{1,0},{2,1},{3,2},{4,7},{5,4},{6,5},{7,6},{8,11},{9,8},{10,9... | collective-permute-start | bytes 1081352 | tf_op jit(solution)/shard_map/ppermute | solution.py:481
  91.2 11.7 %collective-permute-start.4 = (bf16[176,1024]{1,0:T(8,128)(2,1)S(1)}, bf16[176,1024]{1,0:T(8,128)(2,1)S(1)}, u32[]{:S(2)}, u32[]{:S(2)}) collective-permute-start(bf16[176,1024]{1,0:T(8,128)(2,1)S(1)} %get-tuple-element.41), channel_id=1, source_target_pairs={{0,1},{1,2},{2,3},{3,0},{4,5},{5,6},{6,7},{7,4},{8,9},{9,10},{10,1... | collective-permute-start | bytes 1081352 | tf_op jit(solution)/shard_map/ppermute | solution.py:481
  91.4 11.6 %collective-permute-start.5 = (bf16[176,1024]{1,0:T(8,128)(2,1)S(1)}, bf16[176,1024]{1,0:T(8,128)(2,1)S(1)}, u32[]{:S(2)}, u32[]{:S(2)}) collective-permute-start(bf16[176,1024]{1,0:T(8,128)(2,1)S(1)} %get-tuple-element.42), channel_id=1, source_target_pairs={{0,3},{1,0},{2,1},{3,2},{4,7},{5,4},{6,5},{7,6},{8,11},{9,8},{10,9... | collective-permute-start | bytes 1081352 | tf_op jit(solution)/shard_map/ppermute | solution.py:481
  95.2 15.5 %collective-permute-start.3 = (bf16[176,1024]{1,0:T(8,128)(2,1)S(1)}, bf16[176,1024]{1,0:T(8,128)(2,1)S(1)}, u32[]{:S(2)}, u32[]{:S(2)}) collective-permute-start(bf16[176,1024]{1,0:T(8,128)(2,1)S(1)} %get-tuple-element.40), channel_id=1, source_target_pairs={{0,1},{1,2},{2,3},{3,0},{4,5},{5,6},{6,7},{7,4},{8,9},{9,10},{10,1... | collective-permute-start | bytes 1081352 | tf_op jit(solution)/shard_map/ppermute | solution.py:481
  96.1 14.6 %collective-permute-start.6 = (bf16[176,1024]{1,0:T(8,128)(2,1)S(1)}, bf16[176,1024]{1,0:T(8,128)(2,1)S(1)}, u32[]{:S(2)}, u32[]{:S(2)}) collective-permute-start(bf16[176,1024]{1,0:T(8,128)(2,1)S(1)} %get-tuple-element.43), channel_id=1, source_target_pairs={{0,3},{1,0},{2,1},{3,2},{4,7},{5,4},{6,5},{7,6},{8,11},{9,8},{10,9... | collective-permute-start | bytes 1081352 | tf_op jit(solution)/shard_map/ppermute | solution.py:481
  110.7 42.0 %copy-start.4 = (bf16[3,1408]{1,0:T(4,128)(2,1)S(1)}, bf16[3,1408]{1,0:T(4,128)(2,1)}, u32[]{:S(2)}) copy-start(bf16[3,1408]{1,0:T(4,128)(2,1)} %refs_12_.5) | copy-start | bytes 25348
  110.7 41.9 %copy-start.5 = (bf16[3,1408]{1,0:T(4,128)(2,1)S(1)}, bf16[3,1408]{1,0:T(4,128)(2,1)}, u32[]{:S(2)}) copy-start(bf16[3,1408]{1,0:T(4,128)(2,1)} %refs_13_.3) | copy-start | bytes 25348
  114.7 9.1 %collective-permute-start.10 = (bf16[176,1024]{1,0:T(8,128)(2,1)S(1)}, bf16[176,1024]{1,0:T(8,128)(2,1)S(1)}, u32[]{:S(2)}, u32[]{:S(2)}) collective-permute-start(bf16[176,1024]{1,0:T(8,128)(2,1)S(1)} %get-tuple-element.44.refs_2_), channel_id=1, source_target_pairs={{0,3},{1,0},{2,1},{3,2},{4,7},{5,4},{6,5},{7,6},{8,11},{9,8},{10,9... | collective-permute-start | bytes 1081352 | tf_op jit(solution)/shard_map/ppermute | solution.py:481
  117.4 9.7 %collective-permute-start.8 = (bf16[176,1024]{1,0:T(8,128)(2,1)S(1)}, bf16[176,1024]{1,0:T(8,128)(2,1)S(1)}, u32[]{:S(2)}, u32[]{:S(2)}) collective-permute-start(bf16[176,1024]{1,0:T(8,128)(2,1)S(1)} %get-tuple-element.44.refs_2_), channel_id=1, source_target_pairs={{0,1},{1,2},{2,3},{3,0},{4,5},{5,6},{6,7},{7,4},{8,9},{9,10},{10,1... | collective-permute-start | bytes 1081352 | tf_op jit(solution)/shard_map/ppermute | solution.py:481
  117.4 14.1 %collective-permute-start.11 = (bf16[176,1024]{1,0:T(8,128)(2,1)S(1)}, bf16[176,1024]{1,0:T(8,128)(2,1)S(1)}, u32[]{:S(2)}, u32[]{:S(2)}) collective-permute-start(bf16[176,1024]{1,0:T(8,128)(2,1)S(1)} %get-tuple-element.45.refs_3_), channel_id=1, source_target_pairs={{0,3},{1,0},{2,1},{3,2},{4,7},{5,4},{6,5},{7,6},{8,11},{9,8},{10,9... | collective-permute-start | bytes 1081352 | tf_op jit(solution)/shard_map/ppermute | solution.py:481
  120.1 14.7 %collective-permute-start.9 = (bf16[176,1024]{1,0:T(8,128)(2,1)S(1)}, bf16[176,1024]{1,0:T(8,128)(2,1)S(1)}, u32[]{:S(2)}, u32[]{:S(2)}) collective-permute-start(bf16[176,1024]{1,0:T(8,128)(2,1)S(1)} %get-tuple-element.45.refs_3_), channel_id=1, source_target_pairs={{0,1},{1,2},{2,3},{3,0},{4,5},{5,6},{6,7},{7,4},{8,9},{9,10},{10,1... | collective-permute-start | bytes 1081352 | tf_op jit(solution)/shard_map/ppermute | solution.py:481
  134.9 7.1 %collective-permute-start.12 = (bf16[16,2048]{1,0:T(8,128)(2,1)S(1)}, bf16[16,2048]{1,0:T(8,128)(2,1)S(1)}, u32[]{:S(2)}, u32[]{:S(2)}) collective-permute-start(bf16[16,2048]{1,0:T(8,128)(2,1)S(1)} %get-tuple-element.57), channel_id=1, source_target_pairs={{0,4},{2,6},{3,7},{4,8},{6,10},{7,11},{8,12},{10,14},{11,15},{12,1... | collective-permute-start | bytes 196616 | tf_op jit(solution)/shard_map/ppermute | solution.py:499
  138.4 3.5 %collective-permute-start.7 = (bf16[16,2048]{1,0:T(8,128)(2,1)S(1)}, bf16[16,2048]{1,0:T(8,128)(2,1)S(1)}, u32[]{:S(2)}, u32[]{:S(2)}) collective-permute-start(bf16[16,2048]{1,0:T(8,128)(2,1)S(1)} %get-tuple-element.58), channel_id=1, source_target_pairs={{3,5},{7,9},{11,13},{15,17},{19,21},{23,25},{27,29},{31,33},{35,37... | collective-permute-start | bytes 196616 | tf_op jit(solution)/shard_map/ppermute | solution.py:499
  139.1 11.3 %collective-permute-start.13 = (bf16[176,1024]{1,0:T(8,128)(2,1)S(1)}, bf16[176,1024]{1,0:T(8,128)(2,1)S(1)}, u32[]{:S(2)}, u32[]{:S(2)}) collective-permute-start(bf16[176,1024]{1,0:T(8,128)(2,1)S(1)} %collective-permute-done.8.refs_8_), channel_id=1, source_target_pairs={{0,1},{1,2},{2,3},{3,0},{4,5},{5,6},{6,7},{7,4},{8,9},{9,10},{10,1... | collective-permute-start | bytes 1081352 | tf_op jit(solution)/shard_map/ppermute | solution.py:481
  139.3 11.2 %collective-permute-start.14 = (bf16[176,1024]{1,0:T(8,128)(2,1)S(1)}, bf16[176,1024]{1,0:T(8,128)(2,1)S(1)}, u32[]{:S(2)}, u32[]{:S(2)}) collective-permute-start(bf16[176,1024]{1,0:T(8,128)(2,1)S(1)} %collective-permute-done.11.refs_5_), channel_id=1, source_target_pairs={{0,3},{1,0},{2,1},{3,2},{4,7},{5,4},{6,5},{7,6},{8,11},{9,8},{10,9... | collective-permute-start | bytes 1081352 | tf_op jit(solution)/shard_map/ppermute | solution.py:481
  161.4 16.1 %collective-permute-start.15 = (bf16[176,1024]{1,0:T(8,128)(2,1)S(1)}, bf16[176,1024]{1,0:T(8,128)(2,1)S(1)}, u32[]{:S(2)}, u32[]{:S(2)}) collective-permute-start(bf16[176,1024]{1,0:T(8,128)(2,1)S(1)} %get-tuple-element.49), channel_id=1, source_target_pairs={{0,1},{1,2},{2,3},{3,0},{4,5},{5,6},{6,7},{7,4},{8,9},{9,10},{10,1... | collective-permute-start | bytes 1081352 | tf_op jit(solution)/shard_map/ppermute | solution.py:481
  162.7 14.8 %collective-permute-start.16 = (bf16[176,1024]{1,0:T(8,128)(2,1)S(1)}, bf16[176,1024]{1,0:T(8,128)(2,1)S(1)}, u32[]{:S(2)}, u32[]{:S(2)}) collective-permute-start(bf16[176,1024]{1,0:T(8,128)(2,1)S(1)} %get-tuple-element.51), channel_id=1, source_target_pairs={{0,3},{1,0},{2,1},{3,2},{4,7},{5,4},{6,5},{7,6},{8,11},{9,8},{10,9... | collective-permute-start | bytes 1081352 | tf_op jit(solution)/shard_map/ppermute | solution.py:481
  174.8 12.8 %collective-permute-start.18 = (bf16[176,1024]{1,0:T(8,128)(2,1)S(1)}, bf16[176,1024]{1,0:T(8,128)(2,1)S(1)}, u32[]{:S(2)}, u32[]{:S(2)}) collective-permute-start(bf16[176,1024]{1,0:T(8,128)(2,1)S(1)} %get-tuple-element.53), channel_id=1, source_target_pairs={{0,1},{1,2},{2,3},{3,0},{4,5},{5,6},{6,7},{7,4},{8,9},{9,10},{10,1... | collective-permute-start | bytes 1081352 | tf_op jit(solution)/shard_map/ppermute | solution.py:481
  174.9 12.7 %collective-permute-start.19 = (bf16[176,1024]{1,0:T(8,128)(2,1)S(1)}, bf16[176,1024]{1,0:T(8,128)(2,1)S(1)}, u32[]{:S(2)}, u32[]{:S(2)}) collective-permute-start(bf16[176,1024]{1,0:T(8,128)(2,1)S(1)} %get-tuple-element.54), channel_id=1, source_target_pairs={{0,3},{1,0},{2,1},{3,2},{4,7},{5,4},{6,5},{7,6},{8,11},{9,8},{10,9... | collective-permute-start | bytes 1081352 | tf_op jit(solution)/shard_map/ppermute | solution.py:481
  177.8 15.2 %collective-permute-start.17 = (bf16[176,1024]{1,0:T(8,128)(2,1)S(1)}, bf16[176,1024]{1,0:T(8,128)(2,1)S(1)}, u32[]{:S(2)}, u32[]{:S(2)}) collective-permute-start(bf16[176,1024]{1,0:T(8,128)(2,1)S(1)} %get-tuple-element.52), channel_id=1, source_target_pairs={{0,1},{1,2},{2,3},{3,0},{4,5},{5,6},{6,7},{7,4},{8,9},{9,10},{10,1... | collective-permute-start | bytes 1081352 | tf_op jit(solution)/shard_map/ppermute | solution.py:481
  177.9 15.0 %copy-start.2 = (bf16[176,2048]{1,0:T(8,128)(2,1)S(1)}, bf16[176,2048]{1,0:T(8,128)(2,1)}, u32[]{:S(2)}) copy-start(bf16[176,2048]{1,0:T(8,128)(2,1)} %get-tuple-element.56.refs_5_) | copy-start | bytes 2162692
  177.9 15.0 %copy-start.8 = (f32[2048]{0:T(1024)S(1)}, f32[2048]{0:T(1024)}, u32[]{:S(2)}) copy-start(f32[2048]{0:T(1024)} %param.28) | copy-start | bytes 24580
  178.0 15.0 %collective-permute-start.20 = (bf16[176,1024]{1,0:T(8,128)(2,1)S(1)}, bf16[176,1024]{1,0:T(8,128)(2,1)S(1)}, u32[]{:S(2)}, u32[]{:S(2)}) collective-permute-start(bf16[176,1024]{1,0:T(8,128)(2,1)S(1)} %get-tuple-element.55), channel_id=1, source_target_pairs={{0,3},{1,0},{2,1},{3,2},{4,7},{5,4},{6,5},{7,6},{8,11},{9,8},{10,9... | collective-permute-start | bytes 1081352 | tf_op jit(solution)/shard_map/ppermute | solution.py:481
Sparse Core Ops, SparseCore 0:
  24.5 128.0 all-gather.1
